TPU v7x, 32 devices: a whole 2x2x4 slice. The times are simulated.
32 devices in a mesh: grp: 2 (over y), dp: 2 (over x), kv: 4 (over z), tp: 2 (over core).
Axes of the slice: x: 2, y: 2, z: 4, core: 2. Of those that a mesh axis runs over, the one named last changes fastest.
Arguments:
- residual_input: bfloat16 [128, 4096], P(('grp', 'dp', 'tp'), 'kv'), parts along dimension 0, may hold values from -6 to 6
- incoming_state: float32 [128, 16, 64, 128], P(('grp', 'kv'), ('dp', 'tp')), parts along dimension 0, may hold values from -4 to 4
- extra_log_decay: float32 [128, 1024], P(('grp', 'kv'), ('dp', 'tp')), parts along dimension 0, may hold values from -0.7 to 0
- leading_norm_gain: float32 [4096], P('kv'), may hold values from 0.1 to 1.9
- leading_gate_weight: bfloat16 [4096, 11264], P('kv', ('dp', 'tp')), may hold values from -0.09375 to 0.09375
- leading_up_weight: bfloat16 [4096, 11264], P('kv', ('dp', 'tp')), may hold values from -0.09375 to 0.09375
- leading_down_weight: bfloat16 [11264, 4096], P(('dp', 'tp'), 'kv'), may hold values from -0.0546875 to 0.0546875
- attention_norm_gain: float32 [4096], P('kv'), may hold values from 0.1 to 1.9
- query_projector: bfloat16 [4096, 1024], P('kv', ('dp', 'tp')), may hold values from -0.09375 to 0.09375
- key_projector: bfloat16 [4096, 1024], P('kv', ('dp', 'tp')), may hold values from -0.09375 to 0.09375
- value_projector: bfloat16 [4096, 2048], P('kv', ('dp', 'tp')), may hold values from -0.09375 to 0.09375
- output_gate_weight: bfloat16 [4096, 2048], P('kv', ('dp', 'tp')), may hold values from -0.09375 to 0.09375
- forget_weight: bfloat16 [4096, 1024], P('kv', ('dp', 'tp')), may hold values from -0.75 to 0.75
- head_norm_gain: float32 [128], replicated, may hold values from 0.1 to 1.9
- output_projector: bfloat16 [2048, 4096], P(('dp', 'tp'), 'kv'), may hold values from -0.125 to 0.125
- trailing_norm_gain: float32 [4096], P('kv'), may hold values from 0.1 to 1.9
- trailing_gate_weight: bfloat16 [4096, 11264], P('kv', ('dp', 'tp')), may hold values from -0.09375 to 0.09375
- trailing_up_weight: bfloat16 [4096, 11264], P('kv', ('dp', 'tp')), may hold values from -0.09375 to 0.09375
- trailing_down_weight: bfloat16 [11264, 4096], P(('dp', 'tp'), 'kv'), may hold values from -0.0546875 to 0.0546875
Outputs:
- result: bfloat16 [128, 4096], P(('grp', 'dp', 'tp'), 'kv'), parts along dimension 0
- new_state: float32 [128, 16, 64, 128], P(('grp', 'kv'), ('dp', 'tp')), parts along dimension 0
There are 2 independent parts, one for each index of `grp`. A program takes and returns all parts, laid end to end along the dimension named above; an argument that names none is the same for every part. Nothing has to cross between parts.
All inputs are finite; a program needn't handle non-finite values.
Results may differ from a plain program's by a relative error of at most 0.0095.
Values may be sent and summed in bfloat16 or wider, within the bound.
No kernel may reach another device: no remote copies, remote signals or barrier semaphores. Data moves between devices by JAX's collectives and lax.ppermute only.
A program may use at most 128 MiB of HBM per device.

v0:
```python
import jax
import jax.numpy as jnp
from jax import lax
from jax.sharding import PartitionSpec as P

D = 4096
KEY_CHANNELS = 64
VALUE_DIM = 128


epsilon = 1e-06


def batch_rows(row_block):
    return lax.all_gather(row_block, ("dp", "tp"), axis=0, tiled=True)


def channel_mixer(row_block, norm_gain, gate_matrix, up_matrix, down_matrix):
    gathered = batch_rows(row_block)
    widened = gathered.astype(jnp.float32)
    squares = jnp.sum(widened * widened, axis=1)
    scaled = (widened * norm_gain).astype(jnp.bfloat16)
    gate_part = jnp.dot(scaled, gate_matrix, preferred_element_type=jnp.float32)
    up_part = jnp.dot(scaled, up_matrix, preferred_element_type=jnp.float32)
    gate_sum, up_sum, row_total = (
        lax.psum_scatter(gate_part, "kv", scatter_dimension=0, tiled=True),
        lax.psum_scatter(up_part, "kv", scatter_dimension=0, tiled=True),
        lax.psum_scatter(squares, "kv", scatter_dimension=0, tiled=True),
    )
    decay_factor = lax.rsqrt(row_total / D + epsilon)[:, None]
    hidden_share = (jax.nn.silu(decay_factor * gate_sum) * (decay_factor * up_sum)).astype(
        jnp.bfloat16
    )
    hidden = lax.all_gather(hidden_share, "kv", axis=0, tiled=True)
    return lax.psum_scatter(
        jnp.dot(hidden, down_matrix, preferred_element_type=jnp.float32),
        ("dp", "tp"),
        scatter_dimension=0,
        tiled=True,
    )


def per_device(
    residual_input,
    incoming_state,
    extra_log_decay,
    leading_norm_gain,
    leading_gate_weight,
    leading_up_weight,
    leading_down_weight,
    attention_norm_gain,
    query_projector,
    key_projector,
    value_projector,
    output_gate_weight,
    forget_weight,
    head_norm_gain,
    output_projector,
    trailing_norm_gain,
    trailing_gate_weight,
    trailing_up_weight,
    trailing_down_weight,
):
    after_first = (
        residual_input.astype(jnp.float32)
        + 0.5
        * channel_mixer(
            residual_input,
            leading_norm_gain,
            leading_gate_weight,
            leading_up_weight,
            leading_down_weight,
        )
    ).astype(jnp.bfloat16)
    gathered = batch_rows(after_first)
    widened = gathered.astype(jnp.float32)
    squares = jnp.sum(widened * widened, axis=1)
    scaled = (widened * attention_norm_gain).astype(jnp.bfloat16)
    query_part = jnp.dot(scaled, query_projector, preferred_element_type=jnp.float32)
    key_part = jnp.dot(scaled, key_projector, preferred_element_type=jnp.float32)
    value_part = jnp.dot(scaled, value_projector, preferred_element_type=jnp.float32)
    gate_part = jnp.dot(scaled, output_gate_weight, preferred_element_type=jnp.float32)
    decay_part = jnp.dot(scaled, forget_weight, preferred_element_type=jnp.float32)
    query_sum, key_sum, value_sum, gate_sum, decay_total, row_total = (
        lax.psum_scatter(query_part, "kv", scatter_dimension=0, tiled=True),
        lax.psum_scatter(key_part, "kv", scatter_dimension=0, tiled=True),
        lax.psum_scatter(value_part, "kv", scatter_dimension=0, tiled=True),
        lax.psum_scatter(gate_part, "kv", scatter_dimension=0, tiled=True),
        lax.psum_scatter(decay_part, "kv", scatter_dimension=0, tiled=True),
        lax.psum_scatter(squares, "kv", scatter_dimension=0, tiled=True),
    )
    decay_factor = lax.rsqrt(row_total / D + epsilon)[:, None]
    row_count = query_sum.shape[0]
    heads_here = query_sum.shape[1] // KEY_CHANNELS
    queries = (decay_factor * query_sum).reshape(
        row_count, heads_here, KEY_CHANNELS
    ) * KEY_CHANNELS ** (-0.5)
    key_rows = (decay_factor * key_sum).reshape(row_count, heads_here, KEY_CHANNELS)
    value_rows = (decay_factor * value_sum).reshape(row_count, heads_here, VALUE_DIM)
    gate_rows = (decay_factor * gate_sum).reshape(row_count, heads_here, VALUE_DIM)
    decay_logarithm = (
        jax.nn.log_sigmoid(decay_factor * decay_total) / 16.0 + extra_log_decay
    ).reshape(row_count, heads_here, KEY_CHANNELS)
    new_state = (
        jnp.exp(decay_logarithm)[..., None] * incoming_state
        + key_rows[..., None] * value_rows[:, :, None, :]
    )
    read_out = jnp.einsum("bhk,bhkv->bhv", queries, new_state, precision=lax.Precision.HIGHEST)
    normed = read_out * lax.rsqrt(jnp.mean(read_out * read_out, axis=-1, keepdims=True) + epsilon)
    head_rows = (
        (normed * head_norm_gain * jax.nn.silu(gate_rows))
        .astype(jnp.bfloat16)
        .reshape(row_count, heads_here * VALUE_DIM)
    )
    all_heads = lax.all_gather(head_rows, "kv", axis=0, tiled=True)
    mixed_rows = lax.psum_scatter(
        jnp.dot(all_heads, output_projector, preferred_element_type=jnp.float32),
        ("dp", "tp"),
        scatter_dimension=0,
        tiled=True,
    )
    second = (after_first.astype(jnp.float32) + mixed_rows).astype(jnp.bfloat16)
    result = (
        second.astype(jnp.float32)
        + 0.5
        * channel_mixer(
            second,
            trailing_norm_gain,
            trailing_gate_weight,
            trailing_up_weight,
            trailing_down_weight,
        )
    ).astype(jnp.bfloat16)
    return (result, new_state)


def solution(mesh):
    return jax.shard_map(
        per_device,
        mesh=mesh,
        in_specs=(
            P(("grp", "dp", "tp"), "kv"),
            P(("grp", "kv"), ("dp", "tp"), None, None),
            P(("grp", "kv"), ("dp", "tp")),
            P("kv"),
            P("kv", ("dp", "tp")),
            P("kv", ("dp", "tp")),
            P(("dp", "tp"), "kv"),
            P("kv"),
            P("kv", ("dp", "tp")),
            P("kv", ("dp", "tp")),
            P("kv", ("dp", "tp")),
            P("kv", ("dp", "tp")),
            P("kv", ("dp", "tp")),
            P(),
            P(("dp", "tp"), "kv"),
            P("kv"),
            P("kv", ("dp", "tp")),
            P("kv", ("dp", "tp")),
            P(("dp", "tp"), "kv"),
        ),
        out_specs=(P(("grp", "dp", "tp"), "kv"), P(("grp", "kv"), ("dp", "tp"), None, None)),
        check_vma=False,
    )
```

profile of v0, /device:TPU:0, one launch (start us, length us, event | category | flops | bytes accessed | tf_op | source)
XLA Modules:
  0.0 359.7 jit_solution(16201497556303995588)
XLA Ops:
  7.2 6.9 %all_gather.18 = bf16[64,1024]{1,0:T(8,128)(2,1)S(1)} all-gather(bf16[16,1024]{1,0:T(8,128)(2,1)} %param.19), channel_id=1, replica_groups=mesh['grp'=2,'dp'=2,'kv'=4,'tp'=2] {'dp','tp'}, dimensions={0}, use_global_device_ids=true | all-gather | bytes 163840 | tf_op jit(solution)/shard_map/all_gather | solution.py:15
  14.1 4.6 %fusion.10 = f32[64,2816]{1,0:T(8,128)} fusion(bf16[1024,2816]{1,0:T(8,128)(2,1)} %param.24, bf16[64,1024]{1,0:T(8,128)(2,1)S(1)} %all_gather.18, f32[1024]{0:T(1024)} %param.22), kind=kOutput, calls=%fused_computation.17 | convolution fusion | flops 369295360 | bytes 6623232 | tf_op jit(solution)/shard_map/dot_general | solution.py:24
  18.8 4.6 %fusion.12 = f32[64,2816]{1,0:T(8,128)} fusion(bf16[1024,2816]{1,0:T(8,128)(2,1)} %param.23, bf16[64,1024]{1,0:T(8,128)(2,1)S(1)} %all_gather.18, f32[1024]{0:T(1024)S(1)} %copy-done.7), kind=kOutput, calls=%fused_computation.18 | convolution fusion | flops 369295360 | bytes 6623232 | tf_op jit(solution)/shard_map/dot_general | solution.py:23
  24.9 12.7 %all-reduce = f32[64]{0:T(128)S(1)} all-reduce(f32[64]{0:T(128)S(1)} %fusion), channel_id=2, replica_groups=mesh['grp'=2,'dp'=2,'kv'=4,'tp'=2] {'kv'}, use_global_device_ids=true, to_apply=%region_1.0.clone | all-reduce | flops 64 | bytes 512
  37.6 6.1 %reduce-scatter.15.cloned.1.call-done = f32[16,2816]{1,0:T(8,128)} async-done(((f32[64,2816]{1,0:T(8,128)}), f32[16,2816]{1,0:T(8,128)}) %reduce-scatter.15.cloned.1.call-update) | async-done | bytes 180240 | tf_op jit(solution)/shard_map/reduce_scatter | solution.py:27
  43.7 24.4 %reduce-scatter.13.cloned.1.call-done = f32[16,2816]{1,0:T(8,128)} async-done(((f32[64,2816]{1,0:T(8,128)}), f32[16,2816]{1,0:T(8,128)}) %reduce-scatter.13.cloned.1.call-update) | async-done | bytes 180240 | tf_op jit(solution)/shard_map/reduce_scatter | solution.py:26
  69.3 15.1 %all_gather.19 = bf16[64,2816]{1,0:T(8,128)(2,1)S(1)} all-gather(bf16[16,2816]{1,0:T(8,128)(2,1)S(1)} %multiply_convert_fusion.1), channel_id=1, replica_groups=mesh['grp'=2,'dp'=2,'kv'=4,'tp'=2] {'kv'}, dimensions={0}, use_global_device_ids=true | all-gather | bytes 450560 | tf_op jit(solution)/shard_map/all_gather | solution.py:34
  88.9 19.0 %reduce-scatter.17.cloned.1.call-done = f32[16,1024]{1,0:T(8,128)} async-done(((f32[64,1024]{1,0:T(8,128)}), f32[16,1024]{1,0:T(8,128)}) %reduce-scatter.17.cloned.1.call-update) | async-done | bytes 65552 | tf_op jit(solution)/shard_map/reduce_scatter | solution.py:35
  108.8 5.4 %all_gather.20 = bf16[64,1024]{1,0:T(8,128)(2,1)S(1)} all-gather(bf16[16,1024]{1,0:T(8,128)(2,1)S(1)} %add_convert_fusion.2), channel_id=1, replica_groups=mesh['grp'=2,'dp'=2,'kv'=4,'tp'=2] {'dp','tp'}, dimensions={0}, use_global_device_ids=true | all-gather | bytes 163840 | tf_op jit(solution)/shard_map/all_gather | solution.py:15
  121.3 11.8 %all-reduce.1 = f32[64]{0:T(128)S(1)} all-reduce(f32[64]{0:T(128)S(1)} %fusion.2), channel_id=6, replica_groups=mesh['grp'=2,'dp'=2,'kv'=4,'tp'=2] {'kv'}, use_global_device_ids=true, to_apply=%region_6.7.clone | all-reduce | flops 64 | bytes 512
  135.6 19.5 %reduce-scatter.23.cloned.1.call-done = f32[16,256]{1,0:T(8,128)} async-done(((f32[64,256]{1,0:T(8,128)}), f32[16,256]{1,0:T(8,128)}) %reduce-scatter.23.cloned.1.call-update) | async-done | bytes 16400 | tf_op jit(solution)/shard_map/reduce_scatter | solution.py:86
  155.2 19.6 %reduce-scatter.19.cloned.1.call-done = f32[16,256]{1,0:T(8,128)} async-done(((f32[64,256]{1,0:T(8,128)}), f32[16,256]{1,0:T(8,128)}) %reduce-scatter.19.cloned.1.call-update) | async-done | bytes 16400 | tf_op jit(solution)/shard_map/reduce_scatter | solution.py:85
  175.9 18.8 %reduce-scatter.27.cloned.1.call-done = f32[16,512]{1,0:T(8,128)} async-done(((f32[64,512]{1,0:T(8,128)}), f32[16,512]{1,0:T(8,128)}) %reduce-scatter.27.cloned.1.call-update) | async-done | bytes 32784 | tf_op jit(solution)/shard_map/reduce_scatter | solution.py:88
  194.7 20.5 %reduce-scatter.25.cloned.1.call-done = f32[16,512]{1,0:T(8,128)} async-done(((f32[64,512]{1,0:T(8,128)}), f32[16,512]{1,0:T(8,128)}) %reduce-scatter.25.cloned.1.call-update) | async-done | bytes 32784 | tf_op jit(solution)/shard_map/reduce_scatter | solution.py:87
  220.6 13.1 %all_gather.21 = bf16[64,512]{1,0:T(8,128)(2,1)S(1)} all-gather(bf16[16,512]{1,0:T(8,128)(2,1)S(1)} %bitcast.28), channel_id=1, replica_groups=mesh['grp'=2,'dp'=2,'kv'=4,'tp'=2] {'kv'}, dimensions={0}, use_global_device_ids=true | all-gather | bytes 81920 | tf_op jit(solution)/shard_map/all_gather | solution.py:115
  234.8 18.3 %reduce-scatter.29.cloned.1.call-done = f32[16,1024]{1,0:T(8,128)} async-done(((f32[64,1024]{1,0:T(8,128)}), f32[16,1024]{1,0:T(8,128)}) %reduce-scatter.29.cloned.1.call-update) | async-done | bytes 65552 | tf_op jit(solution)/shard_map/reduce_scatter | solution.py:116
  254.0 5.4 %all_gather.22 = bf16[64,1024]{1,0:T(8,128)(2,1)S(1)} all-gather(bf16[16,1024]{1,0:T(8,128)(2,1)S(1)} %add_convert_fusion.1), channel_id=1, replica_groups=mesh['grp'=2,'dp'=2,'kv'=4,'tp'=2] {'dp','tp'}, dimensions={0}, use_global_device_ids=true | all-gather | bytes 163840 | tf_op jit(solution)/shard_map/all_gather | solution.py:15
  259.4 4.6 %fusion.6 = f32[64,2816]{1,0:T(8,128)} fusion(bf16[1024,2816]{1,0:T(8,128)(2,1)} %param.36, bf16[64,1024]{1,0:T(8,128)(2,1)S(1)} %all_gather.22, f32[1024]{0:T(1024)S(1)} %copy-done.8), kind=kOutput, calls=%fused_computation.15 | convolution fusion | flops 369295360 | bytes 6623232 | tf_op jit(solution)/shard_map/dot_general | solution.py:24
  264.1 4.6 %fusion.8 = f32[64,2816]{1,0:T(8,128)} fusion(bf16[1024,2816]{1,0:T(8,128)(2,1)} %param.35, bf16[64,1024]{1,0:T(8,128)(2,1)S(1)} %all_gather.22, f32[1024]{0:T(1024)S(1)} %copy-done.8), kind=kOutput, calls=%fused_computation.16 | convolution fusion | flops 369295360 | bytes 6623232 | tf_op jit(solution)/shard_map/dot_general | solution.py:23
  268.9 12.0 %all-reduce.2 = f32[64]{0:T(128)S(1)} all-reduce(f32[64]{0:T(128)S(1)} %fusion.4), channel_id=13, replica_groups=mesh['grp'=2,'dp'=2,'kv'=4,'tp'=2] {'kv'}, use_global_device_ids=true, to_apply=%region_15.16.clone | all-reduce | flops 64 | bytes 512
  281.0 6.4 %reduce-scatter.33.cloned.1.call-done = f32[16,2816]{1,0:T(8,128)} async-done(((f32[64,2816]{1,0:T(8,128)}), f32[16,2816]{1,0:T(8,128)}) %reduce-scatter.33.cloned.1.call-update) | async-done | bytes 180240 | tf_op jit(solution)/shard_map/reduce_scatter | solution.py:27
  287.4 24.3 %reduce-scatter.31.cloned.1.call-done = f32[16,2816]{1,0:T(8,128)} async-done(((f32[64,2816]{1,0:T(8,128)}), f32[16,2816]{1,0:T(8,128)}) %reduce-scatter.31.cloned.1.call-update) | async-done | bytes 180240 | tf_op jit(solution)/shard_map/reduce_scatter | solution.py:26
  312.8 14.9 %all_gather.23 = bf16[64,2816]{1,0:T(8,128)(2,1)S(1)} all-gather(bf16[16,2816]{1,0:T(8,128)(2,1)S(1)} %multiply_convert_fusion), channel_id=1, replica_groups=mesh['grp'=2,'dp'=2,'kv'=4,'tp'=2] {'kv'}, dimensions={0}, use_global_device_ids=true | all-gather | bytes 450560 | tf_op jit(solution)/shard_map/all_gather | solution.py:34
  332.2 19.2 %reduce-scatter.35.cloned.1.call-done = f32[16,1024]{1,0:T(8,128)} async-done(((f32[64,1024]{1,0:T(8,128)}), f32[16,1024]{1,0:T(8,128)}) %reduce-scatter.35.cloned.1.call-update) | async-done | bytes 65552 | tf_op jit(solution)/shard_map/reduce_scatter | solution.py:35
  (80 shorter events, 32.8 us)
Async XLA Ops:
  7.2 226.6 %copy-start = (bf16[512,1024]{1,0:T(8,128)(2,1)S(1)}, bf16[512,1024]{1,0:T(8,128)(2,1)}, u32[]{:S(2)}) copy-start(bf16[512,1024]{1,0:T(8,128)(2,1)} %param.33) | copy-start | bytes 3145732
  7.2 11.6 %copy-start.7 = (f32[1024]{0:T(1024)S(1)}, f32[1024]{0:T(1024)}, u32[]{:S(2)}) copy-start(f32[1024]{0:T(1024)} %param.22) | copy-start | bytes 12292
  7.2 36.5 %reduce-scatter.15.cloned.1.call-start = ((), (), s32[]{:S(2)}) async-start(), calls=%async_computation.13 | async-start | bytes 901120 | tf_op jit(solution)/shard_map/reduce_scatter | solution.py:27
  14.1 9.4 %copy-start.10 = (u32[32]{0:T(128)S(1)}, u32[32]{0:T(128)}, u32[]{:S(2)}) copy-start(u32[32]{0:T(128)} %constant.31) | copy-start | bytes 388
  18.8 49.4 %reduce-scatter.13.cloned.1.call-start = ((), (), s32[]{:S(2)}) async-start(), calls=%async_computation.12 | async-start | bytes 901120 | tf_op jit(solution)/shard_map/reduce_scatter | solution.py:26
  23.4 84.5 %copy-start.4 = (bf16[16,1024]{1,0:T(8,128)(2,1)S(1)}, bf16[16,1024]{1,0:T(8,128)(2,1)}, u32[]{:S(2)}) copy-start(bf16[16,1024]{1,0:T(8,128)(2,1)} %param.19) | copy-start | bytes 98308
  23.4 90.8 %copy-start.5 = (f32[1024]{0:T(1024)S(1)}, f32[1024]{0:T(1024)}, u32[]{:S(2)}) copy-start(f32[1024]{0:T(1024)} %param.26) | copy-start | bytes 12292
  23.4 96.7 %copy-start.2 = (bf16[1024,512]{1,0:T(8,128)(2,1)S(1)}, bf16[1024,512]{1,0:T(8,128)(2,1)}, u32[]{:S(2)}) copy-start(bf16[1024,512]{1,0:T(8,128)(2,1)} %param.30) | copy-start | bytes 3145732
  23.5 84.5 %reduce-scatter.17.cloned.1.call-start = ((), (), s32[]{:S(2)}) async-start(), calls=%async_computation.14 | async-start | bytes 327680 | tf_op jit(solution)/shard_map/reduce_scatter | solution.py:35
  69.3 63.8 %copy-start.3 = (bf16[1024,512]{1,0:T(8,128)(2,1)S(1)}, bf16[1024,512]{1,0:T(8,128)(2,1)}, u32[]{:S(2)}) copy-start(bf16[1024,512]{1,0:T(8,128)(2,1)} %param.29) | copy-start | bytes 3145732
  84.4 90.4 %copy-start.6 = (f32[16,256]{1,0:T(8,128)S(1)}, f32[16,256]{1,0:T(8,128)}, u32[]{:S(2)}) copy-start(f32[16,256]{1,0:T(8,128)} %param.21) | copy-start | bytes 49156
  88.9 46.8 %reduce-scatter.21.cloned.1.call-start = ((), (), s32[]{:S(2)}) async-start(), calls=%async_computation.16 | async-start | bytes 81920 | tf_op jit(solution)/shard_map/reduce_scatter | solution.py:89
  116.2 104.3 %copy-start.9 = (f32[128]{0:T(128)S(1)}, f32[128]{0:T(128)}, u32[]{:S(2)}) copy-start(f32[128]{0:T(128)} %param.32) | copy-start | bytes 1540
  116.2 39.0 %reduce-scatter.23.cloned.1.call-start = ((), (), s32[]{:S(2)}) async-start(), calls=%async_computation.17 | async-start | bytes 81920 | tf_op jit(solution)/shard_map/reduce_scatter | solution.py:86
  118.1 56.6 %reduce-scatter.19.cloned.1.call-start = ((), (), s32[]{:S(2)}) async-start(), calls=%async_computation.15 | async-start | bytes 81920 | tf_op jit(solution)/shard_map/reduce_scatter | solution.py:85
  120.1 74.6 %reduce-scatter.27.cloned.1.call-start = ((), (), s32[]{:S(2)}) async-start(), calls=%async_computation.19 | async-start | bytes 163840 | tf_op jit(solution)/shard_map/reduce_scatter | solution.py:88
  121.1 138.3 %copy-start.8 = (f32[1024]{0:T(1024)S(1)}, f32[1024]{0:T(1024)}, u32[]{:S(2)}) copy-start(f32[1024]{0:T(1024)} %param.34) | copy-start | bytes 12292
  121.1 94.1 %reduce-scatter.25.cloned.1.call-start = ((), (), s32[]{:S(2)}) async-start(), calls=%async_computation.18 | async-start | bytes 163840 | tf_op jit(solution)/shard_map/reduce_scatter | solution.py:87
  134.0 119.1 %reduce-scatter.29.cloned.1.call-start = ((), (), s32[]{:S(2)}) async-start(), calls=%async_computation.20 | async-start | bytes 327680 | tf_op jit(solution)/shard_map/reduce_scatter | solution.py:116
  218.5 45.5 %copy-start.1 = (f32[16,4,64,128]{3,2,1,0:T(8,128)}, f32[16,4,64,128]{3,2,1,0:T(8,128)S(1)}, u32[]{:S(2)}) copy-start(f32[16,4,64,128]{3,2,1,0:T(8,128)S(1)} %multiply_add_fusion) | copy-start | bytes 6291460
  234.7 52.6 %reduce-scatter.33.cloned.1.call-start = ((), (), s32[]{:S(2)}) async-start(), calls=%async_computation.22 | async-start | bytes 901120 | tf_op jit(solution)/shard_map/reduce_scatter | solution.py:27
  264.0 47.6 %reduce-scatter.31.cloned.1.call-start = ((), (), s32[]{:S(2)}) async-start(), calls=%async_computation.21 | async-start | bytes 901120 | tf_op jit(solution)/shard_map/reduce_scatter | solution.py:26
  268.7 82.7 %reduce-scatter.35.cloned.1.call-start = ((), (), s32[]{:S(2)}) async-start(), calls=%async_computation.23 | async-start | bytes 327680 | tf_op jit(solution)/shard_map/reduce_scatter | solution.py:35
Sparse Core Ops, SparseCore 0:
  18.9 24.7 reduce-scatter.14
  46.0 22.0 reduce-scatter.12
  89.0 18.9 reduce-scatter.16
  116.3 19.3 reduce-scatter.20
  137.7 17.4 reduce-scatter.22
  157.3 17.4 reduce-scatter.18
  177.0 17.6 reduce-scatter.26
  197.5 17.6 reduce-scatter.24
  234.9 18.2 reduce-scatter.28
  264.1 23.1 reduce-scatter.32
  289.7 21.9 reduce-scatter.30
  332.3 18.9 reduce-scatter.34
where the time goes:
time: 361 us; the launch traced here: 360 us
  waiting for transfers between devices  198 us (55%)
  blocking collectives  97.3 us (27%)
  matrix products  37.8 us (10%)
  between operations  15 us (4%)
  other arithmetic  10.4 us (3%)
    reduce_scatter x2, waiting for transfers between devices, channel_mixer(): lax.psum_scatter(gate_part, 'kv', scatter_dimension=0, tiled=True)  48.7 us
    reduce_scatter x2, waiting for transfers between devices, channel_mixer(): lax.psum_scatter(jnp.dot(hidden, down_matrix, preferred_element_type=jnp....  38.2 us
    unnamed x3, blocking collectives  36.4 us
    all_gather x2, blocking collectives, channel_mixer(): hidden = lax.all_gather(hidden_share, 'kv', axis=0, tiled=True)  30 us
    reduce_scatter x1, waiting for transfers between devices, per_device(): lax.psum_scatter(value_part, 'kv', scatter_dimension=0, tiled=True)  20.5 us
    reduce_scatter x1, waiting for transfers between devices, per_device(): lax.psum_scatter(query_part, 'kv', scatter_dimension=0, tiled=True)  19.6 us
    reduce_scatter x1, waiting for transfers between devices, per_device(): lax.psum_scatter(key_part, 'kv', scatter_dimension=0, tiled=True)  19.5 us
    reduce_scatter x1, waiting for transfers between devices, per_device(): lax.psum_scatter(gate_part, 'kv', scatter_dimension=0, tiled=True)  18.8 us
  transfers between devices with their start and end apart: 12, of which 12 were waited for; matrix products, arithmetic and copies ran while one was open for 5% of the time, Pallas kernels for 0%

commit v1 on v0

v1 whole, which is shorter than its diff:
```python
import functools

import jax
import jax.numpy as jnp
from jax import lax
from jax.experimental import pallas as pl
from jax.experimental.pallas import tpu as pltpu
from jax.sharding import PartitionSpec as P

KEY_CHANNELS = 64
VALUE_DIM = 128
EPSILON = 1e-06
LANES = 128
F32 = jnp.float32
BF16 = jnp.bfloat16

VMEM = pl.BlockSpec(memory_space=pltpu.VMEM)
HBM = pl.BlockSpec(memory_space=pl.ANY)


def padded(width):
    return -(-width // LANES) * LANES


def column_step(width):
    return 256 if width % 256 == 0 else width


def linear_index(axes):
    place = 0
    for axis in axes:
        place = place * lax.axis_size(axis) + lax.axis_index(axis)
    return place


def rows_at(block, height):
    return pl.ds(pl.multiple_of(block * height, height), height)


def swap(array, axes, size, offset):
    return lax.ppermute(array, axes, [(i, i ^ offset) for i in range(size)])


def swaps(arrays, axes, size):
    return [swap(array, axes, size, k + 1) for k, array in enumerate(arrays)]


def split_square_sum(rows):
    total = jnp.sum(rows * rows, axis=1, keepdims=True)
    high = total.astype(BF16)
    low = (total - high.astype(F32)).astype(BF16)
    lane = lax.broadcasted_iota(jnp.int32, (rows.shape[0], LANES), 1)
    return jnp.where(lane < LANES // 2, high.astype(F32), low.astype(F32)).astype(BF16)


def stream_columns(weights, buffers, semaphores):
    copies, at = [], 0
    for weight, buffer in zip(weights, buffers):
        width = weight.shape[1]
        step = column_step(width)
        pieces = []
        for low in range(0, width, step):
            piece = (slice(None), pl.ds(low, step))
            copy = pltpu.make_async_copy(weight.at[piece], buffer.at[piece], semaphores.at[at])
            copy.start()
            pieces.append((low, step, copy))
            at += 1
        copies.append(pieces)
    return copies


def count_pieces(weights):
    return sum(w.shape[1] // column_step(w.shape[1]) for w in weights)


def first_mixer_kernel(counts, *refs):
    n_dt, names = counts
    own, refs = refs[0], refs[1:]
    others, refs = refs[: n_dt - 1], refs[n_dt - 1 :]
    gain, gate, up = refs[:3]
    outs = refs[3 : 3 + n_dt]
    gathered = refs[3 + n_dt]
    gate_buffer, up_buffer, semaphores = refs[4 + n_dt :]
    copies = stream_columns((gate, up), (gate_buffer, up_buffer), semaphores)
    height = own.shape[0]
    dt_axes, kv_axes = names
    place = linear_index(dt_axes) ^ linear_index(kv_axes)
    for k, block in enumerate((own, *others)):
        gathered[rows_at(place ^ k, height), :] = block[...]
    widened = gathered[...].astype(F32)
    mix_rows(widened, gain, (gate_buffer, up_buffer), copies, outs)


def mix_rows(widened, gain, buffers, copies, outs):
    scaled = (widened * gain[...]).astype(BF16)
    height = outs[0].shape[0]
    base = 0
    for buffer, pieces in zip(buffers, copies):
        for low, step, copy in pieces:
            copy.wait()
            product = jnp.dot(scaled, buffer[:, low : low + step], preferred_element_type=F32).astype(BF16)
            for k, out in enumerate(outs):
                out[:, base + low : base + low + step] = product[k * height : (k + 1) * height]
        base += padded(buffer.shape[1])
    squares = split_square_sum(widened)
    for k, out in enumerate(outs):
        out[:, base : base + LANES] = squares[k * height : (k + 1) * height]


def project_kernel(half, n_parts, n_weights, n_outs, *refs):
    residual, refs = refs[0], refs[1:]
    parts, refs = refs[:n_parts], refs[n_parts:]
    gain, refs = refs[0], refs[1:]
    weights, refs = refs[:n_weights], refs[n_weights:]
    outs, refs = refs[:n_outs], refs[n_outs:]
    stream, refs = refs[0], refs[1:]
    buffers, semaphores = refs[:n_weights], refs[n_weights]
    copies = stream_columns(weights, buffers, semaphores)
    total = parts[0][...].astype(F32)
    for part in parts[1:]:
        total = total + part[...].astype(F32)
    rounded = (residual[...].astype(F32) + half * total).astype(BF16)
    stream[...] = rounded
    mix_rows(rounded.astype(F32), gain, buffers, copies, outs)


def hidden_kernel(features, n_parts, *refs):
    parts, out = refs[:n_parts], refs[n_parts]
    width = out.shape[1]
    gap = padded(width)

    def summed(low, size):
        total = parts[0][:, low : low + size].astype(F32)
        for part in parts[1:]:
            total = total + part[:, low : low + size].astype(F32)
        return total

    tail = summed(2 * gap, LANES)
    square_sum = tail[:, :1] + tail[:, LANES // 2 : LANES // 2 + 1]
    scale = lax.rsqrt(square_sum / features + EPSILON)
    step = column_step(width)
    for low in range(0, width, step):
        gate = scale * summed(low, step)
        up = scale * summed(gap + low, step)
        out[:, low : low + step] = (jax.nn.silu(gate) * up).astype(BF16)


def down_kernel(n_blocks, *refs):
    blocks, weight = refs[:n_blocks], refs[n_blocks]
    out, rows, buffer, semaphores = refs[n_blocks + 1 :]
    (pieces,) = stream_columns((weight,), (buffer,), semaphores)
    height = blocks[0].shape[0]
    for k, block in enumerate(blocks):
        rows[k * height : (k + 1) * height, :] = block[...]
    for low, step, copy in pieces:
        copy.wait()
        product = jnp.dot(rows[...], buffer[:, low : low + step], preferred_element_type=F32)
        out[:, low : low + step] = product.astype(BF16)


def attention_kernel(features, n_parts, *refs):
    parts, refs = refs[:n_parts], refs[n_parts:]
    extra_decay, state, norm_gain, head_rows, new_state, read, columns = refs
    rows, heads = state.shape[0], state.shape[1]
    keys, values = heads * KEY_CHANNELS, heads * VALUE_DIM
    gap, value_gap = padded(keys), padded(values)

    def summed(low, size):
        total = parts[0][:, low : low + size].astype(F32)
        for part in parts[1:]:
            total = total + part[:, low : low + size].astype(F32)
        return total

    tail = summed(3 * gap + 2 * value_gap, LANES)
    square_sum = tail[:, :1] + tail[:, LANES // 2 : LANES // 2 + 1]
    scale = lax.rsqrt(square_sum / features + EPSILON)
    queries = scale * summed(0, keys) * KEY_CHANNELS ** (-0.5)
    key_rows = scale * summed(gap, keys)
    forget = scale * summed(2 * gap, keys)
    value_rows = scale * summed(3 * gap, values)
    log_sigmoid = jnp.minimum(forget, 0.0) - jnp.log1p(jnp.exp(-jnp.abs(forget)))
    decay = jnp.exp(log_sigmoid / 16.0 + extra_decay[...])
    columns[...] = jnp.zeros_like(columns)
    columns[0:rows, :keys] = decay
    columns[rows : 2 * rows, :keys] = key_rows
    columns[2 * rows : 3 * rows, :keys] = queries
    upright = columns[...].T
    for head in range(heads):
        channels = slice(head * KEY_CHANNELS, (head + 1) * KEY_CHANNELS)
        lanes = slice(head * VALUE_DIM, (head + 1) * VALUE_DIM)
        for row in range(rows):
            kept = upright[channels, row : row + 1] * state[row, head]
            added = upright[channels, rows + row : rows + row + 1] * value_rows[row : row + 1, lanes]
            fresh = kept + added
            new_state[row, head] = fresh
            taken = upright[channels, 2 * rows + row : 2 * rows + row + 1] * fresh
            read[row : row + 1, lanes] = jnp.sum(taken, axis=0, keepdims=True)
    gates = scale * summed(3 * gap + value_gap, values)
    for head in range(heads):
        lanes = slice(head * VALUE_DIM, (head + 1) * VALUE_DIM)
        one = read[:, lanes]
        mean = jnp.mean(one * one, axis=-1, keepdims=True)
        normed = one * lax.rsqrt(mean + EPSILON) * norm_gain[...]
        head_rows[:, lanes] = (normed * jax.nn.silu(gates[:, lanes])).astype(BF16)


def result_kernel(n_parts, names, *refs):
    stream, parts, out = refs[0], refs[1 : 1 + n_parts], refs[1 + n_parts]
    total = parts[0][...].astype(F32)
    for part in parts[1:]:
        total = total + part[...].astype(F32)
    place = linear_index(names[0]) ^ linear_index(names[1])
    own = stream[rows_at(place, out.shape[0]), :].astype(F32)
    out[...] = (own + 0.5 * total).astype(BF16)


def scatter_down_kernel(n_blocks, names, *refs):
    blocks, weight = refs[:n_blocks], refs[n_blocks]
    outs = refs[n_blocks + 1 : 2 * n_blocks + 1]
    rows, product, buffer, semaphores = refs[2 * n_blocks + 1 :]
    (pieces,) = stream_columns((weight,), (buffer,), semaphores)
    height = blocks[0].shape[0]
    for k, block in enumerate(blocks):
        rows[k * height : (k + 1) * height, :] = block[...]
    place = linear_index(names[0]) ^ linear_index(names[1])
    for low, step, copy in pieces:
        copy.wait()
        product[...] = jnp.dot(rows[...], buffer[:, low : low + step], preferred_element_type=F32).astype(BF16)
        for k, out in enumerate(outs):
            out[:, low : low + step] = product[rows_at(place ^ k, height), :]


def call(kernel, name, outs, in_specs, scratch, limit):
    return pl.pallas_call(
        kernel,
        out_shape=outs,
        in_specs=in_specs,
        out_specs=jax.tree.map(lambda _: VMEM, outs),
        scratch_shapes=scratch,
        compiler_params=pltpu.CompilerParams(vmem_limit_bytes=limit),
        name=name,
    )


def weight_scratch(weights):
    return [pltpu.VMEM(w.shape, w.dtype) for w in weights] + [pltpu.SemaphoreType.DMA((count_pieces(weights),))]


def weight_bytes(weights):
    return sum(2 * w.shape[0] * padded(w.shape[1]) for w in weights)


MIB = 1 << 20


def per_device(
    n_dt,
    n_kv,
    residual_input,
    incoming_state,
    extra_log_decay,
    leading_norm_gain,
    leading_gate_weight,
    leading_up_weight,
    leading_down_weight,
    attention_norm_gain,
    query_projector,
    key_projector,
    value_projector,
    output_gate_weight,
    forget_weight,
    head_norm_gain,
    output_projector,
    trailing_norm_gain,
    trailing_gate_weight,
    trailing_up_weight,
    trailing_down_weight,
):
    dt, kv = ("dp", "tp"), ("kv",)
    names = (dt, kv)
    height, width = residual_input.shape
    features = width * n_kv
    rows = height * n_dt
    shape = jax.ShapeDtypeStruct

    def payload(weights):
        span = sum(padded(w.shape[1]) for w in weights) + LANES
        return [shape((height, span), BF16)] * n_kv

    def spread(block):
        return [block] + [swap(block, kv, n_kv, k) for k in range(1, n_kv)]

    def collect(blocks):
        return [blocks[0]] + swaps(blocks[1:], kv, n_kv)

    def total_parts(part):
        offset = 1
        while 2 * offset < n_dt:
            part = (part.astype(F32) + swap(part, dt, n_dt, offset).astype(F32)).astype(BF16)
            offset *= 2
        return [part, swap(part, dt, n_dt, offset)]

    def project_rows(half, residual, parts, gain, weights, name):
        return call(
            functools.partial(project_kernel, half, len(parts), len(weights), n_kv),
            name,
            payload(weights) + [shape((rows, width), BF16)],
            [VMEM] * (2 + len(parts)) + [HBM] * len(weights),
            weight_scratch(weights),
            weight_bytes(weights) + 12 * MIB,
        )(residual, *parts, gain.reshape(1, width), *weights)

    def hidden_rows(blocks, units):
        return call(
            functools.partial(hidden_kernel, features, n_kv),
            "hidden",
            shape((height, units), BF16),
            [VMEM] * n_kv,
            [],
            8 * MIB,
        )(*blocks)

    def down(blocks, weight, name):
        return call(
            functools.partial(down_kernel, n_kv),
            name,
            shape((rows, weight.shape[1]), BF16),
            [VMEM] * n_kv + [HBM],
            [pltpu.VMEM((rows, weight.shape[0]), BF16)] + weight_scratch((weight,)),
            weight_bytes((weight,)) + 8 * MIB,
        )(*blocks, weight)

    first = (leading_gate_weight, leading_up_weight)
    arrived = [swap(residual_input, dt, n_dt, k) for k in range(1, n_dt)]
    *blocks, gathered = call(
        functools.partial(first_mixer_kernel, (n_dt, names)),
        "first_mixer",
        payload(first) + [shape((rows, width), BF16)],
        [VMEM] * (n_dt + 1) + [HBM] * 2,
        weight_scratch(first),
        weight_bytes(first) + 12 * MIB,
    )(residual_input, *arrived, leading_norm_gain.reshape(1, width), *first)
    units = leading_gate_weight.shape[1]
    hidden = spread(hidden_rows(collect(blocks), units))
    parts = total_parts(down(hidden, leading_down_weight, "first_down"))

    mixed = (query_projector, key_projector, forget_weight, value_projector, output_gate_weight)
    *blocks, after_first = project_rows(0.5, gathered, parts, attention_norm_gain, mixed, "attention_in")
    blocks = collect(blocks)
    heads = incoming_state.shape[1]
    head_rows, new_state = call(
        functools.partial(attention_kernel, features, n_kv),
        "attention",
        [shape((height, heads * VALUE_DIM), BF16), shape(incoming_state.shape, F32)],
        [VMEM] * (n_kv + 3),
        [
            pltpu.VMEM((height, heads * VALUE_DIM), F32),
            pltpu.VMEM((padded(3 * height), padded(heads * KEY_CHANNELS)), F32),
        ],
        24 * MIB,
    )(*blocks, extra_log_decay, incoming_state, head_norm_gain.reshape(1, VALUE_DIM))
    parts = total_parts(down(spread(head_rows), output_projector, "attention_out"))

    last = (trailing_gate_weight, trailing_up_weight)
    *blocks, second = project_rows(1.0, after_first, parts, trailing_norm_gain, last, "last_mixer")
    hidden = spread(hidden_rows(collect(blocks), units))
    parts = call(
        functools.partial(scatter_down_kernel, n_kv, names),
        "last_down",
        [shape((height, width), BF16)] * n_dt,
        [VMEM] * n_kv + [HBM],
        [
            pltpu.VMEM((rows, trailing_down_weight.shape[0]), BF16),
            pltpu.VMEM((rows, column_step(width)), BF16),
        ]
        + weight_scratch((trailing_down_weight,)),
        weight_bytes((trailing_down_weight,)) + 8 * MIB,
    )(*hidden, trailing_down_weight)
    parts = [parts[0]] + swaps(parts[1:], dt, n_dt)
    result = call(
        functools.partial(result_kernel, n_dt, names),
        "result",
        shape((height, width), BF16),
        [VMEM] * (n_dt + 1),
        [],
        8 * MIB,
    )(second, *parts)
    return (result, new_state)


def solution(mesh):
    n_dt = mesh.shape["dp"] * mesh.shape["tp"]
    n_kv = mesh.shape["kv"]
    assert n_dt == n_kv and n_kv & (n_kv - 1) == 0
    return jax.shard_map(
        functools.partial(per_device, n_dt, n_kv),
        mesh=mesh,
        in_specs=(
            P(("grp", "dp", "tp"), "kv"),
            P(("grp", "kv"), ("dp", "tp"), None, None),
            P(("grp", "kv"), ("dp", "tp")),
            P("kv"),
            P("kv", ("dp", "tp")),
            P("kv", ("dp", "tp")),
            P(("dp", "tp"), "kv"),
            P("kv"),
            P("kv", ("dp", "tp")),
            P("kv", ("dp", "tp")),
            P("kv", ("dp", "tp")),
            P("kv", ("dp", "tp")),
            P("kv", ("dp", "tp")),
            P(),
            P(("dp", "tp"), "kv"),
            P("kv"),
            P("kv", ("dp", "tp")),
            P("kv", ("dp", "tp")),
            P(("dp", "tp"), "kv"),
        ),
        out_specs=(P(("grp", "dp", "tp"), "kv"), P(("grp", "kv"), ("dp", "tp"), None, None)),
        check_vma=False,
    )
```

time: 361 us -> 136 us (0.38)
  waiting for transfers between devices: 198 us -> 65.1 us
  blocking collectives: 97.3 us -> 0 us
  matrix products: 37.8 us -> 0 us
  starting transfers between devices: 0.5 us -> 34.8 us
  Pallas kernels: 0 us -> 28.3 us
  between operations: 15 us -> 0.93 us
  other arithmetic: 10.4 us -> 0.08 us
  local copies, waits for them, and re-layouts: 0.92 us -> 6.81 us
    reduce_scatter x12 -> x0, waiting for transfers between devices: 198 us -> none  [the longest x2 48.7 us: channel_mixer(): lax.psum_scatter(gate_part, 'kv', scatter_dimension=0, tiled=True)]
    ppermute x0 -> x28, waiting for transfers between devices: none -> 65.1 us  [swap(): return lax.ppermute(array, axes, [(i, i ^ offset) for i in range(size)])]
    all_gather x6 -> x0, blocking collectives: 60.9 us -> none  [the longest x2 30 us: channel_mixer(): hidden = lax.all_gather(hidden_share, 'kv', axis=0, tiled=True)]
    dot_general x13 -> x0, matrix products: 37.8 us -> none  [the longest x2 9.25 us: channel_mixer(): up_part = jnp.dot(scaled, up_matrix, preferred_element_type=jnp.float32)]
    unnamed x3 -> x0, blocking collectives: 36.4 us -> none
    ppermute x0 -> x28, starting transfers between devices: none -> 34.8 us  [swap(): return lax.ppermute(array, axes, [(i, i ^ offset) for i in range(size)])]
    pallas_call x0 -> x10, Pallas kernels: none -> 28.3 us  [the longest x2 9.57 us: project_rows(): call(functools.partial(project_kernel, half, len(parts), len(weights), n_...]
    unnamed x24 -> x44, local copies, waits for them, and re-layouts: 0.65 us -> 6.81 us
  transfers between devices with their start and end apart: 12 -> 28, of which waited for: 12 -> 21; matrix products, arithmetic and copies ran while one was open for 5% -> 0% of each run, Pallas kernels for 0% -> 0%
where the time goes in v1:
time: 136 us
  waiting for transfers between devices  65.1 us (48%)
  starting transfers between devices  34.8 us (26%)
  Pallas kernels  28.3 us (21%)
  local copies, waits for them, and re-layouts  6.81 us (5%)
    ppermute x28, waiting for transfers between devices, swap(): return lax.ppermute(array, axes, [(i, i ^ offset) for i in range(size)])  65.1 us
    ppermute x28, starting transfers between devices, swap(): return lax.ppermute(array, axes, [(i, i ^ offset) for i in range(size)])  34.8 us
    pallas_call x2, Pallas kernels, project_rows(): call(functools.partial(project_kernel, half, len(parts), len(weights), n_...  9.57 us
    pallas_call x1, Pallas kernels, per_device(): call(functools.partial(first_mixer_kernel, (n_dt, names)), 'first_mixer',...  7.09 us
    unnamed x44, local copies, waits for them, and re-layouts  6.81 us
    pallas_call x2, Pallas kernels, down(): call(functools.partial(down_kernel, n_kv), name, shape((rows, weight.shap...  3.97 us
    pallas_call x1, Pallas kernels, per_device(): call(functools.partial(attention_kernel, features, n_kv), 'attention', [s...  3.6 us
    pallas_call x1, Pallas kernels, per_device(): call(functools.partial(scatter_down_kernel, n_kv, names), 'last_down', [s...  2.98 us
  transfers between devices with their start and end apart: 28, of which 21 were waited for; matrix products, arithmetic and copies ran while one was open for 0% of the time, Pallas kernels for 0%

profile of v1, /device:TPU:0, one launch (start us, length us, event | category | flops | bytes accessed | tf_op | source)
XLA Modules:
  0.0 136.0 jit_solution(4713485705078969852)
XLA Ops:
  0.6 3.0 %collective-permute-start.1 = (bf16[16,1024]{1,0:T(8,128)(2,1)}, bf16[16,1024]{1,0:T(8,128)(2,1)S(1)}, u32[]{:S(2)}, u32[]{:S(2)}) collective-permute-start(bf16[16,1024]{1,0:T(8,128)(2,1)} %refs_0_.1), channel_id=1, source_target_pairs={{0,8},{1,9},{8,0},{9,1},{2,10},{3,11},{10,2},{11,3},{4,12},{5,13},... | collective-permute-start | bytes 98312 | tf_op jit(solution)/shard_map/ppermute | solution.py:41
  7.2 2.6 %copy-done.1 = bf16[1024,2816]{1,0:T(8,128)(2,1)S(1)} copy-done((bf16[1024,2816]{1,0:T(8,128)(2,1)S(1)}, bf16[1024,2816]{1,0:T(8,128)(2,1)}, u32[]{:S(2)}) %copy-start.1) | copy-done | bytes 5767192
  9.9 2.6 %copy-done.2 = bf16[1024,2816]{1,0:T(8,128)(2,1)S(1)} copy-done((bf16[1024,2816]{1,0:T(8,128)(2,1)S(1)}, bf16[1024,2816]{1,0:T(8,128)(2,1)}, u32[]{:S(2)}) %copy-start.2) | copy-done | bytes 5767192
  13.9 7.1 %first_mixer.1 = (bf16[16,5760]{1,0:T(8,128)(2,1)S(1)}, bf16[16,5760]{1,0:T(8,128)(2,1)S(1)}, bf16[16,5760]{1,0:T(8,128)(2,1)S(1)}, bf16[16,5760]{1,0:T(8,128)(2,1)S(1)}, bf16[64,1024]{1,0:T(8,128)(2,1)S(1)}) custom-call(bf16[16,1024]{1,0:T(8,128)(2,1)S(1)} %copy-done.10, bf16[16,1024]{1,0:T(8,128)(2,1)S(1)} %collective-permute-done.refs_1_, ...), custom_call_target="tpu_custom_call" | custom-call | tf_op jit(solution)/shard_map/first_mixer/pallas_call | solution.py:335
  22.8 2.6 %collective-permute-start.4 = (bf16[16,5760]{1,0:T(8,128)(2,1)S(1)}, bf16[16,5760]{1,0:T(8,128)(2,1)S(1)}, u32[]{:S(2)}, u32[]{:S(2)}) collective-permute-start(bf16[16,5760]{1,0:T(8,128)(2,1)S(1)} %get-tuple-element.26), channel_id=1, source_target_pairs={{0,4},{2,6},{4,0},{6,2},{1,5},{3,7},{5,1},{7,3},{8,12},{10,14},{12... | collective-permute-start | bytes 552968 | tf_op jit(solution)/shard_map/ppermute | solution.py:41
  25.6 6.2 %collective-permute-done.3.refs_1_ = bf16[16,5760]{1,0:T(8,128)(2,1)S(1)} collective-permute-done((bf16[16,5760]{1,0:T(8,128)(2,1)S(1)}, bf16[16,5760]{1,0:T(8,128)(2,1)S(1)}, u32[]{:S(2)}, u32[]{:S(2)}) %collective-permute-start.3) | collective-permute-done | bytes 184352 | tf_op jit(solution)/shard_map/ppermute | solution.py:41
  31.8 7.4 %collective-permute-done.4.refs_2_ = bf16[16,5760]{1,0:T(8,128)(2,1)S(1)} collective-permute-done((bf16[16,5760]{1,0:T(8,128)(2,1)S(1)}, bf16[16,5760]{1,0:T(8,128)(2,1)S(1)}, u32[]{:S(2)}, u32[]{:S(2)}) %collective-permute-start.4) | collective-permute-done | bytes 184352 | tf_op jit(solution)/shard_map/ppermute | solution.py:41
  39.4 2.5 %collective-permute-start.8 = (bf16[16,2816]{1,0:T(8,128)(2,1)S(1)}, bf16[16,2816]{1,0:T(8,128)(2,1)S(1)}, u32[]{:S(2)}, u32[]{:S(2)}) collective-permute-start(bf16[16,2816]{1,0:T(8,128)(2,1)S(1)} %hidden.2.refs_0_), channel_id=1, source_target_pairs={{0,6},{2,4},{4,2},{6,0},{1,7},{3,5},{5,3},{7,1},{8,14},{10,12},{12... | collective-permute-start | bytes 270344 | tf_op jit(solution)/shard_map/ppermute | solution.py:41
  41.9 2.7 %collective-permute-start.7 = (bf16[16,2816]{1,0:T(8,128)(2,1)S(1)}, bf16[16,2816]{1,0:T(8,128)(2,1)S(1)}, u32[]{:S(2)}, u32[]{:S(2)}) collective-permute-start(bf16[16,2816]{1,0:T(8,128)(2,1)S(1)} %hidden.2.refs_0_), channel_id=1, source_target_pairs={{0,4},{2,6},{4,0},{6,2},{1,5},{3,7},{5,1},{7,3},{8,12},{10,14},{12... | collective-permute-start | bytes 270344 | tf_op jit(solution)/shard_map/ppermute | solution.py:41
  45.9 5.5 %collective-permute-done.7.refs_2_ = bf16[16,2816]{1,0:T(8,128)(2,1)S(1)} collective-permute-done((bf16[16,2816]{1,0:T(8,128)(2,1)S(1)}, bf16[16,2816]{1,0:T(8,128)(2,1)S(1)}, u32[]{:S(2)}, u32[]{:S(2)}) %collective-permute-start.7) | collective-permute-done | bytes 90144 | tf_op jit(solution)/shard_map/ppermute | solution.py:41
  51.4 3.0 %first_down.1 = bf16[64,1024]{1,0:T(8,128)(2,1)S(1)} custom-call(bf16[16,2816]{1,0:T(8,128)(2,1)S(1)} %hidden.2.refs_0_, bf16[16,2816]{1,0:T(8,128)(2,1)S(1)} %collective-permute-done.6.refs_1_, bf16[16,2816]{1,0:T(8,128)(2,1)S(1)} %collective-permute-done.7.refs_2_, bf16[16,2816]{1,0:T(8,128)(2,1)S(1)} %collective-permute-done.8.refs_3_, ...), custom_call_target="tpu_custom_call" | custom-call | tf_op jit(solution)/shard_map/first_down/pallas_call | solution.py:324
  56.1 5.3 %collective-permute-done.10.refs_2_ = bf16[64,1024]{1,0:T(8,128)(2,1)S(1)} collective-permute-done((bf16[64,1024]{1,0:T(8,128)(2,1)S(1)}, bf16[64,1024]{1,0:T(8,128)(2,1)S(1)}, u32[]{:S(2)}, u32[]{:S(2)}) %collective-permute-start.10) | collective-permute-done | bytes 131104 | tf_op jit(solution)/shard_map/ppermute | solution.py:41
  63.8 3.0 %collective-permute-start.12 = (bf16[16,1920]{1,0:T(8,128)(2,1)S(1)}, bf16[16,1920]{1,0:T(8,128)(2,1)S(1)}, u32[]{:S(2)}, u32[]{:S(2)}) collective-permute-start(bf16[16,1920]{1,0:T(8,128)(2,1)S(1)} %get-tuple-element.31), channel_id=1, source_target_pairs={{0,4},{2,6},{4,0},{6,2},{1,5},{3,7},{5,1},{7,3},{8,12},{10,14},{12... | collective-permute-start | bytes 184328 | tf_op jit(solution)/shard_map/ppermute | solution.py:41
  69.8 3.0 %collective-permute-done.13.refs_3_ = bf16[16,1920]{1,0:T(8,128)(2,1)S(1)} collective-permute-done((bf16[16,1920]{1,0:T(8,128)(2,1)S(1)}, bf16[16,1920]{1,0:T(8,128)(2,1)S(1)}, u32[]{:S(2)}, u32[]{:S(2)}) %collective-permute-start.13) | collective-permute-done | bytes 61472 | tf_op jit(solution)/shard_map/ppermute | solution.py:41
  72.9 3.6 %attention.1 = (bf16[16,512]{1,0:T(8,128)(2,1)S(1)}, f32[16,4,64,128]{3,2,1,0:T(8,128)}) custom-call(bf16[16,1920]{1,0:T(8,128)(2,1)S(1)} %get-tuple-element.29.refs_0_, bf16[16,1920]{1,0:T(8,128)(2,1)S(1)} %collective-permute-done.11.refs_1_, bf16[16,1920]{1,0:T(8,128)(2,1)S(1)} %collective-permute-done.12.refs_2_, ...), custom_call_target="tpu_custom_call" | custom-call | tf_op jit(solution)/shard_map/attention/pallas_call | solution.py:351
  77.9 3.0 %collective-permute-start.14 = (bf16[16,512]{1,0:T(8,128)(2,1)S(1)}, bf16[16,512]{1,0:T(8,128)(2,1)S(1)}, u32[]{:S(2)}, u32[]{:S(2)}) collective-permute-start(bf16[16,512]{1,0:T(8,128)(2,1)S(1)} %get-tuple-element.33.refs_0_), channel_id=1, source_target_pairs={{0,2},{2,0},{4,6},{6,4},{1,3},{3,1},{5,7},{7,5},{8,10},{10,8},{12,... | collective-permute-start | bytes 49160 | tf_op jit(solution)/shard_map/ppermute | solution.py:41
  85.7 5.1 %collective-permute-done.18.refs_2_ = bf16[64,1024]{1,0:T(8,128)(2,1)S(1)} collective-permute-done((bf16[64,1024]{1,0:T(8,128)(2,1)S(1)}, bf16[64,1024]{1,0:T(8,128)(2,1)S(1)}, u32[]{:S(2)}, u32[]{:S(2)}) %collective-permute-start.18) | collective-permute-done | bytes 131104 | tf_op jit(solution)/shard_map/ppermute | solution.py:41
  90.9 7.3 %last_mixer.1 = (bf16[16,5760]{1,0:T(8,128)(2,1)S(1)}, bf16[16,5760]{1,0:T(8,128)(2,1)S(1)}, bf16[16,5760]{1,0:T(8,128)(2,1)S(1)}, bf16[16,5760]{1,0:T(8,128)(2,1)S(1)}, bf16[64,1024]{1,0:T(8,128)(2,1)S(1)}) custom-call(bf16[64,1024]{1,0:T(8,128)(2,1)S(1)} %get-tuple-element.28.refs_0_, bf16[64,1024]{1,0:T(8,128)(2,1)S(1)} %add_convert_fusion.refs_1_, ...), custom_call_target="tpu_custom_call" | custom-call | tf_op jit(solution)/shard_map/last_mixer/pallas_call | solution.py:304
  102.7 4.1 %collective-permute-done.19.refs_1_ = bf16[16,5760]{1,0:T(8,128)(2,1)S(1)} collective-permute-done((bf16[16,5760]{1,0:T(8,128)(2,1)S(1)}, bf16[16,5760]{1,0:T(8,128)(2,1)S(1)}, u32[]{:S(2)}, u32[]{:S(2)}) %collective-permute-start.19) | collective-permute-done | bytes 184352 | tf_op jit(solution)/shard_map/ppermute | solution.py:41
  106.8 9.3 %collective-permute-done.20.refs_2_ = bf16[16,5760]{1,0:T(8,128)(2,1)S(1)} collective-permute-done((bf16[16,5760]{1,0:T(8,128)(2,1)S(1)}, bf16[16,5760]{1,0:T(8,128)(2,1)S(1)}, u32[]{:S(2)}, u32[]{:S(2)}) %collective-permute-start.20) | collective-permute-done | bytes 184352 | tf_op jit(solution)/shard_map/ppermute | solution.py:41
  118.2 3.6 %collective-permute-start.23 = (bf16[16,2816]{1,0:T(8,128)(2,1)S(1)}, bf16[16,2816]{1,0:T(8,128)(2,1)S(1)}, u32[]{:S(2)}, u32[]{:S(2)}) collective-permute-start(bf16[16,2816]{1,0:T(8,128)(2,1)S(1)} %hidden.3.refs_0_), channel_id=1, source_target_pairs={{0,4},{2,6},{4,0},{6,2},{1,5},{3,7},{5,1},{7,3},{8,12},{10,14},{12... | collective-permute-start | bytes 270344 | tf_op jit(solution)/shard_map/ppermute | solution.py:41
  123.4 4.5 %collective-permute-done.23.refs_2_ = bf16[16,2816]{1,0:T(8,128)(2,1)S(1)} collective-permute-done((bf16[16,2816]{1,0:T(8,128)(2,1)S(1)}, bf16[16,2816]{1,0:T(8,128)(2,1)S(1)}, u32[]{:S(2)}, u32[]{:S(2)}) %collective-permute-start.23) | collective-permute-done | bytes 90144 | tf_op jit(solution)/shard_map/ppermute | solution.py:41
  127.9 3.0 %last_down.1 = (bf16[16,1024]{1,0:T(8,128)(2,1)S(1)}, bf16[16,1024]{1,0:T(8,128)(2,1)S(1)}, bf16[16,1024]{1,0:T(8,128)(2,1)S(1)}, bf16[16,1024]{1,0:T(8,128)(2,1)S(1)}) custom-call(bf16[16,2816]{1,0:T(8,128)(2,1)S(1)} %hidden.3.refs_0_, bf16[16,2816]{1,0:T(8,128)(2,1)S(1)} %collective-permute-done.22.refs_1_, ...), custom_call_target="tpu_custom_call" | custom-call | tf_op jit(solution)/shard_map/last_down/pallas_call | solution.py:367
  132.8 2.4 %collective-permute-done.26.refs_3_ = bf16[16,1024]{1,0:T(8,128)(2,1)S(1)} collective-permute-done((bf16[16,1024]{1,0:T(8,128)(2,1)S(1)}, bf16[16,1024]{1,0:T(8,128)(2,1)S(1)}, u32[]{:S(2)}, u32[]{:S(2)}) %collective-permute-start.26) | collective-permute-done | bytes 32800 | tf_op jit(solution)/shard_map/ppermute | solution.py:41
  (91 shorter events, 32.6 us)
Async XLA Ops:
  0.6 5.1 %collective-permute-start.1 = (bf16[16,1024]{1,0:T(8,128)(2,1)}, bf16[16,1024]{1,0:T(8,128)(2,1)S(1)}, u32[]{:S(2)}, u32[]{:S(2)}) collective-permute-start(bf16[16,1024]{1,0:T(8,128)(2,1)} %refs_0_.1), channel_id=1, source_target_pairs={{0,8},{1,9},{8,0},{9,1},{2,10},{3,11},{10,2},{11,3},{4,12},{5,13},... | collective-permute-start | bytes 98312 | tf_op jit(solution)/shard_map/ppermute | solution.py:41
  3.7 3.6 %collective-permute-start.2 = (bf16[16,1024]{1,0:T(8,128)(2,1)}, bf16[16,1024]{1,0:T(8,128)(2,1)S(1)}, u32[]{:S(2)}, u32[]{:S(2)}) collective-permute-start(bf16[16,1024]{1,0:T(8,128)(2,1)} %refs_0_.1), channel_id=1, source_target_pairs={{0,9},{1,8},{8,1},{9,0},{2,11},{3,10},{10,3},{11,2},{4,13},{5,12},... | collective-permute-start | bytes 98312 | tf_op jit(solution)/shard_map/ppermute | solution.py:41
  21.1 10.6 %collective-permute-start.3 = (bf16[16,5760]{1,0:T(8,128)(2,1)S(1)}, bf16[16,5760]{1,0:T(8,128)(2,1)S(1)}, u32[]{:S(2)}, u32[]{:S(2)}) collective-permute-start(bf16[16,5760]{1,0:T(8,128)(2,1)S(1)} %get-tuple-element.25), channel_id=1, source_target_pairs={{0,2},{2,0},{4,6},{6,4},{1,3},{3,1},{5,7},{7,5},{8,10},{10,8},{12,... | collective-permute-start | bytes 552968 | tf_op jit(solution)/shard_map/ppermute | solution.py:41
  22.8 16.4 %collective-permute-start.4 = (bf16[16,5760]{1,0:T(8,128)(2,1)S(1)}, bf16[16,5760]{1,0:T(8,128)(2,1)S(1)}, u32[]{:S(2)}, u32[]{:S(2)}) collective-permute-start(bf16[16,5760]{1,0:T(8,128)(2,1)S(1)} %get-tuple-element.26), channel_id=1, source_target_pairs={{0,4},{2,6},{4,0},{6,2},{1,5},{3,7},{5,1},{7,3},{8,12},{10,14},{12... | collective-permute-start | bytes 552968 | tf_op jit(solution)/shard_map/ppermute | solution.py:41
  25.3 13.8 %collective-permute-start.5 = (bf16[16,5760]{1,0:T(8,128)(2,1)S(1)}, bf16[16,5760]{1,0:T(8,128)(2,1)S(1)}, u32[]{:S(2)}, u32[]{:S(2)}) collective-permute-start(bf16[16,5760]{1,0:T(8,128)(2,1)S(1)} %get-tuple-element.27), channel_id=1, source_target_pairs={{0,6},{2,4},{4,2},{6,0},{1,7},{3,5},{5,3},{7,1},{8,14},{10,12},{12... | collective-permute-start | bytes 552968 | tf_op jit(solution)/shard_map/ppermute | solution.py:41
  39.4 6.5 %collective-permute-start.8 = (bf16[16,2816]{1,0:T(8,128)(2,1)S(1)}, bf16[16,2816]{1,0:T(8,128)(2,1)S(1)}, u32[]{:S(2)}, u32[]{:S(2)}) collective-permute-start(bf16[16,2816]{1,0:T(8,128)(2,1)S(1)} %hidden.2.refs_0_), channel_id=1, source_target_pairs={{0,6},{2,4},{4,2},{6,0},{1,7},{3,5},{5,3},{7,1},{8,14},{10,12},{12... | collective-permute-start | bytes 270344 | tf_op jit(solution)/shard_map/ppermute | solution.py:41
  41.9 9.4 %collective-permute-start.7 = (bf16[16,2816]{1,0:T(8,128)(2,1)S(1)}, bf16[16,2816]{1,0:T(8,128)(2,1)S(1)}, u32[]{:S(2)}, u32[]{:S(2)}) collective-permute-start(bf16[16,2816]{1,0:T(8,128)(2,1)S(1)} %hidden.2.refs_0_), channel_id=1, source_target_pairs={{0,4},{2,6},{4,0},{6,2},{1,5},{3,7},{5,1},{7,3},{8,12},{10,14},{12... | collective-permute-start | bytes 270344 | tf_op jit(solution)/shard_map/ppermute | solution.py:41
  44.7 6.7 %collective-permute-start.6 = (bf16[16,2816]{1,0:T(8,128)(2,1)S(1)}, bf16[16,2816]{1,0:T(8,128)(2,1)S(1)}, u32[]{:S(2)}, u32[]{:S(2)}) collective-permute-start(bf16[16,2816]{1,0:T(8,128)(2,1)S(1)} %hidden.2.refs_0_), channel_id=1, source_target_pairs={{0,2},{2,0},{4,6},{6,4},{1,3},{3,1},{5,7},{7,5},{8,10},{10,8},{12,... | collective-permute-start | bytes 270344 | tf_op jit(solution)/shard_map/ppermute | solution.py:41
  55.8 5.6 %collective-permute-start.10 = (bf16[64,1024]{1,0:T(8,128)(2,1)S(1)}, bf16[64,1024]{1,0:T(8,128)(2,1)S(1)}, u32[]{:S(2)}, u32[]{:S(2)}) collective-permute-start(bf16[64,1024]{1,0:T(8,128)(2,1)S(1)} %add_convert_fusion.1.refs_1_), channel_id=1, source_target_pairs={{0,8},{1,9},{8,0},{9,1},{2,10},{3,11},{10,2},{11,3},{4,12},{5,13},... | collective-permute-start | bytes 393224 | tf_op jit(solution)/shard_map/ppermute | solution.py:41
  63.8 4.5 %collective-permute-start.11 = (bf16[16,1920]{1,0:T(8,128)(2,1)S(1)}, bf16[16,1920]{1,0:T(8,128)(2,1)S(1)}, u32[]{:S(2)}, u32[]{:S(2)}) collective-permute-start(bf16[16,1920]{1,0:T(8,128)(2,1)S(1)} %get-tuple-element.30), channel_id=1, source_target_pairs={{0,2},{2,0},{4,6},{6,4},{1,3},{3,1},{5,7},{7,5},{8,10},{10,8},{12,... | collective-permute-start | bytes 184328 | tf_op jit(solution)/shard_map/ppermute | solution.py:41
  63.8 6.0 %collective-permute-start.12 = (bf16[16,1920]{1,0:T(8,128)(2,1)S(1)}, bf16[16,1920]{1,0:T(8,128)(2,1)S(1)}, u32[]{:S(2)}, u32[]{:S(2)}) collective-permute-start(bf16[16,1920]{1,0:T(8,128)(2,1)S(1)} %get-tuple-element.31), channel_id=1, source_target_pairs={{0,4},{2,6},{4,0},{6,2},{1,5},{3,7},{5,1},{7,3},{8,12},{10,14},{12... | collective-permute-start | bytes 184328 | tf_op jit(solution)/shard_map/ppermute | solution.py:41
  66.9 6.0 %collective-permute-start.13 = (bf16[16,1920]{1,0:T(8,128)(2,1)S(1)}, bf16[16,1920]{1,0:T(8,128)(2,1)S(1)}, u32[]{:S(2)}, u32[]{:S(2)}) collective-permute-start(bf16[16,1920]{1,0:T(8,128)(2,1)S(1)} %get-tuple-element.32), channel_id=1, source_target_pairs={{0,6},{2,4},{4,2},{6,0},{1,7},{3,5},{5,3},{7,1},{8,14},{10,12},{12... | collective-permute-start | bytes 184328 | tf_op jit(solution)/shard_map/ppermute | solution.py:41
  76.5 5.5 %collective-permute-start.16 = (bf16[16,512]{1,0:T(8,128)(2,1)S(1)}, bf16[16,512]{1,0:T(8,128)(2,1)S(1)}, u32[]{:S(2)}, u32[]{:S(2)}) collective-permute-start(bf16[16,512]{1,0:T(8,128)(2,1)S(1)} %get-tuple-element.33.refs_0_), channel_id=1, source_target_pairs={{0,6},{2,4},{4,2},{6,0},{1,7},{3,5},{5,3},{7,1},{8,14},{10,12},{12... | collective-permute-start | bytes 49160 | tf_op jit(solution)/shard_map/ppermute | solution.py:41
  77.9 4.6 %collective-permute-start.15 = (bf16[16,512]{1,0:T(8,128)(2,1)S(1)}, bf16[16,512]{1,0:T(8,128)(2,1)S(1)}, u32[]{:S(2)}, u32[]{:S(2)}) collective-permute-start(bf16[16,512]{1,0:T(8,128)(2,1)S(1)} %get-tuple-element.33.refs_0_), channel_id=1, source_target_pairs={{0,4},{2,6},{4,0},{6,2},{1,5},{3,7},{5,1},{7,3},{8,12},{10,14},{12... | collective-permute-start | bytes 49160 | tf_op jit(solution)/shard_map/ppermute | solution.py:41
  77.9 4.8 %collective-permute-start.14 = (bf16[16,512]{1,0:T(8,128)(2,1)S(1)}, bf16[16,512]{1,0:T(8,128)(2,1)S(1)}, u32[]{:S(2)}, u32[]{:S(2)}) collective-permute-start(bf16[16,512]{1,0:T(8,128)(2,1)S(1)} %get-tuple-element.33.refs_0_), channel_id=1, source_target_pairs={{0,2},{2,0},{4,6},{6,4},{1,3},{3,1},{5,7},{7,5},{8,10},{10,8},{12,... | collective-permute-start | bytes 49160 | tf_op jit(solution)/shard_map/ppermute | solution.py:41
  85.2 5.6 %collective-permute-start.18 = (bf16[64,1024]{1,0:T(8,128)(2,1)S(1)}, bf16[64,1024]{1,0:T(8,128)(2,1)S(1)}, u32[]{:S(2)}, u32[]{:S(2)}) collective-permute-start(bf16[64,1024]{1,0:T(8,128)(2,1)S(1)} %add_convert_fusion.refs_1_), channel_id=1, source_target_pairs={{0,8},{1,9},{8,0},{9,1},{2,10},{3,11},{10,2},{11,3},{4,12},{5,13},... | collective-permute-start | bytes 393224 | tf_op jit(solution)/shard_map/ppermute | solution.py:41
  98.2 8.5 %collective-permute-start.19 = (bf16[16,5760]{1,0:T(8,128)(2,1)S(1)}, bf16[16,5760]{1,0:T(8,128)(2,1)S(1)}, u32[]{:S(2)}, u32[]{:S(2)}) collective-permute-start(bf16[16,5760]{1,0:T(8,128)(2,1)S(1)} %get-tuple-element.36), channel_id=1, source_target_pairs={{0,2},{2,0},{4,6},{6,4},{1,3},{3,1},{5,7},{7,5},{8,10},{10,8},{12,... | collective-permute-start | bytes 552968 | tf_op jit(solution)/shard_map/ppermute | solution.py:41
  100.2 15.9 %collective-permute-start.20 = (bf16[16,5760]{1,0:T(8,128)(2,1)S(1)}, bf16[16,5760]{1,0:T(8,128)(2,1)S(1)}, u32[]{:S(2)}, u32[]{:S(2)}) collective-permute-start(bf16[16,5760]{1,0:T(8,128)(2,1)S(1)} %get-tuple-element.37), channel_id=1, source_target_pairs={{0,4},{2,6},{4,0},{6,2},{1,5},{3,7},{5,1},{7,3},{8,12},{10,14},{12... | collective-permute-start | bytes 552968 | tf_op jit(solution)/shard_map/ppermute | solution.py:41
  101.1 15.0 %collective-permute-start.21 = (bf16[16,5760]{1,0:T(8,128)(2,1)S(1)}, bf16[16,5760]{1,0:T(8,128)(2,1)S(1)}, u32[]{:S(2)}, u32[]{:S(2)}) collective-permute-start(bf16[16,5760]{1,0:T(8,128)(2,1)S(1)} %get-tuple-element.38), channel_id=1, source_target_pairs={{0,6},{2,4},{4,2},{6,0},{1,7},{3,5},{5,3},{7,1},{8,14},{10,12},{12... | collective-permute-start | bytes 552968 | tf_op jit(solution)/shard_map/ppermute | solution.py:41
  116.2 7.2 %collective-permute-start.24 = (bf16[16,2816]{1,0:T(8,128)(2,1)S(1)}, bf16[16,2816]{1,0:T(8,128)(2,1)S(1)}, u32[]{:S(2)}, u32[]{:S(2)}) collective-permute-start(bf16[16,2816]{1,0:T(8,128)(2,1)S(1)} %hidden.3.refs_0_), channel_id=1, source_target_pairs={{0,6},{2,4},{4,2},{6,0},{1,7},{3,5},{5,3},{7,1},{8,14},{10,12},{12... | collective-permute-start | bytes 270344 | tf_op jit(solution)/shard_map/ppermute | solution.py:41
  118.2 9.7 %collective-permute-start.23 = (bf16[16,2816]{1,0:T(8,128)(2,1)S(1)}, bf16[16,2816]{1,0:T(8,128)(2,1)S(1)}, u32[]{:S(2)}, u32[]{:S(2)}) collective-permute-start(bf16[16,2816]{1,0:T(8,128)(2,1)S(1)} %hidden.3.refs_0_), channel_id=1, source_target_pairs={{0,4},{2,6},{4,0},{6,2},{1,5},{3,7},{5,1},{7,3},{8,12},{10,14},{12... | collective-permute-start | bytes 270344 | tf_op jit(solution)/shard_map/ppermute | solution.py:41
  121.8 6.1 %collective-permute-start.22 = (bf16[16,2816]{1,0:T(8,128)(2,1)S(1)}, bf16[16,2816]{1,0:T(8,128)(2,1)S(1)}, u32[]{:S(2)}, u32[]{:S(2)}) collective-permute-start(bf16[16,2816]{1,0:T(8,128)(2,1)S(1)} %hidden.3.refs_0_), channel_id=1, source_target_pairs={{0,2},{2,0},{4,6},{6,4},{1,3},{3,1},{5,7},{7,5},{8,10},{10,8},{12,... | collective-permute-start | bytes 270344 | tf_op jit(solution)/shard_map/ppermute | solution.py:41
  130.9 4.2 %collective-permute-start.26 = (bf16[16,1024]{1,0:T(8,128)(2,1)S(1)}, bf16[16,1024]{1,0:T(8,128)(2,1)S(1)}, u32[]{:S(2)}, u32[]{:S(2)}) collective-permute-start(bf16[16,1024]{1,0:T(8,128)(2,1)S(1)} %get-tuple-element.41), channel_id=1, source_target_pairs={{0,8},{1,9},{8,0},{9,1},{2,10},{3,11},{10,2},{11,3},{4,12},{5,13},... | collective-permute-start | bytes 98312 | tf_op jit(solution)/shard_map/ppermute | solution.py:41
  131.7 3.7 %collective-permute-start.27 = (bf16[16,1024]{1,0:T(8,128)(2,1)S(1)}, bf16[16,1024]{1,0:T(8,128)(2,1)S(1)}, u32[]{:S(2)}, u32[]{:S(2)}) collective-permute-start(bf16[16,1024]{1,0:T(8,128)(2,1)S(1)} %get-tuple-element.42), channel_id=1, source_target_pairs={{0,9},{1,8},{8,1},{9,0},{2,11},{3,10},{10,3},{11,2},{4,13},{5,12},... | collective-permute-start | bytes 98312 | tf_op jit(solution)/shard_map/ppermute | solution.py:41
  (26 other events, 753.8 us)

commit v2 on v0

v2 whole, which is shorter than its diff:
```python
import functools

import jax
import jax.numpy as jnp
from jax import lax
from jax.experimental import pallas as pl
from jax.experimental.pallas import tpu as pltpu
from jax.sharding import PartitionSpec as P

KEY_CHANNELS = 64
VALUE_DIM = 128
EPSILON = 1e-06
LANES = 128
F32 = jnp.float32
BF16 = jnp.bfloat16

VMEM = pl.BlockSpec(memory_space=pltpu.VMEM)


def padded(width):
    return -(-width // LANES) * LANES


def column_step(width):
    return 256 if width % 256 == 0 else width


def linear_index(axes):
    place = 0
    for axis in axes:
        place = place * lax.axis_size(axis) + lax.axis_index(axis)
    return place


def rows_at(block, height):
    return pl.ds(pl.multiple_of(block * height, height), height)


def swap(array, axes, size, offset):
    return lax.ppermute(array, axes, [(i, i ^ offset) for i in range(size)])


def swaps(arrays, axes, size):
    return [swap(array, axes, size, k + 1) for k, array in enumerate(arrays)]


def split_square_sum(total):
    high = total.astype(BF16).astype(F32)
    lane = lax.broadcasted_iota(jnp.int32, (total.shape[0], LANES), 1)
    return jnp.where(lane < LANES // 2, high, total - high)


def join_square_sum(block):
    return block[:, :1] + block[:, LANES // 2 : LANES // 2 + 1]


def fetch_kernel(n_weights, *refs):
    weights, outs, semaphores = refs[:n_weights], refs[n_weights : 2 * n_weights], refs[-1]
    copies = []
    for weight, out in zip(weights, outs):
        step = weight.shape[0] // FETCH_PIECES
        for piece in range(FETCH_PIECES):
            part = pl.ds(piece * step, step)
            copies.append(pltpu.make_async_copy(weight.at[part], out.at[part], semaphores.at[len(copies)]))
            copies[-1].start()
    for copy in copies:
        copy.wait()


def multiply_blocks(scaled, weight, base, outs):
    height = outs[0].shape[0]
    width = weight.shape[1]
    step = column_step(width)
    for low in range(0, width, step):
        product = jnp.dot(scaled, weight[:, low : low + step], preferred_element_type=F32)
        for k, out in enumerate(outs):
            block = product[k * height : (k + 1) * height]
            out[:, base + low : base + low + step] = block.astype(out.dtype)


def put_squares(squares, low, outs):
    height = outs[0].shape[0]
    block = split_square_sum(squares)
    for k, out in enumerate(outs):
        out[:, low : low + LANES] = block[k * height : (k + 1) * height].astype(out.dtype)


def project_rows(widened, gain, weights, outs):
    scaled = (widened * gain[...]).astype(BF16)
    base = 0
    for weight in weights:
        multiply_blocks(scaled, weight, base, outs)
        base += padded(weight.shape[1])
    put_squares(jnp.sum(widened * widened, axis=1, keepdims=True), base, outs)


def first_kernel(n_dt, n_kv, names, *refs):
    own, others, refs = refs[0], refs[1:n_dt], refs[n_dt:]
    gain, weights, refs = refs[0], refs[1:3], refs[3:]
    outs, gathered = refs[:n_kv], refs[n_kv]
    height = own.shape[0]
    place = linear_index(names[0]) ^ linear_index(names[1])
    for k, block in enumerate((own, *others)):
        gathered[rows_at(place ^ k, height), :] = block[...]
    project_rows(gathered[...].astype(F32), gain, weights, outs)


def add_parts(residual, parts, half):
    total = parts[0][...].astype(F32)
    for part in parts[1:]:
        total = total + part[...].astype(F32)
    return (residual[...].astype(F32) + half * total).astype(BF16)


def project_kernel(half, n_parts, n_weights, *refs):
    residual, parts, refs = refs[0], refs[1 : 1 + n_parts], refs[1 + n_parts :]
    gain, weights, refs = refs[0], refs[1 : 1 + n_weights], refs[1 + n_weights :]
    outs, stream = refs[:-1], refs[-1]
    stream[...] = add_parts(residual, parts, half)
    project_rows(stream[...].astype(F32), gain, weights, outs)


def sum_columns(parts, low, size):
    total = parts[0][:, low : low + size].astype(F32)
    for part in parts[1:]:
        total = total + part[:, low : low + size].astype(F32)
    return total


def hidden_kernel(features, n_kv, *refs):
    parts, out = refs[:n_kv], refs[n_kv]
    width = out.shape[1]
    gap = padded(width)
    scale = lax.rsqrt(join_square_sum(sum_columns(parts, 2 * gap, LANES)) / features + EPSILON)
    step = column_step(width)
    for low in range(0, width, step):
        gate = jax.nn.silu(scale * sum_columns(parts, low, step))
        out[:, low : low + step] = (gate * (scale * sum_columns(parts, gap + low, step))).astype(BF16)


def stack_rows(blocks, rows):
    height = blocks[0].shape[0]
    for k, block in enumerate(blocks):
        rows[k * height : (k + 1) * height, :] = block[...]


def down_kernel(n_blocks, *refs):
    blocks, weight, (out, rows) = refs[:n_blocks], refs[n_blocks], refs[-2:]
    stack_rows(blocks, rows)
    step = column_step(weight.shape[1])
    for low in range(0, weight.shape[1], step):
        product = jnp.dot(rows[...], weight[:, low : low + step], preferred_element_type=F32)
        out[:, low : low + step] = product.astype(BF16)


def scatter_down_kernel(n_blocks, names, *refs):
    blocks, weight = refs[:n_blocks], refs[n_blocks]
    outs, (rows, product) = refs[n_blocks + 1 : -2], refs[-2:]
    stack_rows(blocks, rows)
    height = blocks[0].shape[0]
    place = linear_index(names[0]) ^ linear_index(names[1])
    step = column_step(weight.shape[1])
    for low in range(0, weight.shape[1], step):
        columns = slice(low, low + step)
        product[:, columns] = jnp.dot(rows[...], weight[:, columns], preferred_element_type=F32).astype(BF16)
    for k, out in enumerate(outs):
        out[...] = product[rows_at(place ^ k, height), :]


def attention_kernel(features, n_parts, *refs):
    parts, refs = refs[:n_parts], refs[n_parts:]
    extra_decay, state, norm_gain, head_rows, upright, value_rows, read, columns = refs
    rows, heads = state.shape[0], state.shape[1]
    keys, values = heads * KEY_CHANNELS, heads * VALUE_DIM
    gap, value_gap = padded(keys), padded(values)
    scale = lax.rsqrt(join_square_sum(sum_columns(parts, 3 * gap + 2 * value_gap, LANES)) / features + EPSILON)
    queries = scale * sum_columns(parts, 0, keys) * KEY_CHANNELS ** (-0.5)
    key_rows = scale * sum_columns(parts, gap, keys)
    forget = scale * sum_columns(parts, 2 * gap, keys)
    value_rows[...] = scale * sum_columns(parts, 3 * gap, values)
    log_sigmoid = jnp.minimum(forget, 0.0) - jnp.log1p(jnp.exp(-jnp.abs(forget)))
    decay = jnp.exp(log_sigmoid / 16.0 + extra_decay[...])
    columns[...] = jnp.zeros_like(columns)
    columns[0:rows, :keys] = decay
    columns[rows : 2 * rows, :keys] = key_rows
    columns[2 * rows : 3 * rows, :keys] = queries * decay
    upright[...] = columns[...].T
    matched = queries * key_rows
    for head in range(heads):
        channels = slice(head * KEY_CHANNELS, (head + 1) * KEY_CHANNELS)
        lanes = slice(head * VALUE_DIM, (head + 1) * VALUE_DIM)
        match = jnp.sum(matched[:, channels], axis=1, keepdims=True)
        for row in range(rows):
            taken = upright[channels, 2 * rows + row : 2 * rows + row + 1] * state[row, head]
            read[row : row + 1, lanes] = jnp.sum(taken, axis=0, keepdims=True)
        one = read[:, lanes] + match * value_rows[:, lanes]
        mean = jnp.mean(one * one, axis=-1, keepdims=True)
        normed = one * lax.rsqrt(mean + EPSILON) * norm_gain[...]
        low = 3 * gap + value_gap + head * VALUE_DIM
        gates = scale * sum_columns(parts, low, VALUE_DIM)
        head_rows[:, lanes] = (normed * jax.nn.silu(gates)).astype(BF16)


def state_kernel(upright, value_rows, state, new_state, finished):
    finished[...] = jnp.zeros_like(finished)
    rows, heads = state.shape[0], state.shape[1]
    for head in range(heads):
        channels = slice(head * KEY_CHANNELS, (head + 1) * KEY_CHANNELS)
        lanes = slice(head * VALUE_DIM, (head + 1) * VALUE_DIM)
        for row in range(rows):
            kept = upright[channels, row : row + 1] * state[row, head]
            added = upright[channels, rows + row : rows + row + 1] * value_rows[row : row + 1, lanes]
            new_state[row, head] = kept + added


def result_kernel(n_parts, names, *refs):
    stream, parts, out = refs[0], refs[1 : 1 + n_parts], refs[1 + n_parts]
    total = parts[0][...].astype(F32)
    for part in parts[1:]:
        total = total + part[...].astype(F32)
    place = linear_index(names[0]) ^ linear_index(names[1])
    own = stream[rows_at(place, out.shape[0]), :].astype(F32)
    out[...] = (own + 0.5 * total).astype(BF16)


MIB = 1 << 20
FETCH_PIECES = 4


def array_bytes(array):
    *lead, width = array.shape
    size = array.dtype.itemsize * padded(width)
    for extent in lead:
        size *= extent
    return size


def call(kernel, name, outs, inputs, scratch=(), in_specs=None, work=0, cores=8 * MIB):
    arrays = [*inputs, *jax.tree.leaves(outs)]
    return pl.pallas_call(
        kernel,
        out_shape=outs,
        in_specs=in_specs or [VMEM] * len(inputs),
        out_specs=jax.tree.map(lambda _: VMEM, outs),
        scratch_shapes=list(scratch),
        compiler_params=pltpu.CompilerParams(vmem_limit_bytes=sum(map(array_bytes, arrays)) + cores),
        cost_estimate=pl.CostEstimate(flops=work, bytes_accessed=0, transcendentals=0),
        name=name,
    )(*inputs)


def per_device(
    n_dt,
    n_kv,
    residual_input,
    incoming_state,
    extra_log_decay,
    leading_norm_gain,
    leading_gate_weight,
    leading_up_weight,
    leading_down_weight,
    attention_norm_gain,
    query_projector,
    key_projector,
    value_projector,
    output_gate_weight,
    forget_weight,
    head_norm_gain,
    output_projector,
    trailing_norm_gain,
    trailing_gate_weight,
    trailing_up_weight,
    trailing_down_weight,
):
    dt, kv = ("dp", "tp"), ("kv",)
    names = (dt, kv)
    height, width = residual_input.shape
    features = width * n_kv
    rows = height * n_dt
    shape = jax.ShapeDtypeStruct

    def collect(blocks):
        return [blocks[0]] + swaps(blocks[1:], kv, n_kv)

    def gather_rows(block):
        return [block] + [swap(block, kv, n_kv, k) for k in range(1, n_kv)]

    def total_parts(part):
        offset = 1
        while 2 * offset < n_dt:
            part = (part.astype(F32) + swap(part, dt, n_dt, offset).astype(F32)).astype(BF16)
            offset *= 2
        return [part, swap(part, dt, n_dt, offset)]

    def project(kernel, name, weights, inputs):
        span = sum(padded(w.shape[1]) for w in weights) + LANES
        outs = [shape((height, span), F32)] + [shape((height, span), BF16)] * (n_kv - 1)
        return call(kernel, name, outs + [shape((rows, width), BF16)], (*inputs, *weights))

    def hidden_rows(blocks, units):
        kernel = functools.partial(hidden_kernel, features, n_kv)
        return gather_rows(call(kernel, "hidden", shape((height, units), BF16), collect(blocks)))

    def down(blocks, weight, name, *after):
        kernel = functools.partial(down_kernel, n_kv)
        scratch = [pltpu.VMEM((rows, weight.shape[0]), BF16)]
        return call(kernel, name, shape((rows, weight.shape[1]), BF16), (*blocks, weight, *after), scratch)

    units = leading_gate_weight.shape[1]
    arrived = [swap(residual_input, dt, n_dt, k) for k in range(1, n_dt)]
    fetched = [
        pltpu.with_memory_space_constraint(w, pltpu.HBM) for w in (leading_gate_weight, leading_up_weight)
    ]
    gate, up = call(
        functools.partial(fetch_kernel, 2),
        "fetch",
        [shape(w.shape, w.dtype) for w in fetched],
        fetched,
        [pltpu.SemaphoreType.DMA((2 * FETCH_PIECES,))],
        [pl.BlockSpec(memory_space=pltpu.HBM)] * 2,
        100000,
    )
    *blocks, gathered = project(
        functools.partial(first_kernel, n_dt, n_kv, names),
        "first",
        (gate, up),
        (residual_input, *arrived, leading_norm_gain.reshape(1, width)),
    )
    parts = total_parts(down(hidden_rows(blocks, units), leading_down_weight, "first_down"))

    mixed = (query_projector, key_projector, forget_weight, value_projector, output_gate_weight)
    *blocks, after_first = project(
        functools.partial(project_kernel, 0.5, len(parts), len(mixed)),
        "attention_in",
        mixed,
        (gathered, *parts, attention_norm_gain.reshape(1, width)),
    )
    blocks = collect(blocks)
    heads = incoming_state.shape[1]
    keys, values = heads * KEY_CHANNELS, heads * VALUE_DIM
    upright = (padded(keys), padded(3 * height))
    head_rows, upright, value_rows = call(
        functools.partial(attention_kernel, features, n_kv),
        "attention",
        [shape((height, values), BF16), shape(upright, F32), shape((height, values), F32)],
        (*blocks, extra_log_decay, incoming_state, head_norm_gain.reshape(1, VALUE_DIM)),
        [pltpu.VMEM((height, values), F32), pltpu.VMEM(upright[::-1], F32)],
    )
    known = gather_rows(head_rows)
    outs = [shape(incoming_state.shape, F32), shape((8, LANES), F32)]
    new_state, finished = call(state_kernel, "state", outs, (upright, value_rows, incoming_state), work=100000)
    parts = total_parts(down(known, output_projector, "attention_out", finished))

    last = (trailing_gate_weight, trailing_up_weight)
    *blocks, second = project(
        functools.partial(project_kernel, 1.0, len(parts), len(last)),
        "last",
        last,
        (after_first, *parts, trailing_norm_gain.reshape(1, width)),
    )
    hidden = hidden_rows(blocks, units)
    parts = call(
        functools.partial(scatter_down_kernel, n_kv, names),
        "last_down",
        [shape((height, width), BF16)] * n_dt,
        (*hidden, trailing_down_weight),
        [pltpu.VMEM((rows, trailing_down_weight.shape[0]), BF16), pltpu.VMEM((rows, width), BF16)],
    )
    parts = [parts[0]] + swaps(parts[1:], dt, n_dt)
    result = call(
        functools.partial(result_kernel, n_dt, names), "result", shape((height, width), BF16), (second, *parts)
    )
    return (result, new_state)


def solution(mesh):
    n_dt = mesh.shape["dp"] * mesh.shape["tp"]
    n_kv = mesh.shape["kv"]
    assert n_dt == n_kv and n_kv & (n_kv - 1) == 0
    return jax.shard_map(
        functools.partial(per_device, n_dt, n_kv),
        mesh=mesh,
        in_specs=(
            P(("grp", "dp", "tp"), "kv"),
            P(("grp", "kv"), ("dp", "tp"), None, None),
            P(("grp", "kv"), ("dp", "tp")),
            P("kv"),
            P("kv", ("dp", "tp")),
            P("kv", ("dp", "tp")),
            P(("dp", "tp"), "kv"),
            P("kv"),
            P("kv", ("dp", "tp")),
            P("kv", ("dp", "tp")),
            P("kv", ("dp", "tp")),
            P("kv", ("dp", "tp")),
            P("kv", ("dp", "tp")),
            P(),
            P(("dp", "tp"), "kv"),
            P("kv"),
            P("kv", ("dp", "tp")),
            P("kv", ("dp", "tp")),
            P(("dp", "tp"), "kv"),
        ),
        out_specs=(P(("grp", "dp", "tp"), "kv"), P(("grp", "kv"), ("dp", "tp"), None, None)),
        check_vma=False,
    )
```

time: 361 us -> 112 us (0.31)
  waiting for transfers between devices: 198 us -> 55.6 us
  blocking collectives: 97.3 us -> 0 us
  matrix products: 37.8 us -> 0 us
  starting transfers between devices: 0.5 us -> 38 us
  Pallas kernels: 0 us -> 17.1 us
  between operations: 15 us -> 1.02 us
  other arithmetic: 10.4 us -> 0.07 us
    reduce_scatter x12 -> x0, waiting for transfers between devices: 198 us -> none  [the longest x2 48.7 us: channel_mixer(): lax.psum_scatter(gate_part, 'kv', scatter_dimension=0, tiled=True)]
    all_gather x6 -> x0, blocking collectives: 60.9 us -> none  [the longest x2 30 us: channel_mixer(): hidden = lax.all_gather(hidden_share, 'kv', axis=0, tiled=True)]
    ppermute x0 -> x28, waiting for transfers between devices: none -> 55.6 us  [swap(): return lax.ppermute(array, axes, [(i, i ^ offset) for i in range(size)])]
    ppermute x0 -> x28, starting transfers between devices: none -> 38 us  [swap(): return lax.ppermute(array, axes, [(i, i ^ offset) for i in range(size)])]
    dot_general x13 -> x0, matrix products: 37.8 us -> none  [the longest x2 9.25 us: channel_mixer(): up_part = jnp.dot(scaled, up_matrix, preferred_element_type=jnp.float32)]
    unnamed x3 -> x0, blocking collectives: 36.4 us -> none
    pallas_call x0 -> x12, Pallas kernels: none -> 17.1 us  [call(): pl.pallas_call(kernel, out_shape=outs, in_specs=in_specs or [VMEM] * len(...]
    convert_element_type x6 -> x2, other arithmetic: 5.52 us -> 0.07 us  [total_parts(): (part.astype(F32) + swap(part, dt, n_dt, offset).astype(F32)).astype(BF16)]
  transfers between devices with their start and end apart: 12 -> 28, of which waited for: 12 -> 18; matrix products, arithmetic and copies ran while one was open for 5% -> 0% of each run, Pallas kernels for 0% -> 6%
where the time goes in v2:
time: 112 us
  waiting for transfers between devices  55.6 us (50%)
  starting transfers between devices  38 us (34%)
  Pallas kernels  17.1 us (15%)
    ppermute x28, waiting for transfers between devices, swap(): return lax.ppermute(array, axes, [(i, i ^ offset) for i in range(size)])  55.6 us
    ppermute x28, starting transfers between devices, swap(): return lax.ppermute(array, axes, [(i, i ^ offset) for i in range(size)])  38 us
    pallas_call x12, Pallas kernels, call(): pl.pallas_call(kernel, out_shape=outs, in_specs=in_specs or [VMEM] * len(...  17.1 us
  transfers between devices with their start and end apart: 28, of which 18 were waited for; matrix products, arithmetic and copies ran while one was open for 0% of the time, Pallas kernels for 6%

profile of v2, /device:TPU:0, one launch (start us, length us, event | category | flops | bytes accessed | tf_op | source)
XLA Modules:
  0.0 111.9 jit_solution(16450926433860456756)
XLA Ops:
  0.7 3.0 %collective-permute-start.1 = (bf16[16,1024]{1,0:T(8,128)(2,1)}, bf16[16,1024]{1,0:T(8,128)(2,1)S(1)}, u32[]{:S(2)}, u32[]{:S(2)}) collective-permute-start(bf16[16,1024]{1,0:T(8,128)(2,1)} %refs_0_.3), channel_id=1, source_target_pairs={{0,8},{1,9},{8,0},{9,1},{2,10},{3,11},{10,2},{11,3},{4,12},{5,13},... | collective-permute-start | bytes 98312 | tf_op jit(solution)/shard_map/ppermute | solution.py:40
  3.9 4.5 %fetch.1 = (bf16[1024,2816]{1,0:T(8,128)(2,1)S(1)}, bf16[1024,2816]{1,0:T(8,128)(2,1)S(1)}) custom-call(bf16[1024,2816]{1,0:T(8,128)(2,1)} %refs_0_.2, bf16[1024,2816]{1,0:T(8,128)(2,1)} %refs_1_.1), custom_call_target="tpu_custom_call" | custom-call | flops 100000 | tf_op jit(solution)/shard_map/fetch/pallas_call | solution.py:240
  8.5 2.1 %first.1 = (f32[16,5760]{1,0:T(8,128)S(1)}, bf16[16,5760]{1,0:T(8,128)(2,1)S(1)}, bf16[16,5760]{1,0:T(8,128)(2,1)S(1)}, bf16[16,5760]{1,0:T(8,128)(2,1)S(1)}, bf16[64,1024]{1,0:T(8,128)(2,1)S(1)}) custom-call(bf16[16,1024]{1,0:T(8,128)(2,1)S(1)} %copy-done.7, bf16[16,1024]{1,0:T(8,128)(2,1)S(1)} %collective-permute-done.refs_1_, ...), custom_call_target="tpu_custom_call" | custom-call | tf_op jit(solution)/shard_map/first/pallas_call | solution.py:240
  10.7 2.1 %collective-permute-start.3 = (bf16[16,5760]{1,0:T(8,128)(2,1)S(1)}, bf16[16,5760]{1,0:T(8,128)(2,1)S(1)}, u32[]{:S(2)}, u32[]{:S(2)}) collective-permute-start(bf16[16,5760]{1,0:T(8,128)(2,1)S(1)} %get-tuple-element.32), channel_id=1, source_target_pairs={{0,2},{2,0},{4,6},{6,4},{1,3},{3,1},{5,7},{7,5},{8,10},{10,8},{12,... | collective-permute-start | bytes 552968 | tf_op jit(solution)/shard_map/ppermute | solution.py:40
  12.8 2.6 %collective-permute-start.4 = (bf16[16,5760]{1,0:T(8,128)(2,1)S(1)}, bf16[16,5760]{1,0:T(8,128)(2,1)S(1)}, u32[]{:S(2)}, u32[]{:S(2)}) collective-permute-start(bf16[16,5760]{1,0:T(8,128)(2,1)S(1)} %get-tuple-element.33), channel_id=1, source_target_pairs={{0,4},{2,6},{4,0},{6,2},{1,5},{3,7},{5,1},{7,3},{8,12},{10,14},{12... | collective-permute-start | bytes 552968 | tf_op jit(solution)/shard_map/ppermute | solution.py:40
  15.3 5.5 %collective-permute-done.3.refs_1_ = bf16[16,5760]{1,0:T(8,128)(2,1)S(1)} collective-permute-done((bf16[16,5760]{1,0:T(8,128)(2,1)S(1)}, bf16[16,5760]{1,0:T(8,128)(2,1)S(1)}, u32[]{:S(2)}, u32[]{:S(2)}) %collective-permute-start.3) | collective-permute-done | bytes 184352 | tf_op jit(solution)/shard_map/ppermute | solution.py:40
  20.9 8.2 %collective-permute-done.4.refs_2_ = bf16[16,5760]{1,0:T(8,128)(2,1)S(1)} collective-permute-done((bf16[16,5760]{1,0:T(8,128)(2,1)S(1)}, bf16[16,5760]{1,0:T(8,128)(2,1)S(1)}, u32[]{:S(2)}, u32[]{:S(2)}) %collective-permute-start.4) | collective-permute-done | bytes 184352 | tf_op jit(solution)/shard_map/ppermute | solution.py:40
  29.3 2.5 %collective-permute-start.8 = (bf16[16,2816]{1,0:T(8,128)(2,1)S(1)}, bf16[16,2816]{1,0:T(8,128)(2,1)S(1)}, u32[]{:S(2)}, u32[]{:S(2)}) collective-permute-start(bf16[16,2816]{1,0:T(8,128)(2,1)S(1)} %hidden.2.refs_0_), channel_id=1, source_target_pairs={{0,6},{2,4},{4,2},{6,0},{1,7},{3,5},{5,3},{7,1},{8,14},{10,12},{12... | collective-permute-start | bytes 270344 | tf_op jit(solution)/shard_map/ppermute | solution.py:40
  31.8 3.3 %collective-permute-start.7 = (bf16[16,2816]{1,0:T(8,128)(2,1)S(1)}, bf16[16,2816]{1,0:T(8,128)(2,1)S(1)}, u32[]{:S(2)}, u32[]{:S(2)}) collective-permute-start(bf16[16,2816]{1,0:T(8,128)(2,1)S(1)} %hidden.2.refs_0_), channel_id=1, source_target_pairs={{0,4},{2,6},{4,0},{6,2},{1,5},{3,7},{5,1},{7,3},{8,12},{10,14},{12... | collective-permute-start | bytes 270344 | tf_op jit(solution)/shard_map/ppermute | solution.py:40
  35.9 4.5 %collective-permute-done.7.refs_2_ = bf16[16,2816]{1,0:T(8,128)(2,1)S(1)} collective-permute-done((bf16[16,2816]{1,0:T(8,128)(2,1)S(1)}, bf16[16,2816]{1,0:T(8,128)(2,1)S(1)}, u32[]{:S(2)}, u32[]{:S(2)}) %collective-permute-start.7) | collective-permute-done | bytes 90144 | tf_op jit(solution)/shard_map/ppermute | solution.py:40
  44.5 4.1 %collective-permute-done.10.refs_2_ = bf16[64,1024]{1,0:T(8,128)(2,1)S(1)} collective-permute-done((bf16[64,1024]{1,0:T(8,128)(2,1)S(1)}, bf16[64,1024]{1,0:T(8,128)(2,1)S(1)}, u32[]{:S(2)}, u32[]{:S(2)}) %collective-permute-start.10) | collective-permute-done | bytes 131104 | tf_op jit(solution)/shard_map/ppermute | solution.py:40
  49.8 2.9 %collective-permute-start.12 = (bf16[16,1920]{1,0:T(8,128)(2,1)S(1)}, bf16[16,1920]{1,0:T(8,128)(2,1)S(1)}, u32[]{:S(2)}, u32[]{:S(2)}) collective-permute-start(bf16[16,1920]{1,0:T(8,128)(2,1)S(1)} %get-tuple-element.38), channel_id=1, source_target_pairs={{0,4},{2,6},{4,0},{6,2},{1,5},{3,7},{5,1},{7,3},{8,12},{10,14},{12... | collective-permute-start | bytes 184328 | tf_op jit(solution)/shard_map/ppermute | solution.py:40
  55.5 3.3 %collective-permute-done.13.refs_3_ = bf16[16,1920]{1,0:T(8,128)(2,1)S(1)} collective-permute-done((bf16[16,1920]{1,0:T(8,128)(2,1)S(1)}, bf16[16,1920]{1,0:T(8,128)(2,1)S(1)}, u32[]{:S(2)}, u32[]{:S(2)}) %collective-permute-start.13) | collective-permute-done | bytes 61472 | tf_op jit(solution)/shard_map/ppermute | solution.py:40
  61.4 3.3 %collective-permute-start.14 = (bf16[16,512]{1,0:T(8,128)(2,1)S(1)}, bf16[16,512]{1,0:T(8,128)(2,1)S(1)}, u32[]{:S(2)}, u32[]{:S(2)}) collective-permute-start(bf16[16,512]{1,0:T(8,128)(2,1)S(1)} %get-tuple-element.40.refs_0_), channel_id=1, source_target_pairs={{0,2},{2,0},{4,6},{6,4},{1,3},{3,1},{5,7},{7,5},{8,10},{10,8},{12,... | collective-permute-start | bytes 49160 | tf_op jit(solution)/shard_map/ppermute | solution.py:40
  64.6 2.7 %state.2 = (f32[16,4,64,128]{3,2,1,0:T(8,128)}, f32[8,128]{1,0:T(8,128)S(1)}) custom-call(f32[256,128]{1,0:T(8,128)S(1)} %get-tuple-element.41.upright, f32[16,512]{1,0:T(8,128)S(1)} %get-tuple-element.42.value_rows, f32[16,4,64,128]{3,2,1,0:T(8,128)S(1)} %copy-done), custom_call_target="tpu_custom_call" | custom-call | flops 100000 | tf_op jit(solution)/shard_map/state/pallas_call | solution.py:240
  70.7 4.0 %collective-permute-done.18.refs_2_ = bf16[64,1024]{1,0:T(8,128)(2,1)S(1)} collective-permute-done((bf16[64,1024]{1,0:T(8,128)(2,1)S(1)}, bf16[64,1024]{1,0:T(8,128)(2,1)S(1)}, u32[]{:S(2)}, u32[]{:S(2)}) %collective-permute-start.18) | collective-permute-done | bytes 131104 | tf_op jit(solution)/shard_map/ppermute | solution.py:40
  74.8 2.1 %last.1 = (f32[16,5760]{1,0:T(8,128)S(1)}, bf16[16,5760]{1,0:T(8,128)(2,1)S(1)}, bf16[16,5760]{1,0:T(8,128)(2,1)S(1)}, bf16[16,5760]{1,0:T(8,128)(2,1)S(1)}, bf16[64,1024]{1,0:T(8,128)(2,1)S(1)}) custom-call(bf16[64,1024]{1,0:T(8,128)(2,1)S(1)} %get-tuple-element.35.refs_0_, bf16[64,1024]{1,0:T(8,128)(2,1)S(1)} %add_convert_fusion.refs_1_, ...), custom_call_target="tpu_custom_call" | custom-call | tf_op jit(solution)/shard_map/last/pallas_call | solution.py:240
  78.9 2.4 %collective-permute-start.21 = (bf16[16,5760]{1,0:T(8,128)(2,1)S(1)}, bf16[16,5760]{1,0:T(8,128)(2,1)S(1)}, u32[]{:S(2)}, u32[]{:S(2)}) collective-permute-start(bf16[16,5760]{1,0:T(8,128)(2,1)S(1)} %get-tuple-element.48), channel_id=1, source_target_pairs={{0,6},{2,4},{4,2},{6,0},{1,7},{3,5},{5,3},{7,1},{8,14},{10,12},{12... | collective-permute-start | bytes 552968 | tf_op jit(solution)/shard_map/ppermute | solution.py:40
  81.3 4.0 %collective-permute-done.19.refs_1_ = bf16[16,5760]{1,0:T(8,128)(2,1)S(1)} collective-permute-done((bf16[16,5760]{1,0:T(8,128)(2,1)S(1)}, bf16[16,5760]{1,0:T(8,128)(2,1)S(1)}, u32[]{:S(2)}, u32[]{:S(2)}) %collective-permute-start.19) | collective-permute-done | bytes 184352 | tf_op jit(solution)/shard_map/ppermute | solution.py:40
  85.3 8.4 %collective-permute-done.20.refs_2_ = bf16[16,5760]{1,0:T(8,128)(2,1)S(1)} collective-permute-done((bf16[16,5760]{1,0:T(8,128)(2,1)S(1)}, bf16[16,5760]{1,0:T(8,128)(2,1)S(1)}, u32[]{:S(2)}, u32[]{:S(2)}) %collective-permute-start.20) | collective-permute-done | bytes 184352 | tf_op jit(solution)/shard_map/ppermute | solution.py:40
  95.7 3.9 %collective-permute-start.23 = (bf16[16,2816]{1,0:T(8,128)(2,1)S(1)}, bf16[16,2816]{1,0:T(8,128)(2,1)S(1)}, u32[]{:S(2)}, u32[]{:S(2)}) collective-permute-start(bf16[16,2816]{1,0:T(8,128)(2,1)S(1)} %hidden.3.refs_0_), channel_id=1, source_target_pairs={{0,4},{2,6},{4,0},{6,2},{1,5},{3,7},{5,1},{7,3},{8,12},{10,14},{12... | collective-permute-start | bytes 270344 | tf_op jit(solution)/shard_map/ppermute | solution.py:40
  99.6 1.8 %collective-permute-done.24.refs_3_ = bf16[16,2816]{1,0:T(8,128)(2,1)S(1)} collective-permute-done((bf16[16,2816]{1,0:T(8,128)(2,1)S(1)}, bf16[16,2816]{1,0:T(8,128)(2,1)S(1)}, u32[]{:S(2)}, u32[]{:S(2)}) %collective-permute-start.24) | collective-permute-done | bytes 90144 | tf_op jit(solution)/shard_map/ppermute | solution.py:40
  101.4 3.5 %collective-permute-done.23.refs_2_ = bf16[16,2816]{1,0:T(8,128)(2,1)S(1)} collective-permute-done((bf16[16,2816]{1,0:T(8,128)(2,1)S(1)}, bf16[16,2816]{1,0:T(8,128)(2,1)S(1)}, u32[]{:S(2)}, u32[]{:S(2)}) %collective-permute-start.23) | collective-permute-done | bytes 90144 | tf_op jit(solution)/shard_map/ppermute | solution.py:40
  108.2 2.1 %collective-permute-done.26.refs_3_ = bf16[16,1024]{1,0:T(8,128)(2,1)S(1)} collective-permute-done((bf16[16,1024]{1,0:T(8,128)(2,1)S(1)}, bf16[16,1024]{1,0:T(8,128)(2,1)S(1)}, u32[]{:S(2)}, u32[]{:S(2)}) %collective-permute-start.26) | collective-permute-done | bytes 32800 | tf_op jit(solution)/shard_map/ppermute | solution.py:40
  (92 shorter events, 24.1 us)
Async XLA Ops:
  0.7 7.7 %collective-permute-start.1 = (bf16[16,1024]{1,0:T(8,128)(2,1)}, bf16[16,1024]{1,0:T(8,128)(2,1)S(1)}, u32[]{:S(2)}, u32[]{:S(2)}) collective-permute-start(bf16[16,1024]{1,0:T(8,128)(2,1)} %refs_0_.3), channel_id=1, source_target_pairs={{0,8},{1,9},{8,0},{9,1},{2,10},{3,11},{10,2},{11,3},{4,12},{5,13},... | collective-permute-start | bytes 98312 | tf_op jit(solution)/shard_map/ppermute | solution.py:40
  3.7 4.7 %collective-permute-start = (bf16[16,1024]{1,0:T(8,128)(2,1)}, bf16[16,1024]{1,0:T(8,128)(2,1)S(1)}, u32[]{:S(2)}, u32[]{:S(2)}) collective-permute-start(bf16[16,1024]{1,0:T(8,128)(2,1)} %refs_0_.3), channel_id=1, source_target_pairs={{0,1},{1,0},{8,9},{9,8},{2,3},{3,2},{10,11},{11,10},{4,5},{5,4},{1... | collective-permute-start | bytes 98312 | tf_op jit(solution)/shard_map/ppermute | solution.py:40
  3.7 4.7 %collective-permute-start.2 = (bf16[16,1024]{1,0:T(8,128)(2,1)}, bf16[16,1024]{1,0:T(8,128)(2,1)S(1)}, u32[]{:S(2)}, u32[]{:S(2)}) collective-permute-start(bf16[16,1024]{1,0:T(8,128)(2,1)} %refs_0_.3), channel_id=1, source_target_pairs={{0,9},{1,8},{8,1},{9,0},{2,11},{3,10},{10,3},{11,2},{4,13},{5,12},... | collective-permute-start | bytes 98312 | tf_op jit(solution)/shard_map/ppermute | solution.py:40
  10.7 10.2 %collective-permute-start.3 = (bf16[16,5760]{1,0:T(8,128)(2,1)S(1)}, bf16[16,5760]{1,0:T(8,128)(2,1)S(1)}, u32[]{:S(2)}, u32[]{:S(2)}) collective-permute-start(bf16[16,5760]{1,0:T(8,128)(2,1)S(1)} %get-tuple-element.32), channel_id=1, source_target_pairs={{0,2},{2,0},{4,6},{6,4},{1,3},{3,1},{5,7},{7,5},{8,10},{10,8},{12,... | collective-permute-start | bytes 552968 | tf_op jit(solution)/shard_map/ppermute | solution.py:40
  12.8 16.3 %collective-permute-start.4 = (bf16[16,5760]{1,0:T(8,128)(2,1)S(1)}, bf16[16,5760]{1,0:T(8,128)(2,1)S(1)}, u32[]{:S(2)}, u32[]{:S(2)}) collective-permute-start(bf16[16,5760]{1,0:T(8,128)(2,1)S(1)} %get-tuple-element.33), channel_id=1, source_target_pairs={{0,4},{2,6},{4,0},{6,2},{1,5},{3,7},{5,1},{7,3},{8,12},{10,14},{12... | collective-permute-start | bytes 552968 | tf_op jit(solution)/shard_map/ppermute | solution.py:40
  15.3 13.7 %collective-permute-start.5 = (bf16[16,5760]{1,0:T(8,128)(2,1)S(1)}, bf16[16,5760]{1,0:T(8,128)(2,1)S(1)}, u32[]{:S(2)}, u32[]{:S(2)}) collective-permute-start(bf16[16,5760]{1,0:T(8,128)(2,1)S(1)} %get-tuple-element.34), channel_id=1, source_target_pairs={{0,6},{2,4},{4,2},{6,0},{1,7},{3,5},{5,3},{7,1},{8,14},{10,12},{12... | collective-permute-start | bytes 552968 | tf_op jit(solution)/shard_map/ppermute | solution.py:40
  29.3 6.6 %collective-permute-start.8 = (bf16[16,2816]{1,0:T(8,128)(2,1)S(1)}, bf16[16,2816]{1,0:T(8,128)(2,1)S(1)}, u32[]{:S(2)}, u32[]{:S(2)}) collective-permute-start(bf16[16,2816]{1,0:T(8,128)(2,1)S(1)} %hidden.2.refs_0_), channel_id=1, source_target_pairs={{0,6},{2,4},{4,2},{6,0},{1,7},{3,5},{5,3},{7,1},{8,14},{10,12},{12... | collective-permute-start | bytes 270344 | tf_op jit(solution)/shard_map/ppermute | solution.py:40
  31.8 8.5 %collective-permute-start.7 = (bf16[16,2816]{1,0:T(8,128)(2,1)S(1)}, bf16[16,2816]{1,0:T(8,128)(2,1)S(1)}, u32[]{:S(2)}, u32[]{:S(2)}) collective-permute-start(bf16[16,2816]{1,0:T(8,128)(2,1)S(1)} %hidden.2.refs_0_), channel_id=1, source_target_pairs={{0,4},{2,6},{4,0},{6,2},{1,5},{3,7},{5,1},{7,3},{8,12},{10,14},{12... | collective-permute-start | bytes 270344 | tf_op jit(solution)/shard_map/ppermute | solution.py:40
  35.1 5.3 %collective-permute-start.6 = (bf16[16,2816]{1,0:T(8,128)(2,1)S(1)}, bf16[16,2816]{1,0:T(8,128)(2,1)S(1)}, u32[]{:S(2)}, u32[]{:S(2)}) collective-permute-start(bf16[16,2816]{1,0:T(8,128)(2,1)S(1)} %hidden.2.refs_0_), channel_id=1, source_target_pairs={{0,2},{2,0},{4,6},{6,4},{1,3},{3,1},{5,7},{7,5},{8,10},{10,8},{12,... | collective-permute-start | bytes 270344 | tf_op jit(solution)/shard_map/ppermute | solution.py:40
  43.0 5.6 %collective-permute-start.10 = (bf16[64,1024]{1,0:T(8,128)(2,1)S(1)}, bf16[64,1024]{1,0:T(8,128)(2,1)S(1)}, u32[]{:S(2)}, u32[]{:S(2)}) collective-permute-start(bf16[64,1024]{1,0:T(8,128)(2,1)S(1)} %add_convert_fusion.1.refs_1_), channel_id=1, source_target_pairs={{0,8},{1,9},{8,0},{9,1},{2,10},{3,11},{10,2},{11,3},{4,12},{5,13},... | collective-permute-start | bytes 393224 | tf_op jit(solution)/shard_map/ppermute | solution.py:40
  49.4 4.5 %collective-permute-start.11 = (bf16[16,1920]{1,0:T(8,128)(2,1)S(1)}, bf16[16,1920]{1,0:T(8,128)(2,1)S(1)}, u32[]{:S(2)}, u32[]{:S(2)}) collective-permute-start(bf16[16,1920]{1,0:T(8,128)(2,1)S(1)} %get-tuple-element.37), channel_id=1, source_target_pairs={{0,2},{2,0},{4,6},{6,4},{1,3},{3,1},{5,7},{7,5},{8,10},{10,8},{12,... | collective-permute-start | bytes 184328 | tf_op jit(solution)/shard_map/ppermute | solution.py:40
  49.8 5.7 %collective-permute-start.12 = (bf16[16,1920]{1,0:T(8,128)(2,1)S(1)}, bf16[16,1920]{1,0:T(8,128)(2,1)S(1)}, u32[]{:S(2)}, u32[]{:S(2)}) collective-permute-start(bf16[16,1920]{1,0:T(8,128)(2,1)S(1)} %get-tuple-element.38), channel_id=1, source_target_pairs={{0,4},{2,6},{4,0},{6,2},{1,5},{3,7},{5,1},{7,3},{8,12},{10,14},{12... | collective-permute-start | bytes 184328 | tf_op jit(solution)/shard_map/ppermute | solution.py:40
  52.8 6.0 %collective-permute-start.13 = (bf16[16,1920]{1,0:T(8,128)(2,1)S(1)}, bf16[16,1920]{1,0:T(8,128)(2,1)S(1)}, u32[]{:S(2)}, u32[]{:S(2)}) collective-permute-start(bf16[16,1920]{1,0:T(8,128)(2,1)S(1)} %get-tuple-element.39), channel_id=1, source_target_pairs={{0,6},{2,4},{4,2},{6,0},{1,7},{3,5},{5,3},{7,1},{8,14},{10,12},{12... | collective-permute-start | bytes 184328 | tf_op jit(solution)/shard_map/ppermute | solution.py:40
  60.2 7.1 %collective-permute-start.16 = (bf16[16,512]{1,0:T(8,128)(2,1)S(1)}, bf16[16,512]{1,0:T(8,128)(2,1)S(1)}, u32[]{:S(2)}, u32[]{:S(2)}) collective-permute-start(bf16[16,512]{1,0:T(8,128)(2,1)S(1)} %get-tuple-element.40.refs_0_), channel_id=1, source_target_pairs={{0,6},{2,4},{4,2},{6,0},{1,7},{3,5},{5,3},{7,1},{8,14},{10,12},{12... | collective-permute-start | bytes 49160 | tf_op jit(solution)/shard_map/ppermute | solution.py:40
  61.4 6.0 %collective-permute-start.15 = (bf16[16,512]{1,0:T(8,128)(2,1)S(1)}, bf16[16,512]{1,0:T(8,128)(2,1)S(1)}, u32[]{:S(2)}, u32[]{:S(2)}) collective-permute-start(bf16[16,512]{1,0:T(8,128)(2,1)S(1)} %get-tuple-element.40.refs_0_), channel_id=1, source_target_pairs={{0,4},{2,6},{4,0},{6,2},{1,5},{3,7},{5,1},{7,3},{8,12},{10,14},{12... | collective-permute-start | bytes 49160 | tf_op jit(solution)/shard_map/ppermute | solution.py:40
  61.4 6.0 %collective-permute-start.14 = (bf16[16,512]{1,0:T(8,128)(2,1)S(1)}, bf16[16,512]{1,0:T(8,128)(2,1)S(1)}, u32[]{:S(2)}, u32[]{:S(2)}) collective-permute-start(bf16[16,512]{1,0:T(8,128)(2,1)S(1)} %get-tuple-element.40.refs_0_), channel_id=1, source_target_pairs={{0,2},{2,0},{4,6},{6,4},{1,3},{3,1},{5,7},{7,5},{8,10},{10,8},{12,... | collective-permute-start | bytes 49160 | tf_op jit(solution)/shard_map/ppermute | solution.py:40
  69.1 5.6 %collective-permute-start.18 = (bf16[64,1024]{1,0:T(8,128)(2,1)S(1)}, bf16[64,1024]{1,0:T(8,128)(2,1)S(1)}, u32[]{:S(2)}, u32[]{:S(2)}) collective-permute-start(bf16[64,1024]{1,0:T(8,128)(2,1)S(1)} %add_convert_fusion.refs_1_), channel_id=1, source_target_pairs={{0,8},{1,9},{8,0},{9,1},{2,10},{3,11},{10,2},{11,3},{4,12},{5,13},... | collective-permute-start | bytes 393224 | tf_op jit(solution)/shard_map/ppermute | solution.py:40
  76.9 8.4 %collective-permute-start.19 = (bf16[16,5760]{1,0:T(8,128)(2,1)S(1)}, bf16[16,5760]{1,0:T(8,128)(2,1)S(1)}, u32[]{:S(2)}, u32[]{:S(2)}) collective-permute-start(bf16[16,5760]{1,0:T(8,128)(2,1)S(1)} %get-tuple-element.46), channel_id=1, source_target_pairs={{0,2},{2,0},{4,6},{6,4},{1,3},{3,1},{5,7},{7,5},{8,10},{10,8},{12,... | collective-permute-start | bytes 552968 | tf_op jit(solution)/shard_map/ppermute | solution.py:40
  78.0 15.7 %collective-permute-start.20 = (bf16[16,5760]{1,0:T(8,128)(2,1)S(1)}, bf16[16,5760]{1,0:T(8,128)(2,1)S(1)}, u32[]{:S(2)}, u32[]{:S(2)}) collective-permute-start(bf16[16,5760]{1,0:T(8,128)(2,1)S(1)} %get-tuple-element.47), channel_id=1, source_target_pairs={{0,4},{2,6},{4,0},{6,2},{1,5},{3,7},{5,1},{7,3},{8,12},{10,14},{12... | collective-permute-start | bytes 552968 | tf_op jit(solution)/shard_map/ppermute | solution.py:40
  78.9 14.8 %collective-permute-start.21 = (bf16[16,5760]{1,0:T(8,128)(2,1)S(1)}, bf16[16,5760]{1,0:T(8,128)(2,1)S(1)}, u32[]{:S(2)}, u32[]{:S(2)}) collective-permute-start(bf16[16,5760]{1,0:T(8,128)(2,1)S(1)} %get-tuple-element.48), channel_id=1, source_target_pairs={{0,6},{2,4},{4,2},{6,0},{1,7},{3,5},{5,3},{7,1},{8,14},{10,12},{12... | collective-permute-start | bytes 552968 | tf_op jit(solution)/shard_map/ppermute | solution.py:40
  93.9 7.5 %collective-permute-start.24 = (bf16[16,2816]{1,0:T(8,128)(2,1)S(1)}, bf16[16,2816]{1,0:T(8,128)(2,1)S(1)}, u32[]{:S(2)}, u32[]{:S(2)}) collective-permute-start(bf16[16,2816]{1,0:T(8,128)(2,1)S(1)} %hidden.3.refs_0_), channel_id=1, source_target_pairs={{0,6},{2,4},{4,2},{6,0},{1,7},{3,5},{5,3},{7,1},{8,14},{10,12},{12... | collective-permute-start | bytes 270344 | tf_op jit(solution)/shard_map/ppermute | solution.py:40
  95.7 9.1 %collective-permute-start.23 = (bf16[16,2816]{1,0:T(8,128)(2,1)S(1)}, bf16[16,2816]{1,0:T(8,128)(2,1)S(1)}, u32[]{:S(2)}, u32[]{:S(2)}) collective-permute-start(bf16[16,2816]{1,0:T(8,128)(2,1)S(1)} %hidden.3.refs_0_), channel_id=1, source_target_pairs={{0,4},{2,6},{4,0},{6,2},{1,5},{3,7},{5,1},{7,3},{8,12},{10,14},{12... | collective-permute-start | bytes 270344 | tf_op jit(solution)/shard_map/ppermute | solution.py:40
  99.6 5.5 %collective-permute-start.22 = (bf16[16,2816]{1,0:T(8,128)(2,1)S(1)}, bf16[16,2816]{1,0:T(8,128)(2,1)S(1)}, u32[]{:S(2)}, u32[]{:S(2)}) collective-permute-start(bf16[16,2816]{1,0:T(8,128)(2,1)S(1)} %hidden.3.refs_0_), channel_id=1, source_target_pairs={{0,2},{2,0},{4,6},{6,4},{1,3},{3,1},{5,7},{7,5},{8,10},{10,8},{12,... | collective-permute-start | bytes 270344 | tf_op jit(solution)/shard_map/ppermute | solution.py:40
  106.3 4.0 %collective-permute-start.26 = (bf16[16,1024]{1,0:T(8,128)(2,1)S(1)}, bf16[16,1024]{1,0:T(8,128)(2,1)S(1)}, u32[]{:S(2)}, u32[]{:S(2)}) collective-permute-start(bf16[16,1024]{1,0:T(8,128)(2,1)S(1)} %get-tuple-element.51), channel_id=1, source_target_pairs={{0,8},{1,9},{8,0},{9,1},{2,10},{3,11},{10,2},{11,3},{4,12},{5,13},... | collective-permute-start | bytes 98312 | tf_op jit(solution)/shard_map/ppermute | solution.py:40
  (25 other events, 708.7 us)

commit v3 on v2

--- a/solution.py
+++ b/solution.py
@@ -67,12 +67,13 @@
         copy.wait()
 
 
-def multiply_blocks(scaled, weight, base, outs):
+def multiply_blocks(scaled, weight, columns, base, outs):
     height = outs[0].shape[0]
-    width = weight.shape[1]
+    first, width = columns
     step = column_step(width)
     for low in range(0, width, step):
-        product = jnp.dot(scaled, weight[:, low : low + step], preferred_element_type=F32)
+        piece = weight[:, first + low : first + low + step]
+        product = jnp.dot(scaled, piece, preferred_element_type=F32)
         for k, out in enumerate(outs):
             block = product[k * height : (k + 1) * height]
             out[:, base + low : base + low + step] = block.astype(out.dtype)
@@ -85,24 +86,42 @@
         out[:, low : low + LANES] = block[k * height : (k + 1) * height].astype(out.dtype)
 
 
-def project_rows(widened, gain, weights, outs):
-    scaled = (widened * gain[...]).astype(BF16)
+def project_rows(scaled, weights, columns, outs):
     base = 0
     for weight in weights:
-        multiply_blocks(scaled, weight, base, outs)
-        base += padded(weight.shape[1])
+        span = columns or (0, weight.shape[1])
+        multiply_blocks(scaled, weight, span, base, outs)
+        base += padded(span[1])
+    return base
+
+
+def project_with_squares(widened, gain, weights, columns, outs):
+    scaled = (widened * gain[...]).astype(BF16)
+    base = project_rows(scaled, weights, columns, outs)
     put_squares(jnp.sum(widened * widened, axis=1, keepdims=True), base, outs)
-
-
-def first_kernel(n_dt, n_kv, names, *refs):
+    return scaled
+
+
+def first_kernel(n_dt, n_kv, names, columns, *refs):
     own, others, refs = refs[0], refs[1:n_dt], refs[n_dt:]
     gain, weights, refs = refs[0], refs[1:3], refs[3:]
-    outs, gathered = refs[:n_kv], refs[n_kv]
+    outs, (gathered, scaled) = refs[:n_kv], refs[n_kv:]
     height = own.shape[0]
     place = linear_index(names[0]) ^ linear_index(names[1])
     for k, block in enumerate((own, *others)):
         gathered[rows_at(place ^ k, height), :] = block[...]
-    project_rows(gathered[...].astype(F32), gain, weights, outs)
+    scaled[...] = project_with_squares(gathered[...].astype(F32), gain, weights, columns, outs)
+
+
+def last_kernel(n_parts, columns, *refs):
+    residual, parts, refs = refs[0], refs[1 : 1 + n_parts], refs[1 + n_parts :]
+    gain, weights, (*outs, stream, scaled) = refs[0], refs[1:3], refs[3:]
+    stream[...] = add_parts(residual, parts, 1.0)
+    scaled[...] = project_with_squares(stream[...].astype(F32), gain, weights, columns, outs)
+
+
+def more_kernel(columns, scaled, gate, up, *outs):
+    project_rows(scaled[...], (gate, up), columns, outs)
 
 
 def add_parts(residual, parts, half):
@@ -117,7 +136,7 @@
     gain, weights, refs = refs[0], refs[1 : 1 + n_weights], refs[1 + n_weights :]
     outs, stream = refs[:-1], refs[-1]
     stream[...] = add_parts(residual, parts, half)
-    project_rows(stream[...].astype(F32), gain, weights, outs)
+    project_with_squares(stream[...].astype(F32), gain, weights, None, outs)
 
 
 def sum_columns(parts, low, size):
@@ -128,10 +147,20 @@
 
 
 def hidden_kernel(features, n_kv, *refs):
-    parts, out = refs[:n_kv], refs[n_kv]
+    parts, out, scale = refs[:n_kv], refs[n_kv], refs[n_kv + 1]
+    squares = join_square_sum(sum_columns(parts, 2 * padded(out.shape[1]), LANES))
+    factor = lax.rsqrt(squares / features + EPSILON)
+    scale[...] = jnp.broadcast_to(factor, scale.shape)
+    activate(factor, parts, out)
+
+
+def more_hidden_kernel(n_kv, *refs):
+    activate(refs[n_kv][:, :1], refs[:n_kv], refs[n_kv + 1])
+
+
+def activate(scale, parts, out):
     width = out.shape[1]
     gap = padded(width)
-    scale = lax.rsqrt(join_square_sum(sum_columns(parts, 2 * gap, LANES)) / features + EPSILON)
     step = column_step(width)
     for low in range(0, width, step):
         gate = jax.nn.silu(scale * sum_columns(parts, low, step))
@@ -144,25 +173,35 @@
         rows[k * height : (k + 1) * height, :] = block[...]
 
 
-def down_kernel(n_blocks, *refs):
-    blocks, weight, (out, rows) = refs[:n_blocks], refs[n_blocks], refs[-2:]
-    stack_rows(blocks, rows)
+def multiply_down(rows, weight, first_row, out, addend=None):
     step = column_step(weight.shape[1])
     for low in range(0, weight.shape[1], step):
-        product = jnp.dot(rows[...], weight[:, low : low + step], preferred_element_type=F32)
-        out[:, low : low + step] = product.astype(BF16)
-
-
-def scatter_down_kernel(n_blocks, names, *refs):
-    blocks, weight = refs[:n_blocks], refs[n_blocks]
-    outs, (rows, product) = refs[n_blocks + 1 : -2], refs[-2:]
+        piece = weight[first_row : first_row + rows.shape[1], low : low + step]
+        product = jnp.dot(rows[...], piece, preferred_element_type=F32)
+        if addend is not None:
+            product = product + addend[:, low : low + step]
+        out[:, low : low + step] = product.astype(out.dtype)
+
+
+def down_kernel(n_blocks, *refs):
+    blocks, (weight, out, rows) = refs[:n_blocks], refs[n_blocks:]
     stack_rows(blocks, rows)
+    multiply_down(rows, weight, 0, out)
+
+
+def more_down_kernel(n_blocks, first_row, *refs):
+    blocks, (weight, addend, out, rows) = refs[:n_blocks], refs[n_blocks:]
+    stack_rows(blocks, rows)
+    multiply_down(rows, weight, first_row, out, addend)
+
+
+def scatter_down_kernel(n_blocks, first_row, names, *refs):
+    blocks, (weight, addend), refs = refs[:n_blocks], refs[n_blocks : n_blocks + 2], refs[n_blocks + 2 :]
+    outs, (rows, product) = refs[:-2], refs[-2:]
+    stack_rows(blocks, rows)
+    multiply_down(rows, weight, first_row, product, addend)
     height = blocks[0].shape[0]
     place = linear_index(names[0]) ^ linear_index(names[1])
-    step = column_step(weight.shape[1])
-    for low in range(0, weight.shape[1], step):
-        columns = slice(low, low + step)
-        product[:, columns] = jnp.dot(rows[...], weight[:, columns], preferred_element_type=F32).astype(BF16)
     for k, out in enumerate(outs):
         out[...] = product[rows_at(place ^ k, height), :]
 
@@ -235,18 +274,22 @@
     return size
 
 
-def call(kernel, name, outs, inputs, scratch=(), in_specs=None, work=0, cores=8 * MIB):
+def call(kernel, name, outs, inputs, scratch=(), in_specs=None, work=0, after=()):
     arrays = [*inputs, *jax.tree.leaves(outs)]
+
+    def body(*refs):
+        kernel(*refs[: len(inputs)], *refs[len(inputs) + len(after) :])
+
     return pl.pallas_call(
-        kernel,
+        body,
         out_shape=outs,
-        in_specs=in_specs or [VMEM] * len(inputs),
+        in_specs=(in_specs or [VMEM] * len(inputs)) + [pl.BlockSpec(memory_space=pl.ANY)] * len(after),
         out_specs=jax.tree.map(lambda _: VMEM, outs),
         scratch_shapes=list(scratch),
-        compiler_params=pltpu.CompilerParams(vmem_limit_bytes=sum(map(array_bytes, arrays)) + cores),
+        compiler_params=pltpu.CompilerParams(vmem_limit_bytes=sum(map(array_bytes, arrays)) + 8 * MIB),
         cost_estimate=pl.CostEstimate(flops=work, bytes_accessed=0, transcendentals=0),
         name=name,
-    )(*inputs)
+    )(*inputs, *after)
 
 
 def per_device(
@@ -286,27 +329,56 @@
         return [block] + [swap(block, kv, n_kv, k) for k in range(1, n_kv)]
 
     def total_parts(part):
-        offset = 1
-        while 2 * offset < n_dt:
+        offset = n_dt // 2
+        while offset > 1:
             part = (part.astype(F32) + swap(part, dt, n_dt, offset).astype(F32)).astype(BF16)
-            offset *= 2
+            offset //= 2
         return [part, swap(part, dt, n_dt, offset)]
 
-    def project(kernel, name, weights, inputs):
-        span = sum(padded(w.shape[1]) for w in weights) + LANES
-        outs = [shape((height, span), F32)] + [shape((height, span), BF16)] * (n_kv - 1)
-        return call(kernel, name, outs + [shape((rows, width), BF16)], (*inputs, *weights))
-
-    def hidden_rows(blocks, units):
-        kernel = functools.partial(hidden_kernel, features, n_kv)
-        return gather_rows(call(kernel, "hidden", shape((height, units), BF16), collect(blocks)))
+    def row_blocks(span):
+        return [shape((height, span), F32)] + [shape((height, span), BF16)] * (n_kv - 1)
+
+    def stack(unit):
+        return [pltpu.VMEM((rows, unit), BF16)]
+
+    def mixer(kernel, name, inputs, weights, down_weight, finish, finish_outs, finish_scratch):
+        units = weights[0].shape[1]
+        near = min(-(-units // 2 // 256) * 256, units)
+        rest = units - near
+        *blocks, stream, scaled = call(
+            functools.partial(kernel, (0, near)),
+            name,
+            row_blocks(2 * padded(near) + LANES) + [shape((rows, width), BF16)] * 2,
+            (*inputs, *weights),
+        )
+        more = call(
+            functools.partial(more_kernel, (near, rest)), name + "_more", row_blocks(2 * padded(rest)), (scaled, *weights)
+        )
+        outs = [shape((height, near), BF16), shape((height, LANES), F32)]
+        parts = collect(blocks)
+        more_parts = collect(more)
+        hidden, scale = call(functools.partial(hidden_kernel, features, n_kv), "hidden", outs, parts)
+        hidden = gather_rows(hidden)
+        more_hidden = call(
+            functools.partial(more_hidden_kernel, n_kv), "hidden_more", shape((height, rest), BF16), (*more_parts, scale)
+        )
+        more_hidden = gather_rows(more_hidden)
+        product = call(
+            functools.partial(down_kernel, n_kv), name + "_down", shape((rows, width), F32), (*hidden, down_weight), stack(near)
+        )
+        return stream, call(
+            functools.partial(finish, n_kv, near),
+            name + "_down_more",
+            finish_outs,
+            (*more_hidden, down_weight, product),
+            stack(rest) + finish_scratch,
+        )
 
     def down(blocks, weight, name, *after):
         kernel = functools.partial(down_kernel, n_kv)
-        scratch = [pltpu.VMEM((rows, weight.shape[0]), BF16)]
-        return call(kernel, name, shape((rows, weight.shape[1]), BF16), (*blocks, weight, *after), scratch)
-
-    units = leading_gate_weight.shape[1]
+        inputs = (*blocks, weight)
+        return call(kernel, name, shape((rows, weight.shape[1]), BF16), inputs, stack(weight.shape[0]), after=after)
+
     arrived = [swap(residual_input, dt, n_dt, k) for k in range(1, n_dt)]
     fetched = [
         pltpu.with_memory_space_constraint(w, pltpu.HBM) for w in (leading_gate_weight, leading_up_weight)
@@ -320,20 +392,26 @@
         [pl.BlockSpec(memory_space=pltpu.HBM)] * 2,
         100000,
     )
-    *blocks, gathered = project(
+    whole_rows = shape((rows, width), BF16)
+    gathered, part = mixer(
         functools.partial(first_kernel, n_dt, n_kv, names),
         "first",
+        (residual_input, *arrived, leading_norm_gain.reshape(1, width)),
         (gate, up),
-        (residual_input, *arrived, leading_norm_gain.reshape(1, width)),
-    )
-    parts = total_parts(down(hidden_rows(blocks, units), leading_down_weight, "first_down"))
+        leading_down_weight,
+        more_down_kernel,
+        whole_rows,
+        [],
+    )
+    parts = total_parts(part)
 
     mixed = (query_projector, key_projector, forget_weight, value_projector, output_gate_weight)
-    *blocks, after_first = project(
+    span = sum(padded(w.shape[1]) for w in mixed) + LANES
+    *blocks, after_first = call(
         functools.partial(project_kernel, 0.5, len(parts), len(mixed)),
         "attention_in",
-        mixed,
-        (gathered, *parts, attention_norm_gain.reshape(1, width)),
+        row_blocks(span) + [whole_rows],
+        (gathered, *parts, attention_norm_gain.reshape(1, width), *mixed),
     )
     blocks = collect(blocks)
     heads = incoming_state.shape[1]
@@ -351,20 +429,15 @@
     new_state, finished = call(state_kernel, "state", outs, (upright, value_rows, incoming_state), work=100000)
     parts = total_parts(down(known, output_projector, "attention_out", finished))
 
-    last = (trailing_gate_weight, trailing_up_weight)
-    *blocks, second = project(
-        functools.partial(project_kernel, 1.0, len(parts), len(last)),
+    second, parts = mixer(
+        functools.partial(last_kernel, len(parts)),
         "last",
-        last,
         (after_first, *parts, trailing_norm_gain.reshape(1, width)),
-    )
-    hidden = hidden_rows(blocks, units)
-    parts = call(
-        functools.partial(scatter_down_kernel, n_kv, names),
-        "last_down",
+        (trailing_gate_weight, trailing_up_weight),
+        trailing_down_weight,
+        lambda n_blocks, first_row, *refs: scatter_down_kernel(n_blocks, first_row, names, *refs),
         [shape((height, width), BF16)] * n_dt,
-        (*hidden, trailing_down_weight),
-        [pltpu.VMEM((rows, trailing_down_weight.shape[0]), BF16), pltpu.VMEM((rows, width), BF16)],
+        [pltpu.VMEM((rows, width), BF16)],
     )
     parts = [parts[0]] + swaps(parts[1:], dt, n_dt)
     result = call(

time: 112 us -> 109 us (0.973)
  waiting for transfers between devices: 55.6 us -> 29.7 us
  starting transfers between devices: 38 us -> 60.3 us
    ppermute x28 -> x40, waiting for transfers between devices: 55.6 us -> 29.7 us  [swap(): return lax.ppermute(array, axes, [(i, i ^ offset) for i in range(size)])]
    ppermute x28 -> x40, starting transfers between devices: 38 us -> 60.3 us  [swap(): return lax.ppermute(array, axes, [(i, i ^ offset) for i in range(size)])]
    pallas_call x12 -> x18, Pallas kernels: 17.1 us -> 17.6 us  [call(): pl.pallas_call(body, out_shape=outs, in_specs=(in_specs or [VMEM] * len(i...]
  transfers between devices with their start and end apart: 28 -> 40, of which waited for: 18 -> 18; matrix products, arithmetic and copies ran while one was open for 0% -> 0% of each run, Pallas kernels for 6% -> 10%
where the time goes in v3:
time: 109 us
  starting transfers between devices  60.3 us (55%)
  waiting for transfers between devices  29.7 us (27%)
  Pallas kernels  17.6 us (16%)
  between operations  1.09 us (1%)
    ppermute x40, starting transfers between devices, swap(): return lax.ppermute(array, axes, [(i, i ^ offset) for i in range(size)])  60.3 us
    ppermute x40, waiting for transfers between devices, swap(): return lax.ppermute(array, axes, [(i, i ^ offset) for i in range(size)])  29.7 us
    pallas_call x18, Pallas kernels, call(): pl.pallas_call(body, out_shape=outs, in_specs=(in_specs or [VMEM] * len(i...  17.6 us
  transfers between devices with their start and end apart: 40, of which 18 were waited for; matrix products, arithmetic and copies ran while one was open for 0% of the time, Pallas kernels for 10%

profile of v3, /device:TPU:0, one launch (start us, length us, event | category | flops | bytes accessed | tf_op | source)
XLA Modules:
  0.0 108.9 jit_solution(14518318388410970871)
XLA Ops:
  1.2 2.6 %collective-permute-start.1 = (bf16[16,1024]{1,0:T(8,128)(2,1)}, bf16[16,1024]{1,0:T(8,128)(2,1)S(1)}, u32[]{:S(2)}, u32[]{:S(2)}) collective-permute-start(bf16[16,1024]{1,0:T(8,128)(2,1)} %refs_0_.3), channel_id=1, source_target_pairs={{0,8},{1,9},{8,0},{9,1},{2,10},{3,11},{10,2},{11,3},{4,12},{5,13},... | collective-permute-start | bytes 98312 | tf_op jit(solution)/shard_map/ppermute | solution.py:40
  3.8 4.4 %fetch.1 = (bf16[1024,2816]{1,0:T(8,128)(2,1)S(1)}, bf16[1024,2816]{1,0:T(8,128)(2,1)S(1)}) custom-call(bf16[1024,2816]{1,0:T(8,128)(2,1)} %refs_0_.2, bf16[1024,2816]{1,0:T(8,128)(2,1)} %refs_1_.2), custom_call_target="tpu_custom_call" | custom-call | flops 100000 | tf_op jit(solution)/shard_map/fetch/pallas_call | solution.py:283
  9.5 1.9 %collective-permute-start.6 = (bf16[16,3200]{1,0:T(8,128)(2,1)S(1)}, bf16[16,3200]{1,0:T(8,128)(2,1)S(1)}, u32[]{:S(2)}, u32[]{:S(2)}) collective-permute-start(bf16[16,3200]{1,0:T(8,128)(2,1)S(1)} %get-tuple-element.51), channel_id=1, source_target_pairs={{0,2},{2,0},{4,6},{6,4},{1,3},{3,1},{5,7},{7,5},{8,10},{10,8},{12,... | collective-permute-start | bytes 307208 | tf_op jit(solution)/shard_map/ppermute | solution.py:40
  11.4 2.6 %collective-permute-start.7 = (bf16[16,3200]{1,0:T(8,128)(2,1)S(1)}, bf16[16,3200]{1,0:T(8,128)(2,1)S(1)}, u32[]{:S(2)}, u32[]{:S(2)}) collective-permute-start(bf16[16,3200]{1,0:T(8,128)(2,1)S(1)} %get-tuple-element.52), channel_id=1, source_target_pairs={{0,4},{2,6},{4,0},{6,2},{1,5},{3,7},{5,1},{7,3},{8,12},{10,14},{12... | collective-permute-start | bytes 307208 | tf_op jit(solution)/shard_map/ppermute | solution.py:40
  16.0 3.5 %collective-permute-start.4 = (bf16[16,2560]{1,0:T(8,128)(2,1)S(1)}, bf16[16,2560]{1,0:T(8,128)(2,1)S(1)}, u32[]{:S(2)}, u32[]{:S(2)}) collective-permute-start(bf16[16,2560]{1,0:T(8,128)(2,1)S(1)} %get-tuple-element.48), channel_id=1, source_target_pairs={{0,4},{2,6},{4,0},{6,2},{1,5},{3,7},{5,1},{7,3},{8,12},{10,14},{12... | collective-permute-start | bytes 245768 | tf_op jit(solution)/shard_map/ppermute | solution.py:40
  19.6 2.8 %collective-permute-done.7.refs_2_ = bf16[16,3200]{1,0:T(8,128)(2,1)S(1)} collective-permute-done((bf16[16,3200]{1,0:T(8,128)(2,1)S(1)}, bf16[16,3200]{1,0:T(8,128)(2,1)S(1)}, u32[]{:S(2)}, u32[]{:S(2)}) %collective-permute-start.7) | collective-permute-done | bytes 102432 | tf_op jit(solution)/shard_map/ppermute | solution.py:40
  22.6 6.3 %collective-permute-start.12 = (bf16[16,1536]{1,0:T(8,128)(2,1)S(1)}, bf16[16,1536]{1,0:T(8,128)(2,1)S(1)}, u32[]{:S(2)}, u32[]{:S(2)}) collective-permute-start(bf16[16,1536]{1,0:T(8,128)(2,1)S(1)} %get-tuple-element.55.refs_0_), channel_id=1, source_target_pairs={{0,2},{2,0},{4,6},{6,4},{1,3},{3,1},{5,7},{7,5},{8,10},{10,8},{12,... | collective-permute-start | bytes 147464 | tf_op jit(solution)/shard_map/ppermute | solution.py:40
  31.7 2.4 %collective-permute-start.10 = (bf16[16,1280]{1,0:T(8,128)(2,1)S(1)}, bf16[16,1280]{1,0:T(8,128)(2,1)S(1)}, u32[]{:S(2)}, u32[]{:S(2)}) collective-permute-start(bf16[16,1280]{1,0:T(8,128)(2,1)S(1)} %hidden_more.2.refs_0_), channel_id=1, source_target_pairs={{0,4},{2,6},{4,0},{6,2},{1,5},{3,7},{5,1},{7,3},{8,12},{10,14},{12... | collective-permute-start | bytes 122888 | tf_op jit(solution)/shard_map/ppermute | solution.py:40
  37.8 2.0 %collective-permute-done.11.refs_3_ = bf16[16,1280]{1,0:T(8,128)(2,1)S(1)} collective-permute-done((bf16[16,1280]{1,0:T(8,128)(2,1)S(1)}, bf16[16,1280]{1,0:T(8,128)(2,1)S(1)}, u32[]{:S(2)}, u32[]{:S(2)}) %collective-permute-start.11) | collective-permute-done | bytes 40992 | tf_op jit(solution)/shard_map/ppermute | solution.py:40
  42.0 3.5 %collective-permute-done.15 = bf16[64,1024]{1,0:T(8,128)(2,1)S(1)} collective-permute-done((bf16[64,1024]{1,0:T(8,128)(2,1)S(1)}, bf16[64,1024]{1,0:T(8,128)(2,1)S(1)}, u32[]{:S(2)}, u32[]{:S(2)}) %collective-permute-start.15) | collective-permute-done | bytes 131104 | tf_op jit(solution)/shard_map/ppermute | solution.py:40
  47.8 2.6 %collective-permute-start.18 = (bf16[16,1920]{1,0:T(8,128)(2,1)S(1)}, bf16[16,1920]{1,0:T(8,128)(2,1)S(1)}, u32[]{:S(2)}, u32[]{:S(2)}) collective-permute-start(bf16[16,1920]{1,0:T(8,128)(2,1)S(1)} %get-tuple-element.59), channel_id=1, source_target_pairs={{0,4},{2,6},{4,0},{6,2},{1,5},{3,7},{5,1},{7,3},{8,12},{10,14},{12... | collective-permute-start | bytes 184328 | tf_op jit(solution)/shard_map/ppermute | solution.py:40
  52.9 2.6 %collective-permute-done.18.refs_2_ = bf16[16,1920]{1,0:T(8,128)(2,1)S(1)} collective-permute-done((bf16[16,1920]{1,0:T(8,128)(2,1)S(1)}, bf16[16,1920]{1,0:T(8,128)(2,1)S(1)}, u32[]{:S(2)}, u32[]{:S(2)}) %collective-permute-start.18) | collective-permute-done | bytes 61472 | tf_op jit(solution)/shard_map/ppermute | solution.py:40
  60.4 2.0 %collective-permute-start.22 = (bf16[16,512]{1,0:T(8,128)(2,1)S(1)}, bf16[16,512]{1,0:T(8,128)(2,1)S(1)}, u32[]{:S(2)}, u32[]{:S(2)}) collective-permute-start(bf16[16,512]{1,0:T(8,128)(2,1)S(1)} %get-tuple-element.61.refs_0_), channel_id=1, source_target_pairs={{0,6},{2,4},{4,2},{6,0},{1,7},{3,5},{5,3},{7,1},{8,14},{10,12},{12... | collective-permute-start | bytes 49160 | tf_op jit(solution)/shard_map/ppermute | solution.py:40
  62.4 2.7 %state.1 = (f32[16,4,64,128]{3,2,1,0:T(8,128)}, f32[8,128]{1,0:T(8,128)S(1)}) custom-call(f32[256,128]{1,0:T(8,128)S(1)} %get-tuple-element.62.refs_0_, f32[16,512]{1,0:T(8,128)S(1)} %get-tuple-element.63.refs_1_, f32[16,4,64,128]{3,2,1,0:T(8,128)S(1)} %copy-done), custom_call_target="tpu_custom_call" | custom-call | flops 100000 | tf_op jit(solution)/shard_map/state/pallas_call | solution.py:283
  67.8 3.5 %collective-permute-done.23 = bf16[64,1024]{1,0:T(8,128)(2,1)S(1)} collective-permute-done((bf16[64,1024]{1,0:T(8,128)(2,1)S(1)}, bf16[64,1024]{1,0:T(8,128)(2,1)S(1)}, u32[]{:S(2)}, u32[]{:S(2)}) %collective-permute-start.23) | collective-permute-done | bytes 131104 | tf_op jit(solution)/shard_map/ppermute | solution.py:40
  74.0 2.6 %collective-permute-start.29 = (bf16[16,3200]{1,0:T(8,128)(2,1)S(1)}, bf16[16,3200]{1,0:T(8,128)(2,1)S(1)}, u32[]{:S(2)}, u32[]{:S(2)}) collective-permute-start(bf16[16,3200]{1,0:T(8,128)(2,1)S(1)} %get-tuple-element.73), channel_id=1, source_target_pairs={{0,4},{2,6},{4,0},{6,2},{1,5},{3,7},{5,1},{7,3},{8,12},{10,14},{12... | collective-permute-start | bytes 307208 | tf_op jit(solution)/shard_map/ppermute | solution.py:40
  76.6 1.8 %collective-permute-start.30 = (bf16[16,3200]{1,0:T(8,128)(2,1)S(1)}, bf16[16,3200]{1,0:T(8,128)(2,1)S(1)}, u32[]{:S(2)}, u32[]{:S(2)}) collective-permute-start(bf16[16,3200]{1,0:T(8,128)(2,1)S(1)} %get-tuple-element.74), channel_id=1, source_target_pairs={{0,6},{2,4},{4,2},{6,0},{1,7},{3,5},{5,3},{7,1},{8,14},{10,12},{12... | collective-permute-start | bytes 307208 | tf_op jit(solution)/shard_map/ppermute | solution.py:40
  79.5 2.6 %collective-permute-start.26 = (bf16[16,2560]{1,0:T(8,128)(2,1)S(1)}, bf16[16,2560]{1,0:T(8,128)(2,1)S(1)}, u32[]{:S(2)}, u32[]{:S(2)}) collective-permute-start(bf16[16,2560]{1,0:T(8,128)(2,1)S(1)} %get-tuple-element.69), channel_id=1, source_target_pairs={{0,4},{2,6},{4,0},{6,2},{1,5},{3,7},{5,1},{7,3},{8,12},{10,14},{12... | collective-permute-start | bytes 245768 | tf_op jit(solution)/shard_map/ppermute | solution.py:40
  82.1 1.8 %collective-permute-start.27 = (bf16[16,2560]{1,0:T(8,128)(2,1)S(1)}, bf16[16,2560]{1,0:T(8,128)(2,1)S(1)}, u32[]{:S(2)}, u32[]{:S(2)}) collective-permute-start(bf16[16,2560]{1,0:T(8,128)(2,1)S(1)} %get-tuple-element.70), channel_id=1, source_target_pairs={{0,6},{2,4},{4,2},{6,0},{1,7},{3,5},{5,3},{7,1},{8,14},{10,12},{12... | collective-permute-start | bytes 245768 | tf_op jit(solution)/shard_map/ppermute | solution.py:40
  85.9 5.9 %collective-permute-start.34 = (bf16[16,1536]{1,0:T(8,128)(2,1)S(1)}, bf16[16,1536]{1,0:T(8,128)(2,1)S(1)}, u32[]{:S(2)}, u32[]{:S(2)}) collective-permute-start(bf16[16,1536]{1,0:T(8,128)(2,1)S(1)} %get-tuple-element.76.refs_0_), channel_id=1, source_target_pairs={{0,2},{2,0},{4,6},{6,4},{1,3},{3,1},{5,7},{7,5},{8,10},{10,8},{12,... | collective-permute-start | bytes 147464 | tf_op jit(solution)/shard_map/ppermute | solution.py:40
  92.3 1.8 %collective-permute-start.36 = (bf16[16,1536]{1,0:T(8,128)(2,1)S(1)}, bf16[16,1536]{1,0:T(8,128)(2,1)S(1)}, u32[]{:S(2)}, u32[]{:S(2)}) collective-permute-start(bf16[16,1536]{1,0:T(8,128)(2,1)S(1)} %get-tuple-element.76.refs_0_), channel_id=1, source_target_pairs={{0,6},{2,4},{4,2},{6,0},{1,7},{3,5},{5,3},{7,1},{8,14},{10,12},{12... | collective-permute-start | bytes 147464 | tf_op jit(solution)/shard_map/ppermute | solution.py:40
  96.9 1.8 %collective-permute-start.33 = (bf16[16,1280]{1,0:T(8,128)(2,1)S(1)}, bf16[16,1280]{1,0:T(8,128)(2,1)S(1)}, u32[]{:S(2)}, u32[]{:S(2)}) collective-permute-start(bf16[16,1280]{1,0:T(8,128)(2,1)S(1)} %hidden_more.3.refs_0_), channel_id=1, source_target_pairs={{0,6},{2,4},{4,2},{6,0},{1,7},{3,5},{5,3},{7,1},{8,14},{10,12},{12... | collective-permute-start | bytes 122888 | tf_op jit(solution)/shard_map/ppermute | solution.py:40
  100.3 2.4 %collective-permute-done.33.refs_3_ = bf16[16,1280]{1,0:T(8,128)(2,1)S(1)} collective-permute-done((bf16[16,1280]{1,0:T(8,128)(2,1)S(1)}, bf16[16,1280]{1,0:T(8,128)(2,1)S(1)}, u32[]{:S(2)}, u32[]{:S(2)}) %collective-permute-start.33) | collective-permute-done | bytes 40992 | tf_op jit(solution)/shard_map/ppermute | solution.py:40
  105.2 2.1 %collective-permute-done.38.refs_3_ = bf16[16,1024]{1,0:T(8,128)(2,1)S(1)} collective-permute-done((bf16[16,1024]{1,0:T(8,128)(2,1)S(1)}, bf16[16,1024]{1,0:T(8,128)(2,1)S(1)}, u32[]{:S(2)}, u32[]{:S(2)}) %collective-permute-start.38) | collective-permute-done | bytes 32800 | tf_op jit(solution)/shard_map/ppermute | solution.py:40
  (122 shorter events, 39.7 us)
Async XLA Ops:
  0.7 7.6 %collective-permute-start = (bf16[16,1024]{1,0:T(8,128)(2,1)}, bf16[16,1024]{1,0:T(8,128)(2,1)S(1)}, u32[]{:S(2)}, u32[]{:S(2)}) collective-permute-start(bf16[16,1024]{1,0:T(8,128)(2,1)} %refs_0_.3), channel_id=1, source_target_pairs={{0,1},{1,0},{8,9},{9,8},{2,3},{3,2},{10,11},{11,10},{4,5},{5,4},{1... | collective-permute-start | bytes 98312 | tf_op jit(solution)/shard_map/ppermute | solution.py:40
  1.2 7.0 %collective-permute-start.1 = (bf16[16,1024]{1,0:T(8,128)(2,1)}, bf16[16,1024]{1,0:T(8,128)(2,1)S(1)}, u32[]{:S(2)}, u32[]{:S(2)}) collective-permute-start(bf16[16,1024]{1,0:T(8,128)(2,1)} %refs_0_.3), channel_id=1, source_target_pairs={{0,8},{1,9},{8,0},{9,1},{2,10},{3,11},{10,2},{11,3},{4,12},{5,13},... | collective-permute-start | bytes 98312 | tf_op jit(solution)/shard_map/ppermute | solution.py:40
  9.5 10.0 %collective-permute-start.6 = (bf16[16,3200]{1,0:T(8,128)(2,1)S(1)}, bf16[16,3200]{1,0:T(8,128)(2,1)S(1)}, u32[]{:S(2)}, u32[]{:S(2)}) collective-permute-start(bf16[16,3200]{1,0:T(8,128)(2,1)S(1)} %get-tuple-element.51), channel_id=1, source_target_pairs={{0,2},{2,0},{4,6},{6,4},{1,3},{3,1},{5,7},{7,5},{8,10},{10,8},{12,... | collective-permute-start | bytes 307208 | tf_op jit(solution)/shard_map/ppermute | solution.py:40
  11.4 11.1 %collective-permute-start.7 = (bf16[16,3200]{1,0:T(8,128)(2,1)S(1)}, bf16[16,3200]{1,0:T(8,128)(2,1)S(1)}, u32[]{:S(2)}, u32[]{:S(2)}) collective-permute-start(bf16[16,3200]{1,0:T(8,128)(2,1)S(1)} %get-tuple-element.52), channel_id=1, source_target_pairs={{0,4},{2,6},{4,0},{6,2},{1,5},{3,7},{5,1},{7,3},{8,12},{10,14},{12... | collective-permute-start | bytes 307208 | tf_op jit(solution)/shard_map/ppermute | solution.py:40
  14.0 8.5 %collective-permute-start.8 = (bf16[16,3200]{1,0:T(8,128)(2,1)S(1)}, bf16[16,3200]{1,0:T(8,128)(2,1)S(1)}, u32[]{:S(2)}, u32[]{:S(2)}) collective-permute-start(bf16[16,3200]{1,0:T(8,128)(2,1)S(1)} %get-tuple-element.53), channel_id=1, source_target_pairs={{0,6},{2,4},{4,2},{6,0},{1,7},{3,5},{5,3},{7,1},{8,14},{10,12},{12... | collective-permute-start | bytes 307208 | tf_op jit(solution)/shard_map/ppermute | solution.py:40
  15.0 15.1 %collective-permute-start.3 = (bf16[16,2560]{1,0:T(8,128)(2,1)S(1)}, bf16[16,2560]{1,0:T(8,128)(2,1)S(1)}, u32[]{:S(2)}, u32[]{:S(2)}) collective-permute-start(bf16[16,2560]{1,0:T(8,128)(2,1)S(1)} %get-tuple-element.47), channel_id=1, source_target_pairs={{0,2},{2,0},{4,6},{6,4},{1,3},{3,1},{5,7},{7,5},{8,10},{10,8},{12,... | collective-permute-start | bytes 245768 | tf_op jit(solution)/shard_map/ppermute | solution.py:40
  16.0 15.5 %collective-permute-start.4 = (bf16[16,2560]{1,0:T(8,128)(2,1)S(1)}, bf16[16,2560]{1,0:T(8,128)(2,1)S(1)}, u32[]{:S(2)}, u32[]{:S(2)}) collective-permute-start(bf16[16,2560]{1,0:T(8,128)(2,1)S(1)} %get-tuple-element.48), channel_id=1, source_target_pairs={{0,4},{2,6},{4,0},{6,2},{1,5},{3,7},{5,1},{7,3},{8,12},{10,14},{12... | collective-permute-start | bytes 245768 | tf_op jit(solution)/shard_map/ppermute | solution.py:40
  19.5 12.0 %collective-permute-start.5 = (bf16[16,2560]{1,0:T(8,128)(2,1)S(1)}, bf16[16,2560]{1,0:T(8,128)(2,1)S(1)}, u32[]{:S(2)}, u32[]{:S(2)}) collective-permute-start(bf16[16,2560]{1,0:T(8,128)(2,1)S(1)} %get-tuple-element.49), channel_id=1, source_target_pairs={{0,6},{2,4},{4,2},{6,0},{1,7},{3,5},{5,3},{7,1},{8,14},{10,12},{12... | collective-permute-start | bytes 245768 | tf_op jit(solution)/shard_map/ppermute | solution.py:40
  22.6 12.4 %collective-permute-start.12 = (bf16[16,1536]{1,0:T(8,128)(2,1)S(1)}, bf16[16,1536]{1,0:T(8,128)(2,1)S(1)}, u32[]{:S(2)}, u32[]{:S(2)}) collective-permute-start(bf16[16,1536]{1,0:T(8,128)(2,1)S(1)} %get-tuple-element.55.refs_0_), channel_id=1, source_target_pairs={{0,2},{2,0},{4,6},{6,4},{1,3},{3,1},{5,7},{7,5},{8,10},{10,8},{12,... | collective-permute-start | bytes 147464 | tf_op jit(solution)/shard_map/ppermute | solution.py:40
  29.0 6.5 %collective-permute-start.13 = (bf16[16,1536]{1,0:T(8,128)(2,1)S(1)}, bf16[16,1536]{1,0:T(8,128)(2,1)S(1)}, u32[]{:S(2)}, u32[]{:S(2)}) collective-permute-start(bf16[16,1536]{1,0:T(8,128)(2,1)S(1)} %get-tuple-element.55.refs_0_), channel_id=1, source_target_pairs={{0,4},{2,6},{4,0},{6,2},{1,5},{3,7},{5,1},{7,3},{8,12},{10,14},{12... | collective-permute-start | bytes 147464 | tf_op jit(solution)/shard_map/ppermute | solution.py:40
  30.1 6.3 %collective-permute-start.14 = (bf16[16,1536]{1,0:T(8,128)(2,1)S(1)}, bf16[16,1536]{1,0:T(8,128)(2,1)S(1)}, u32[]{:S(2)}, u32[]{:S(2)}) collective-permute-start(bf16[16,1536]{1,0:T(8,128)(2,1)S(1)} %get-tuple-element.55.refs_0_), channel_id=1, source_target_pairs={{0,6},{2,4},{4,2},{6,0},{1,7},{3,5},{5,3},{7,1},{8,14},{10,12},{12... | collective-permute-start | bytes 147464 | tf_op jit(solution)/shard_map/ppermute | solution.py:40
  31.7 6.1 %collective-permute-start.10 = (bf16[16,1280]{1,0:T(8,128)(2,1)S(1)}, bf16[16,1280]{1,0:T(8,128)(2,1)S(1)}, u32[]{:S(2)}, u32[]{:S(2)}) collective-permute-start(bf16[16,1280]{1,0:T(8,128)(2,1)S(1)} %hidden_more.2.refs_0_), channel_id=1, source_target_pairs={{0,4},{2,6},{4,0},{6,2},{1,5},{3,7},{5,1},{7,3},{8,12},{10,14},{12... | collective-permute-start | bytes 122888 | tf_op jit(solution)/shard_map/ppermute | solution.py:40
  47.8 7.7 %collective-permute-start.18 = (bf16[16,1920]{1,0:T(8,128)(2,1)S(1)}, bf16[16,1920]{1,0:T(8,128)(2,1)S(1)}, u32[]{:S(2)}, u32[]{:S(2)}) collective-permute-start(bf16[16,1920]{1,0:T(8,128)(2,1)S(1)} %get-tuple-element.59), channel_id=1, source_target_pairs={{0,4},{2,6},{4,0},{6,2},{1,5},{3,7},{5,1},{7,3},{8,12},{10,14},{12... | collective-permute-start | bytes 184328 | tf_op jit(solution)/shard_map/ppermute | solution.py:40
  50.4 6.1 %collective-permute-start.19 = (bf16[16,1920]{1,0:T(8,128)(2,1)S(1)}, bf16[16,1920]{1,0:T(8,128)(2,1)S(1)}, u32[]{:S(2)}, u32[]{:S(2)}) collective-permute-start(bf16[16,1920]{1,0:T(8,128)(2,1)S(1)} %get-tuple-element.60), channel_id=1, source_target_pairs={{0,6},{2,4},{4,2},{6,0},{1,7},{3,5},{5,3},{7,1},{8,14},{10,12},{12... | collective-permute-start | bytes 184328 | tf_op jit(solution)/shard_map/ppermute | solution.py:40
  58.0 7.1 %collective-permute-start.20 = (bf16[16,512]{1,0:T(8,128)(2,1)S(1)}, bf16[16,512]{1,0:T(8,128)(2,1)S(1)}, u32[]{:S(2)}, u32[]{:S(2)}) collective-permute-start(bf16[16,512]{1,0:T(8,128)(2,1)S(1)} %get-tuple-element.61.refs_0_), channel_id=1, source_target_pairs={{0,2},{2,0},{4,6},{6,4},{1,3},{3,1},{5,7},{7,5},{8,10},{10,8},{12,... | collective-permute-start | bytes 49160 | tf_op jit(solution)/shard_map/ppermute | solution.py:40
  74.0 8.1 %collective-permute-start.28 = (bf16[16,3200]{1,0:T(8,128)(2,1)S(1)}, bf16[16,3200]{1,0:T(8,128)(2,1)S(1)}, u32[]{:S(2)}, u32[]{:S(2)}) collective-permute-start(bf16[16,3200]{1,0:T(8,128)(2,1)S(1)} %get-tuple-element.72), channel_id=1, source_target_pairs={{0,2},{2,0},{4,6},{6,4},{1,3},{3,1},{5,7},{7,5},{8,10},{10,8},{12,... | collective-permute-start | bytes 307208 | tf_op jit(solution)/shard_map/ppermute | solution.py:40
  74.0 11.6 %collective-permute-start.29 = (bf16[16,3200]{1,0:T(8,128)(2,1)S(1)}, bf16[16,3200]{1,0:T(8,128)(2,1)S(1)}, u32[]{:S(2)}, u32[]{:S(2)}) collective-permute-start(bf16[16,3200]{1,0:T(8,128)(2,1)S(1)} %get-tuple-element.73), channel_id=1, source_target_pairs={{0,4},{2,6},{4,0},{6,2},{1,5},{3,7},{5,1},{7,3},{8,12},{10,14},{12... | collective-permute-start | bytes 307208 | tf_op jit(solution)/shard_map/ppermute | solution.py:40
  76.6 9.1 %collective-permute-start.30 = (bf16[16,3200]{1,0:T(8,128)(2,1)S(1)}, bf16[16,3200]{1,0:T(8,128)(2,1)S(1)}, u32[]{:S(2)}, u32[]{:S(2)}) collective-permute-start(bf16[16,3200]{1,0:T(8,128)(2,1)S(1)} %get-tuple-element.74), channel_id=1, source_target_pairs={{0,6},{2,4},{4,2},{6,0},{1,7},{3,5},{5,3},{7,1},{8,14},{10,12},{12... | collective-permute-start | bytes 307208 | tf_op jit(solution)/shard_map/ppermute | solution.py:40
  79.4 12.9 %collective-permute-start.25 = (bf16[16,2560]{1,0:T(8,128)(2,1)S(1)}, bf16[16,2560]{1,0:T(8,128)(2,1)S(1)}, u32[]{:S(2)}, u32[]{:S(2)}) collective-permute-start(bf16[16,2560]{1,0:T(8,128)(2,1)S(1)} %get-tuple-element.68), channel_id=1, source_target_pairs={{0,2},{2,0},{4,6},{6,4},{1,3},{3,1},{5,7},{7,5},{8,10},{10,8},{12,... | collective-permute-start | bytes 245768 | tf_op jit(solution)/shard_map/ppermute | solution.py:40
  79.5 14.6 %collective-permute-start.26 = (bf16[16,2560]{1,0:T(8,128)(2,1)S(1)}, bf16[16,2560]{1,0:T(8,128)(2,1)S(1)}, u32[]{:S(2)}, u32[]{:S(2)}) collective-permute-start(bf16[16,2560]{1,0:T(8,128)(2,1)S(1)} %get-tuple-element.69), channel_id=1, source_target_pairs={{0,4},{2,6},{4,0},{6,2},{1,5},{3,7},{5,1},{7,3},{8,12},{10,14},{12... | collective-permute-start | bytes 245768 | tf_op jit(solution)/shard_map/ppermute | solution.py:40
  82.1 12.1 %collective-permute-start.27 = (bf16[16,2560]{1,0:T(8,128)(2,1)S(1)}, bf16[16,2560]{1,0:T(8,128)(2,1)S(1)}, u32[]{:S(2)}, u32[]{:S(2)}) collective-permute-start(bf16[16,2560]{1,0:T(8,128)(2,1)S(1)} %get-tuple-element.70), channel_id=1, source_target_pairs={{0,6},{2,4},{4,2},{6,0},{1,7},{3,5},{5,3},{7,1},{8,14},{10,12},{12... | collective-permute-start | bytes 245768 | tf_op jit(solution)/shard_map/ppermute | solution.py:40
  85.9 11.1 %collective-permute-start.34 = (bf16[16,1536]{1,0:T(8,128)(2,1)S(1)}, bf16[16,1536]{1,0:T(8,128)(2,1)S(1)}, u32[]{:S(2)}, u32[]{:S(2)}) collective-permute-start(bf16[16,1536]{1,0:T(8,128)(2,1)S(1)} %get-tuple-element.76.refs_0_), channel_id=1, source_target_pairs={{0,2},{2,0},{4,6},{6,4},{1,3},{3,1},{5,7},{7,5},{8,10},{10,8},{12,... | collective-permute-start | bytes 147464 | tf_op jit(solution)/shard_map/ppermute | solution.py:40
  91.7 7.0 %collective-permute-start.35 = (bf16[16,1536]{1,0:T(8,128)(2,1)S(1)}, bf16[16,1536]{1,0:T(8,128)(2,1)S(1)}, u32[]{:S(2)}, u32[]{:S(2)}) collective-permute-start(bf16[16,1536]{1,0:T(8,128)(2,1)S(1)} %get-tuple-element.76.refs_0_), channel_id=1, source_target_pairs={{0,4},{2,6},{4,0},{6,2},{1,5},{3,7},{5,1},{7,3},{8,12},{10,14},{12... | collective-permute-start | bytes 147464 | tf_op jit(solution)/shard_map/ppermute | solution.py:40
  92.3 6.4 %collective-permute-start.36 = (bf16[16,1536]{1,0:T(8,128)(2,1)S(1)}, bf16[16,1536]{1,0:T(8,128)(2,1)S(1)}, u32[]{:S(2)}, u32[]{:S(2)}) collective-permute-start(bf16[16,1536]{1,0:T(8,128)(2,1)S(1)} %get-tuple-element.76.refs_0_), channel_id=1, source_target_pairs={{0,6},{2,4},{4,2},{6,0},{1,7},{3,5},{5,3},{7,1},{8,14},{10,12},{12... | collective-permute-start | bytes 147464 | tf_op jit(solution)/shard_map/ppermute | solution.py:40
  (37 other events, 520.3 us)

commit v4 on v3

--- a/solution.py
+++ b/solution.py
@@ -54,14 +54,15 @@
     return block[:, :1] + block[:, LANES // 2 : LANES // 2 + 1]
 
 
-def fetch_kernel(n_weights, *refs):
+def fetch_kernel(n_weights, first, *refs):
     weights, outs, semaphores = refs[:n_weights], refs[n_weights : 2 * n_weights], refs[-1]
     copies = []
     for weight, out in zip(weights, outs):
         step = weight.shape[0] // FETCH_PIECES
         for piece in range(FETCH_PIECES):
             part = pl.ds(piece * step, step)
-            copies.append(pltpu.make_async_copy(weight.at[part], out.at[part], semaphores.at[len(copies)]))
+            source = weight.at[part, pl.ds(first, out.shape[1])]
+            copies.append(pltpu.make_async_copy(source, out.at[part], semaphores.at[len(copies)]))
             copies[-1].start()
     for copy in copies:
         copy.wait()
@@ -264,6 +265,11 @@
 
 MIB = 1 << 20
 FETCH_PIECES = 4
+NEAR_SHARE = 2
+
+
+def first_chunk(units):
+    return min(-(-units * NEAR_SHARE // 1024) * 256, units)
 
 
 def array_bytes(array):
@@ -341,18 +347,25 @@
     def stack(unit):
         return [pltpu.VMEM((rows, unit), BF16)]
 
-    def mixer(kernel, name, inputs, weights, down_weight, finish, finish_outs, finish_scratch):
-        units = weights[0].shape[1]
-        near = min(-(-units // 2 // 256) * 256, units)
+    def mixer(kernel, name, inputs, weights, more_weights, down_weight, finish, finish_outs, finish_scratch):
+        units = down_weight.shape[0]
+        near = first_chunk(units)
         rest = units - near
         *blocks, stream, scaled = call(
-            functools.partial(kernel, (0, near)),
+            kernel,
             name,
             row_blocks(2 * padded(near) + LANES) + [shape((rows, width), BF16)] * 2,
             (*inputs, *weights),
         )
+        if callable(more_weights):
+            more_weights, columns = more_weights(scaled), None
+        else:
+            columns = (near, rest)
         more = call(
-            functools.partial(more_kernel, (near, rest)), name + "_more", row_blocks(2 * padded(rest)), (scaled, *weights)
+            functools.partial(more_kernel, columns),
+            name + "_more",
+            row_blocks(2 * padded(rest)),
+            (scaled, *more_weights),
         )
         outs = [shape((height, near), BF16), shape((height, LANES), F32)]
         parts = collect(blocks)
@@ -380,24 +393,28 @@
         return call(kernel, name, shape((rows, weight.shape[1]), BF16), inputs, stack(weight.shape[0]), after=after)
 
     arrived = [swap(residual_input, dt, n_dt, k) for k in range(1, n_dt)]
-    fetched = [
-        pltpu.with_memory_space_constraint(w, pltpu.HBM) for w in (leading_gate_weight, leading_up_weight)
-    ]
-    gate, up = call(
-        functools.partial(fetch_kernel, 2),
-        "fetch",
-        [shape(w.shape, w.dtype) for w in fetched],
-        fetched,
-        [pltpu.SemaphoreType.DMA((2 * FETCH_PIECES,))],
-        [pl.BlockSpec(memory_space=pltpu.HBM)] * 2,
-        100000,
-    )
+    def fetch(weights, first, size, after):
+        return call(
+            functools.partial(fetch_kernel, len(weights), first),
+            "fetch",
+            [shape((w.shape[0], size), w.dtype) for w in weights],
+            [pltpu.with_memory_space_constraint(w, pltpu.HBM) for w in weights],
+            [pltpu.SemaphoreType.DMA((len(weights) * FETCH_PIECES,))],
+            [pl.BlockSpec(memory_space=pltpu.HBM)] * len(weights),
+            100000,
+            after,
+        )
+
+    units = leading_gate_weight.shape[1]
+    near = first_chunk(units)
+    first = (leading_gate_weight, leading_up_weight)
     whole_rows = shape((rows, width), BF16)
     gathered, part = mixer(
-        functools.partial(first_kernel, n_dt, n_kv, names),
+        functools.partial(first_kernel, n_dt, n_kv, names, None),
         "first",
         (residual_input, *arrived, leading_norm_gain.reshape(1, width)),
-        (gate, up),
+        fetch(first, 0, near, ()),
+        lambda scaled: fetch(first, near, units - near, (scaled,)),
         leading_down_weight,
         more_down_kernel,
         whole_rows,
@@ -429,11 +446,13 @@
     new_state, finished = call(state_kernel, "state", outs, (upright, value_rows, incoming_state), work=100000)
     parts = total_parts(down(known, output_projector, "attention_out", finished))
 
+    last = (trailing_gate_weight, trailing_up_weight)
     second, parts = mixer(
-        functools.partial(last_kernel, len(parts)),
+        functools.partial(last_kernel, len(parts), (0, near)),
         "last",
         (after_first, *parts, trailing_norm_gain.reshape(1, width)),
-        (trailing_gate_weight, trailing_up_weight),
+        last,
+        last,
         trailing_down_weight,
         lambda n_blocks, first_row, *refs: scatter_down_kernel(n_blocks, first_row, names, *refs),
         [shape((height, width), BF16)] * n_dt,

time: 109 us -> 107 us (0.982)
  waiting for transfers between devices: 29.7 us -> 25.6 us
  Pallas kernels: 17.6 us -> 18.8 us
    ppermute x40, waiting for transfers between devices: 29.7 us -> 25.6 us  [swap(): return lax.ppermute(array, axes, [(i, i ^ offset) for i in range(size)])]
    pallas_call x18 -> x19, Pallas kernels: 17.6 us -> 18.8 us  [call(): pl.pallas_call(body, out_shape=outs, in_specs=(in_specs or [VMEM] * len(i...]
  transfers between devices with their start and end apart: 40 -> 40, of which waited for: 18 -> 16; matrix products, arithmetic and copies ran while one was open for 0% -> 0% of each run, Pallas kernels for 10% -> 11%
where the time goes in v4:
time: 107 us
  starting transfers between devices  61.3 us (57%)
  waiting for transfers between devices  25.6 us (24%)
  Pallas kernels  18.8 us (18%)
  between operations  1.1 us (1%)
    ppermute x40, starting transfers between devices, swap(): return lax.ppermute(array, axes, [(i, i ^ offset) for i in range(size)])  61.3 us
    ppermute x40, waiting for transfers between devices, swap(): return lax.ppermute(array, axes, [(i, i ^ offset) for i in range(size)])  25.6 us
    pallas_call x19, Pallas kernels, call(): pl.pallas_call(body, out_shape=outs, in_specs=(in_specs or [VMEM] * len(i...  18.8 us
  transfers between devices with their start and end apart: 40, of which 16 were waited for; matrix products, arithmetic and copies ran while one was open for 0% of the time, Pallas kernels for 11%

profile of v4, /device:TPU:0, one launch (start us, length us, event | category | flops | bytes accessed | tf_op | source)
XLA Modules:
  0.0 107.0 jit_solution(14950110580944278628)
XLA Ops:
  0.6 3.0 %collective-permute-start.1 = (bf16[16,1024]{1,0:T(8,128)(2,1)}, bf16[16,1024]{1,0:T(8,128)(2,1)S(1)}, u32[]{:S(2)}, u32[]{:S(2)}) collective-permute-start(bf16[16,1024]{1,0:T(8,128)(2,1)} %refs_0_.4), channel_id=1, source_target_pairs={{0,8},{1,9},{8,0},{9,1},{2,10},{3,11},{10,2},{11,3},{4,12},{5,13},... | collective-permute-start | bytes 98312 | tf_op jit(solution)/shard_map/ppermute | solution.py:40
  3.9 2.9 %fetch.2 = (bf16[1024,1536]{1,0:T(8,128)(2,1)S(1)}, bf16[1024,1536]{1,0:T(8,128)(2,1)S(1)}) custom-call(bf16[1024,2816]{1,0:T(8,128)(2,1)} %refs_0_.5, bf16[1024,2816]{1,0:T(8,128)(2,1)} %refs_1_.4), custom_call_target="tpu_custom_call" | custom-call | flops 100000 | tf_op jit(solution)/shard_map/fetch/pallas_call | solution.py:289
  10.1 2.6 %collective-permute-start.7 = (bf16[16,3200]{1,0:T(8,128)(2,1)S(1)}, bf16[16,3200]{1,0:T(8,128)(2,1)S(1)}, u32[]{:S(2)}, u32[]{:S(2)}) collective-permute-start(bf16[16,3200]{1,0:T(8,128)(2,1)S(1)} %get-tuple-element.56), channel_id=1, source_target_pairs={{0,4},{2,6},{4,0},{6,2},{1,5},{3,7},{5,1},{7,3},{8,12},{10,14},{12... | collective-permute-start | bytes 307208 | tf_op jit(solution)/shard_map/ppermute | solution.py:40
  12.9 2.7 %fetch.3 = (bf16[1024,1280]{1,0:T(8,128)(2,1)S(1)}, bf16[1024,1280]{1,0:T(8,128)(2,1)S(1)}) custom-call(bf16[1024,2816]{1,0:T(8,128)(2,1)} %refs_0_.5, bf16[1024,2816]{1,0:T(8,128)(2,1)} %refs_1_.4, bf16[64,1024]{1,0:T(8,128)(2,1)S(1)} %get-tuple-element.47.refs_2_.refs_0_), custom_call_target="tpu_custom_call" | custom-call | flops 100000 | tf_op jit(solution)/shard_map/fetch/pallas_call | solution.py:289
  17.4 3.5 %collective-permute-start.4 = (bf16[16,2560]{1,0:T(8,128)(2,1)S(1)}, bf16[16,2560]{1,0:T(8,128)(2,1)S(1)}, u32[]{:S(2)}, u32[]{:S(2)}) collective-permute-start(bf16[16,2560]{1,0:T(8,128)(2,1)S(1)} %get-tuple-element.52), channel_id=1, source_target_pairs={{0,4},{2,6},{4,0},{6,2},{1,5},{3,7},{5,1},{7,3},{8,12},{10,14},{12... | collective-permute-start | bytes 245768 | tf_op jit(solution)/shard_map/ppermute | solution.py:40
  21.3 3.6 %collective-permute-start.14 = (bf16[16,1536]{1,0:T(8,128)(2,1)S(1)}, bf16[16,1536]{1,0:T(8,128)(2,1)S(1)}, u32[]{:S(2)}, u32[]{:S(2)}) collective-permute-start(bf16[16,1536]{1,0:T(8,128)(2,1)S(1)} %get-tuple-element.59.refs_0_), channel_id=1, source_target_pairs={{0,6},{2,4},{4,2},{6,0},{1,7},{3,5},{5,3},{7,1},{8,14},{10,12},{12... | collective-permute-start | bytes 147464 | tf_op jit(solution)/shard_map/ppermute | solution.py:40
  25.0 5.7 %collective-permute-start.13 = (bf16[16,1536]{1,0:T(8,128)(2,1)S(1)}, bf16[16,1536]{1,0:T(8,128)(2,1)S(1)}, u32[]{:S(2)}, u32[]{:S(2)}) collective-permute-start(bf16[16,1536]{1,0:T(8,128)(2,1)S(1)} %get-tuple-element.59.refs_0_), channel_id=1, source_target_pairs={{0,4},{2,6},{4,0},{6,2},{1,5},{3,7},{5,1},{7,3},{8,12},{10,14},{12... | collective-permute-start | bytes 147464 | tf_op jit(solution)/shard_map/ppermute | solution.py:40
  30.9 2.1 %collective-permute-start.11 = (bf16[16,1280]{1,0:T(8,128)(2,1)S(1)}, bf16[16,1280]{1,0:T(8,128)(2,1)S(1)}, u32[]{:S(2)}, u32[]{:S(2)}) collective-permute-start(bf16[16,1280]{1,0:T(8,128)(2,1)S(1)} %hidden_more.2.refs_0_), channel_id=1, source_target_pairs={{0,6},{2,4},{4,2},{6,0},{1,7},{3,5},{5,3},{7,1},{8,14},{10,12},{12... | collective-permute-start | bytes 122888 | tf_op jit(solution)/shard_map/ppermute | solution.py:40
  40.7 3.4 %collective-permute-done.15 = bf16[64,1024]{1,0:T(8,128)(2,1)S(1)} collective-permute-done((bf16[64,1024]{1,0:T(8,128)(2,1)S(1)}, bf16[64,1024]{1,0:T(8,128)(2,1)S(1)}, u32[]{:S(2)}, u32[]{:S(2)}) %collective-permute-start.15) | collective-permute-done | bytes 131104 | tf_op jit(solution)/shard_map/ppermute | solution.py:40
  47.3 1.9 %collective-permute-start.18 = (bf16[16,1920]{1,0:T(8,128)(2,1)S(1)}, bf16[16,1920]{1,0:T(8,128)(2,1)S(1)}, u32[]{:S(2)}, u32[]{:S(2)}) collective-permute-start(bf16[16,1920]{1,0:T(8,128)(2,1)S(1)} %get-tuple-element.63), channel_id=1, source_target_pairs={{0,4},{2,6},{4,0},{6,2},{1,5},{3,7},{5,1},{7,3},{8,12},{10,14},{12... | collective-permute-start | bytes 184328 | tf_op jit(solution)/shard_map/ppermute | solution.py:40
  50.8 3.9 %collective-permute-done.18.refs_2_ = bf16[16,1920]{1,0:T(8,128)(2,1)S(1)} collective-permute-done((bf16[16,1920]{1,0:T(8,128)(2,1)S(1)}, bf16[16,1920]{1,0:T(8,128)(2,1)S(1)}, u32[]{:S(2)}, u32[]{:S(2)}) %collective-permute-start.18) | collective-permute-done | bytes 61472 | tf_op jit(solution)/shard_map/ppermute | solution.py:40
  56.8 1.9 %collective-permute-start.22 = (bf16[16,512]{1,0:T(8,128)(2,1)S(1)}, bf16[16,512]{1,0:T(8,128)(2,1)S(1)}, u32[]{:S(2)}, u32[]{:S(2)}) collective-permute-start(bf16[16,512]{1,0:T(8,128)(2,1)S(1)} %get-tuple-element.65.refs_0_), channel_id=1, source_target_pairs={{0,6},{2,4},{4,2},{6,0},{1,7},{3,5},{5,3},{7,1},{8,14},{10,12},{12... | collective-permute-start | bytes 49160 | tf_op jit(solution)/shard_map/ppermute | solution.py:40
  59.4 1.8 %collective-permute-start.20 = (bf16[16,512]{1,0:T(8,128)(2,1)S(1)}, bf16[16,512]{1,0:T(8,128)(2,1)S(1)}, u32[]{:S(2)}, u32[]{:S(2)}) collective-permute-start(bf16[16,512]{1,0:T(8,128)(2,1)S(1)} %get-tuple-element.65.refs_0_), channel_id=1, source_target_pairs={{0,2},{2,0},{4,6},{6,4},{1,3},{3,1},{5,7},{7,5},{8,10},{10,8},{12,... | collective-permute-start | bytes 49160 | tf_op jit(solution)/shard_map/ppermute | solution.py:40
  61.2 2.7 %state.1 = (f32[16,4,64,128]{3,2,1,0:T(8,128)}, f32[8,128]{1,0:T(8,128)S(1)}) custom-call(f32[256,128]{1,0:T(8,128)S(1)} %get-tuple-element.66.refs_0_, f32[16,512]{1,0:T(8,128)S(1)} %get-tuple-element.67.refs_1_, f32[16,4,64,128]{3,2,1,0:T(8,128)S(1)} %copy-done), custom_call_target="tpu_custom_call" | custom-call | flops 100000 | tf_op jit(solution)/shard_map/state/pallas_call | solution.py:289
  65.7 3.6 %collective-permute-done.23 = bf16[64,1024]{1,0:T(8,128)(2,1)S(1)} collective-permute-done((bf16[64,1024]{1,0:T(8,128)(2,1)S(1)}, bf16[64,1024]{1,0:T(8,128)(2,1)S(1)}, u32[]{:S(2)}, u32[]{:S(2)}) %collective-permute-start.23) | collective-permute-done | bytes 131104 | tf_op jit(solution)/shard_map/ppermute | solution.py:40
  74.5 1.9 %collective-permute-start.30 = (bf16[16,3200]{1,0:T(8,128)(2,1)S(1)}, bf16[16,3200]{1,0:T(8,128)(2,1)S(1)}, u32[]{:S(2)}, u32[]{:S(2)}) collective-permute-start(bf16[16,3200]{1,0:T(8,128)(2,1)S(1)} %get-tuple-element.78), channel_id=1, source_target_pairs={{0,6},{2,4},{4,2},{6,0},{1,7},{3,5},{5,3},{7,1},{8,14},{10,12},{12... | collective-permute-start | bytes 307208 | tf_op jit(solution)/shard_map/ppermute | solution.py:40
  77.7 2.3 %collective-permute-start.26 = (bf16[16,2560]{1,0:T(8,128)(2,1)S(1)}, bf16[16,2560]{1,0:T(8,128)(2,1)S(1)}, u32[]{:S(2)}, u32[]{:S(2)}) collective-permute-start(bf16[16,2560]{1,0:T(8,128)(2,1)S(1)} %get-tuple-element.73), channel_id=1, source_target_pairs={{0,4},{2,6},{4,0},{6,2},{1,5},{3,7},{5,1},{7,3},{8,12},{10,14},{12... | collective-permute-start | bytes 245768 | tf_op jit(solution)/shard_map/ppermute | solution.py:40
  80.0 1.9 %collective-permute-start.27 = (bf16[16,2560]{1,0:T(8,128)(2,1)S(1)}, bf16[16,2560]{1,0:T(8,128)(2,1)S(1)}, u32[]{:S(2)}, u32[]{:S(2)}) collective-permute-start(bf16[16,2560]{1,0:T(8,128)(2,1)S(1)} %get-tuple-element.74), channel_id=1, source_target_pairs={{0,6},{2,4},{4,2},{6,0},{1,7},{3,5},{5,3},{7,1},{8,14},{10,12},{12... | collective-permute-start | bytes 245768 | tf_op jit(solution)/shard_map/ppermute | solution.py:40
  81.9 2.6 %collective-permute-done.29.refs_2_ = bf16[16,3200]{1,0:T(8,128)(2,1)S(1)} collective-permute-done((bf16[16,3200]{1,0:T(8,128)(2,1)S(1)}, bf16[16,3200]{1,0:T(8,128)(2,1)S(1)}, u32[]{:S(2)}, u32[]{:S(2)}) %collective-permute-start.29) | collective-permute-done | bytes 102432 | tf_op jit(solution)/shard_map/ppermute | solution.py:40
  84.7 2.0 %collective-permute-start.36 = (bf16[16,1536]{1,0:T(8,128)(2,1)S(1)}, bf16[16,1536]{1,0:T(8,128)(2,1)S(1)}, u32[]{:S(2)}, u32[]{:S(2)}) collective-permute-start(bf16[16,1536]{1,0:T(8,128)(2,1)S(1)} %get-tuple-element.80.refs_0_), channel_id=1, source_target_pairs={{0,6},{2,4},{4,2},{6,0},{1,7},{3,5},{5,3},{7,1},{8,14},{10,12},{12... | collective-permute-start | bytes 147464 | tf_op jit(solution)/shard_map/ppermute | solution.py:40
  86.7 5.7 %collective-permute-start.35 = (bf16[16,1536]{1,0:T(8,128)(2,1)S(1)}, bf16[16,1536]{1,0:T(8,128)(2,1)S(1)}, u32[]{:S(2)}, u32[]{:S(2)}) collective-permute-start(bf16[16,1536]{1,0:T(8,128)(2,1)S(1)} %get-tuple-element.80.refs_0_), channel_id=1, source_target_pairs={{0,4},{2,6},{4,0},{6,2},{1,5},{3,7},{5,1},{7,3},{8,12},{10,14},{12... | collective-permute-start | bytes 147464 | tf_op jit(solution)/shard_map/ppermute | solution.py:40
  92.5 2.0 %collective-permute-start.33 = (bf16[16,1280]{1,0:T(8,128)(2,1)S(1)}, bf16[16,1280]{1,0:T(8,128)(2,1)S(1)}, u32[]{:S(2)}, u32[]{:S(2)}) collective-permute-start(bf16[16,1280]{1,0:T(8,128)(2,1)S(1)} %hidden_more.3.refs_0_), channel_id=1, source_target_pairs={{0,6},{2,4},{4,2},{6,0},{1,7},{3,5},{5,3},{7,1},{8,14},{10,12},{12... | collective-permute-start | bytes 122888 | tf_op jit(solution)/shard_map/ppermute | solution.py:40
  94.5 2.4 %collective-permute-start.32 = (bf16[16,1280]{1,0:T(8,128)(2,1)S(1)}, bf16[16,1280]{1,0:T(8,128)(2,1)S(1)}, u32[]{:S(2)}, u32[]{:S(2)}) collective-permute-start(bf16[16,1280]{1,0:T(8,128)(2,1)S(1)} %hidden_more.3.refs_0_), channel_id=1, source_target_pairs={{0,4},{2,6},{4,0},{6,2},{1,5},{3,7},{5,1},{7,3},{8,12},{10,14},{12... | collective-permute-start | bytes 122888 | tf_op jit(solution)/shard_map/ppermute | solution.py:40
  103.4 2.1 %collective-permute-done.38.refs_3_ = bf16[16,1024]{1,0:T(8,128)(2,1)S(1)} collective-permute-done((bf16[16,1024]{1,0:T(8,128)(2,1)S(1)}, bf16[16,1024]{1,0:T(8,128)(2,1)S(1)}, u32[]{:S(2)}, u32[]{:S(2)}) %collective-permute-start.38) | collective-permute-done | bytes 32800 | tf_op jit(solution)/shard_map/ppermute | solution.py:40
  (123 shorter events, 37.7 us)
Async XLA Ops:
  0.6 6.1 %collective-permute-start.1 = (bf16[16,1024]{1,0:T(8,128)(2,1)}, bf16[16,1024]{1,0:T(8,128)(2,1)S(1)}, u32[]{:S(2)}, u32[]{:S(2)}) collective-permute-start(bf16[16,1024]{1,0:T(8,128)(2,1)} %refs_0_.4), channel_id=1, source_target_pairs={{0,8},{1,9},{8,0},{9,1},{2,10},{3,11},{10,2},{11,3},{4,12},{5,13},... | collective-permute-start | bytes 98312 | tf_op jit(solution)/shard_map/ppermute | solution.py:40
  8.4 12.4 %collective-permute-start.6 = (bf16[16,3200]{1,0:T(8,128)(2,1)S(1)}, bf16[16,3200]{1,0:T(8,128)(2,1)S(1)}, u32[]{:S(2)}, u32[]{:S(2)}) collective-permute-start(bf16[16,3200]{1,0:T(8,128)(2,1)S(1)} %get-tuple-element.55), channel_id=1, source_target_pairs={{0,2},{2,0},{4,6},{6,4},{1,3},{3,1},{5,7},{7,5},{8,10},{10,8},{12,... | collective-permute-start | bytes 307208 | tf_op jit(solution)/shard_map/ppermute | solution.py:40
  10.1 11.0 %collective-permute-start.7 = (bf16[16,3200]{1,0:T(8,128)(2,1)S(1)}, bf16[16,3200]{1,0:T(8,128)(2,1)S(1)}, u32[]{:S(2)}, u32[]{:S(2)}) collective-permute-start(bf16[16,3200]{1,0:T(8,128)(2,1)S(1)} %get-tuple-element.56), channel_id=1, source_target_pairs={{0,4},{2,6},{4,0},{6,2},{1,5},{3,7},{5,1},{7,3},{8,12},{10,14},{12... | collective-permute-start | bytes 307208 | tf_op jit(solution)/shard_map/ppermute | solution.py:40
  12.7 8.5 %collective-permute-start.8 = (bf16[16,3200]{1,0:T(8,128)(2,1)S(1)}, bf16[16,3200]{1,0:T(8,128)(2,1)S(1)}, u32[]{:S(2)}, u32[]{:S(2)}) collective-permute-start(bf16[16,3200]{1,0:T(8,128)(2,1)S(1)} %get-tuple-element.57), channel_id=1, source_target_pairs={{0,6},{2,4},{4,2},{6,0},{1,7},{3,5},{5,3},{7,1},{8,14},{10,12},{12... | collective-permute-start | bytes 307208 | tf_op jit(solution)/shard_map/ppermute | solution.py:40
  16.6 14.1 %collective-permute-start.3 = (bf16[16,2560]{1,0:T(8,128)(2,1)S(1)}, bf16[16,2560]{1,0:T(8,128)(2,1)S(1)}, u32[]{:S(2)}, u32[]{:S(2)}) collective-permute-start(bf16[16,2560]{1,0:T(8,128)(2,1)S(1)} %get-tuple-element.51), channel_id=1, source_target_pairs={{0,2},{2,0},{4,6},{6,4},{1,3},{3,1},{5,7},{7,5},{8,10},{10,8},{12,... | collective-permute-start | bytes 245768 | tf_op jit(solution)/shard_map/ppermute | solution.py:40
  17.4 13.3 %collective-permute-start.4 = (bf16[16,2560]{1,0:T(8,128)(2,1)S(1)}, bf16[16,2560]{1,0:T(8,128)(2,1)S(1)}, u32[]{:S(2)}, u32[]{:S(2)}) collective-permute-start(bf16[16,2560]{1,0:T(8,128)(2,1)S(1)} %get-tuple-element.52), channel_id=1, source_target_pairs={{0,4},{2,6},{4,0},{6,2},{1,5},{3,7},{5,1},{7,3},{8,12},{10,14},{12... | collective-permute-start | bytes 245768 | tf_op jit(solution)/shard_map/ppermute | solution.py:40
  20.9 9.8 %collective-permute-start.5 = (bf16[16,2560]{1,0:T(8,128)(2,1)S(1)}, bf16[16,2560]{1,0:T(8,128)(2,1)S(1)}, u32[]{:S(2)}, u32[]{:S(2)}) collective-permute-start(bf16[16,2560]{1,0:T(8,128)(2,1)S(1)} %get-tuple-element.53), channel_id=1, source_target_pairs={{0,6},{2,4},{4,2},{6,0},{1,7},{3,5},{5,3},{7,1},{8,14},{10,12},{12... | collective-permute-start | bytes 245768 | tf_op jit(solution)/shard_map/ppermute | solution.py:40
  21.3 13.1 %collective-permute-start.14 = (bf16[16,1536]{1,0:T(8,128)(2,1)S(1)}, bf16[16,1536]{1,0:T(8,128)(2,1)S(1)}, u32[]{:S(2)}, u32[]{:S(2)}) collective-permute-start(bf16[16,1536]{1,0:T(8,128)(2,1)S(1)} %get-tuple-element.59.refs_0_), channel_id=1, source_target_pairs={{0,6},{2,4},{4,2},{6,0},{1,7},{3,5},{5,3},{7,1},{8,14},{10,12},{12... | collective-permute-start | bytes 147464 | tf_op jit(solution)/shard_map/ppermute | solution.py:40
  25.0 10.4 %collective-permute-start.13 = (bf16[16,1536]{1,0:T(8,128)(2,1)S(1)}, bf16[16,1536]{1,0:T(8,128)(2,1)S(1)}, u32[]{:S(2)}, u32[]{:S(2)}) collective-permute-start(bf16[16,1536]{1,0:T(8,128)(2,1)S(1)} %get-tuple-element.59.refs_0_), channel_id=1, source_target_pairs={{0,4},{2,6},{4,0},{6,2},{1,5},{3,7},{5,1},{7,3},{8,12},{10,14},{12... | collective-permute-start | bytes 147464 | tf_op jit(solution)/shard_map/ppermute | solution.py:40
  30.9 6.0 %collective-permute-start.11 = (bf16[16,1280]{1,0:T(8,128)(2,1)S(1)}, bf16[16,1280]{1,0:T(8,128)(2,1)S(1)}, u32[]{:S(2)}, u32[]{:S(2)}) collective-permute-start(bf16[16,1280]{1,0:T(8,128)(2,1)S(1)} %hidden_more.2.refs_0_), channel_id=1, source_target_pairs={{0,6},{2,4},{4,2},{6,0},{1,7},{3,5},{5,3},{7,1},{8,14},{10,12},{12... | collective-permute-start | bytes 122888 | tf_op jit(solution)/shard_map/ppermute | solution.py:40
  47.3 7.3 %collective-permute-start.18 = (bf16[16,1920]{1,0:T(8,128)(2,1)S(1)}, bf16[16,1920]{1,0:T(8,128)(2,1)S(1)}, u32[]{:S(2)}, u32[]{:S(2)}) collective-permute-start(bf16[16,1920]{1,0:T(8,128)(2,1)S(1)} %get-tuple-element.63), channel_id=1, source_target_pairs={{0,4},{2,6},{4,0},{6,2},{1,5},{3,7},{5,1},{7,3},{8,12},{10,14},{12... | collective-permute-start | bytes 184328 | tf_op jit(solution)/shard_map/ppermute | solution.py:40
  49.2 6.1 %collective-permute-start.19 = (bf16[16,1920]{1,0:T(8,128)(2,1)S(1)}, bf16[16,1920]{1,0:T(8,128)(2,1)S(1)}, u32[]{:S(2)}, u32[]{:S(2)}) collective-permute-start(bf16[16,1920]{1,0:T(8,128)(2,1)S(1)} %get-tuple-element.64), channel_id=1, source_target_pairs={{0,6},{2,4},{4,2},{6,0},{1,7},{3,5},{5,3},{7,1},{8,14},{10,12},{12... | collective-permute-start | bytes 184328 | tf_op jit(solution)/shard_map/ppermute | solution.py:40
  56.8 7.1 %collective-permute-start.22 = (bf16[16,512]{1,0:T(8,128)(2,1)S(1)}, bf16[16,512]{1,0:T(8,128)(2,1)S(1)}, u32[]{:S(2)}, u32[]{:S(2)}) collective-permute-start(bf16[16,512]{1,0:T(8,128)(2,1)S(1)} %get-tuple-element.65.refs_0_), channel_id=1, source_target_pairs={{0,6},{2,4},{4,2},{6,0},{1,7},{3,5},{5,3},{7,1},{8,14},{10,12},{12... | collective-permute-start | bytes 49160 | tf_op jit(solution)/shard_map/ppermute | solution.py:40
  58.7 5.1 %collective-permute-start.21 = (bf16[16,512]{1,0:T(8,128)(2,1)S(1)}, bf16[16,512]{1,0:T(8,128)(2,1)S(1)}, u32[]{:S(2)}, u32[]{:S(2)}) collective-permute-start(bf16[16,512]{1,0:T(8,128)(2,1)S(1)} %get-tuple-element.65.refs_0_), channel_id=1, source_target_pairs={{0,4},{2,6},{4,0},{6,2},{1,5},{3,7},{5,1},{7,3},{8,12},{10,14},{12... | collective-permute-start | bytes 49160 | tf_op jit(solution)/shard_map/ppermute | solution.py:40
  72.0 8.0 %collective-permute-start.28 = (bf16[16,3200]{1,0:T(8,128)(2,1)S(1)}, bf16[16,3200]{1,0:T(8,128)(2,1)S(1)}, u32[]{:S(2)}, u32[]{:S(2)}) collective-permute-start(bf16[16,3200]{1,0:T(8,128)(2,1)S(1)} %get-tuple-element.76), channel_id=1, source_target_pairs={{0,2},{2,0},{4,6},{6,4},{1,3},{3,1},{5,7},{7,5},{8,10},{10,8},{12,... | collective-permute-start | bytes 307208 | tf_op jit(solution)/shard_map/ppermute | solution.py:40
  73.1 11.4 %collective-permute-start.29 = (bf16[16,3200]{1,0:T(8,128)(2,1)S(1)}, bf16[16,3200]{1,0:T(8,128)(2,1)S(1)}, u32[]{:S(2)}, u32[]{:S(2)}) collective-permute-start(bf16[16,3200]{1,0:T(8,128)(2,1)S(1)} %get-tuple-element.77), channel_id=1, source_target_pairs={{0,4},{2,6},{4,0},{6,2},{1,5},{3,7},{5,1},{7,3},{8,12},{10,14},{12... | collective-permute-start | bytes 307208 | tf_op jit(solution)/shard_map/ppermute | solution.py:40
  74.5 10.0 %collective-permute-start.30 = (bf16[16,3200]{1,0:T(8,128)(2,1)S(1)}, bf16[16,3200]{1,0:T(8,128)(2,1)S(1)}, u32[]{:S(2)}, u32[]{:S(2)}) collective-permute-start(bf16[16,3200]{1,0:T(8,128)(2,1)S(1)} %get-tuple-element.78), channel_id=1, source_target_pairs={{0,6},{2,4},{4,2},{6,0},{1,7},{3,5},{5,3},{7,1},{8,14},{10,12},{12... | collective-permute-start | bytes 307208 | tf_op jit(solution)/shard_map/ppermute | solution.py:40
  77.5 14.9 %collective-permute-start.25 = (bf16[16,2560]{1,0:T(8,128)(2,1)S(1)}, bf16[16,2560]{1,0:T(8,128)(2,1)S(1)}, u32[]{:S(2)}, u32[]{:S(2)}) collective-permute-start(bf16[16,2560]{1,0:T(8,128)(2,1)S(1)} %get-tuple-element.72), channel_id=1, source_target_pairs={{0,2},{2,0},{4,6},{6,4},{1,3},{3,1},{5,7},{7,5},{8,10},{10,8},{12,... | collective-permute-start | bytes 245768 | tf_op jit(solution)/shard_map/ppermute | solution.py:40
  77.7 14.7 %collective-permute-start.26 = (bf16[16,2560]{1,0:T(8,128)(2,1)S(1)}, bf16[16,2560]{1,0:T(8,128)(2,1)S(1)}, u32[]{:S(2)}, u32[]{:S(2)}) collective-permute-start(bf16[16,2560]{1,0:T(8,128)(2,1)S(1)} %get-tuple-element.73), channel_id=1, source_target_pairs={{0,4},{2,6},{4,0},{6,2},{1,5},{3,7},{5,1},{7,3},{8,12},{10,14},{12... | collective-permute-start | bytes 245768 | tf_op jit(solution)/shard_map/ppermute | solution.py:40
  80.0 12.4 %collective-permute-start.27 = (bf16[16,2560]{1,0:T(8,128)(2,1)S(1)}, bf16[16,2560]{1,0:T(8,128)(2,1)S(1)}, u32[]{:S(2)}, u32[]{:S(2)}) collective-permute-start(bf16[16,2560]{1,0:T(8,128)(2,1)S(1)} %get-tuple-element.74), channel_id=1, source_target_pairs={{0,6},{2,4},{4,2},{6,0},{1,7},{3,5},{5,3},{7,1},{8,14},{10,12},{12... | collective-permute-start | bytes 245768 | tf_op jit(solution)/shard_map/ppermute | solution.py:40
  84.7 12.2 %collective-permute-start.36 = (bf16[16,1536]{1,0:T(8,128)(2,1)S(1)}, bf16[16,1536]{1,0:T(8,128)(2,1)S(1)}, u32[]{:S(2)}, u32[]{:S(2)}) collective-permute-start(bf16[16,1536]{1,0:T(8,128)(2,1)S(1)} %get-tuple-element.80.refs_0_), channel_id=1, source_target_pairs={{0,6},{2,4},{4,2},{6,0},{1,7},{3,5},{5,3},{7,1},{8,14},{10,12},{12... | collective-permute-start | bytes 147464 | tf_op jit(solution)/shard_map/ppermute | solution.py:40
  86.7 12.0 %collective-permute-start.35 = (bf16[16,1536]{1,0:T(8,128)(2,1)S(1)}, bf16[16,1536]{1,0:T(8,128)(2,1)S(1)}, u32[]{:S(2)}, u32[]{:S(2)}) collective-permute-start(bf16[16,1536]{1,0:T(8,128)(2,1)S(1)} %get-tuple-element.80.refs_0_), channel_id=1, source_target_pairs={{0,4},{2,6},{4,0},{6,2},{1,5},{3,7},{5,1},{7,3},{8,12},{10,14},{12... | collective-permute-start | bytes 147464 | tf_op jit(solution)/shard_map/ppermute | solution.py:40
  92.4 6.2 %collective-permute-start.34 = (bf16[16,1536]{1,0:T(8,128)(2,1)S(1)}, bf16[16,1536]{1,0:T(8,128)(2,1)S(1)}, u32[]{:S(2)}, u32[]{:S(2)}) collective-permute-start(bf16[16,1536]{1,0:T(8,128)(2,1)S(1)} %get-tuple-element.80.refs_0_), channel_id=1, source_target_pairs={{0,2},{2,0},{4,6},{6,4},{1,3},{3,1},{5,7},{7,5},{8,10},{10,8},{12,... | collective-permute-start | bytes 147464 | tf_op jit(solution)/shard_map/ppermute | solution.py:40
  92.5 6.8 %collective-permute-start.33 = (bf16[16,1280]{1,0:T(8,128)(2,1)S(1)}, bf16[16,1280]{1,0:T(8,128)(2,1)S(1)}, u32[]{:S(2)}, u32[]{:S(2)}) collective-permute-start(bf16[16,1280]{1,0:T(8,128)(2,1)S(1)} %hidden_more.3.refs_0_), channel_id=1, source_target_pairs={{0,6},{2,4},{4,2},{6,0},{1,7},{3,5},{5,3},{7,1},{8,14},{10,12},{12... | collective-permute-start | bytes 122888 | tf_op jit(solution)/shard_map/ppermute | solution.py:40
  (37 other events, 498.6 us)
